TPU v7x, 512 devices: a whole 4x4x16 slice. The times are simulated.
512 devices in a mesh: fs: 16 (over y, x), tp: 32 (over z, core).
Axes of the slice: x: 4, y: 4, z: 16, core: 2. Of those that a mesh axis runs over, the one named last changes fastest.
Arguments:
- normed: bfloat16 [2048, 49152], P('tp', 'fs'), may hold values from -6 to 6
- key_cot: bfloat16 [2048, 49152], P('tp', 'fs'), may hold values from -6 to 6
- first_map: bfloat16 [2048, 49152], P('tp', 'fs'), may hold values from -6 to 6
- second_map: bfloat16 [2048, 49152], P('tp', 'fs'), may hold values from -6 to 6
- lambdas: float32 [8], replicated, may hold values from 0.3 to 0.8
- factor: bfloat16 [2048, 256], replicated, may hold values from -0.125 to 0.125
- key_master: float32 [2048, 2048], P('fs', 'tp'), may hold values from -0.125 to 0.125
- value_master: float32 [2048, 2048], P('fs', 'tp'), may hold values from -0.125 to 0.125
- key_first: float32 [256, 2048], P('fs', 'tp'), may hold values from -6 to 6
- key_second: float32 [256, 2048], P('fs', 'tp'), may hold values from 0.5 to 2
- value_first: float32 [256, 2048], P('fs', 'tp'), may hold values from -6 to 6
- value_second: float32 [256, 2048], P('fs', 'tp'), may hold values from 0.5 to 2
Outputs:
- key_master_new: float32 [2048, 2048], P('fs', 'tp')
- value_master_new: float32 [2048, 2048], P('fs', 'tp')
- key_copy: bfloat16 [2048, 2048], P(None, 'tp')
- value_copy: bfloat16 [2048, 2048], P(None, 'tp')
- key_first_new: float32 [256, 2048], P('fs', 'tp')
- key_second_new: float32 [256, 2048], P('fs', 'tp')
- value_first_new: float32 [256, 2048], P('fs', 'tp')
- value_second_new: float32 [256, 2048], P('fs', 'tp')
All inputs are finite; a program needn't handle non-finite values.
Results may differ from a plain program's by a relative error of at most 0.0012.
Values may be sent and summed in bfloat16 or wider, within the bound.
No kernel may reach another device: no remote copies, remote signals or barrier semaphores. Data moves between devices by JAX's collectives and lax.ppermute only.
A program may use at most 64 MiB of HBM per device.

v0:
```python
import math

import jax
import jax.numpy as jnp
from jax import lax
from jax.sharding import Mesh
from jax.sharding import PartitionSpec as P

VALUE_DIM = 256
TP = ("tp_0", "tp_1")
FS = ("fs_0", "fs_1")
FS_TP = ("fs_0", "fs_1", "tp_0", "tp_1")


def cut_along(shard, dim, size):
    lengths = shard.shape
    pieces = shard.reshape(*lengths[:dim], size, lengths[dim] // size, *lengths[dim + 1 :])
    return jnp.moveaxis(pieces, dim, 0)


def summed_on_arrival(shard, axis, dim):
    size = lax.axis_size(axis)
    pieces = lax.all_to_all(cut_along(shard, dim, size), axis, 0, 0, tiled=True)
    return jnp.sum(pieces, axis=0)


def sent_to_all(shard, axis):
    size = lax.axis_size(axis)
    return lax.all_to_all(
        jnp.broadcast_to(shard[None], (size, *shard.shape)), axis, 0, 0, tiled=True
    )


def in_order(pieces, dim):
    lengths = list(pieces.shape[1:])
    lengths[dim] *= pieces.shape[0]
    return jnp.moveaxis(pieces, 0, dim).reshape(lengths)


def collect(shard, axis, dim):
    pieces = sent_to_all(shard, axis)
    return in_order(pieces, dim)


def over_axes(shard, axes):
    for axis in axes:
        shard = lax.psum(shard, axis)
    return shard


def local(
    normed,
    key_cot,
    first_map,
    second_map,
    lambdas,
    factor,
    key_master,
    value_master,
    key_first,
    key_second,
    value_first,
    value_second,
):
    width = first_map.shape[0]
    key_width = key_cot.shape[0]
    heads = lambdas.shape[0]
    tok_local = normed.shape[1]
    rows_here = lax.axis_index(TP) * width + lax.iota(jnp.int32, width)
    owners = rows_here // VALUE_DIM
    picked = (owners[:, None] == lax.iota(jnp.int32, heads)[None, :]).astype(jnp.float32)
    row_lambda = jnp.sum(picked * lambdas[None, :], axis=1)
    value_cot = (
        first_map.astype(jnp.float32) - row_lambda[:, None] * second_map.astype(jnp.float32)
    ).astype(jnp.bfloat16)
    cotangents = jnp.concatenate([key_cot, value_cot], axis=0)
    norm_scale = 1.0 / math.sqrt(tok_local * lax.axis_size(FS))
    fs_rows = key_master.shape[0]
    factor_rows = lax.dynamic_slice_in_dim(factor, lax.axis_index(FS) * fs_rows, fs_rows, 0).astype(
        jnp.float32
    )
    term = lax.dot_general(
        lax.all_gather(normed, TP, axis=0, tiled=True),
        cotangents,
        (((1,), (1,)), ((), ())),
        preferred_element_type=jnp.float32,
    )
    gradient = summed_on_arrival(term, FS, 0) * norm_scale
    partial_value = lax.dot_general(
        factor_rows, gradient, (((0,), (0,)), ((), ())), precision=lax.Precision.HIGHEST
    )
    small = summed_on_arrival(partial_value, FS, 0)
    first = jnp.concatenate([key_first, value_first], axis=1)
    second = jnp.concatenate([key_second, value_second], axis=1)
    first_new = 0.8 * first + 0.2 * small
    second_new = 0.9 * second + 0.1 * small * small
    direction = first_new / (jnp.sqrt(second_new) + 1e-06)
    directions = collect(direction, FS, 0)
    raw = jnp.dot(factor_rows, directions, precision=lax.Precision.HIGHEST)
    key_raw = raw[:, :key_width]
    value_raw = raw[:, key_width:]
    squares = (
        over_axes(jnp.sum(key_raw * key_raw), FS_TP),
        over_axes(jnp.sum(value_raw * value_raw), FS_TP),
    )
    key_cells = fs_rows * lax.axis_size(FS) * key_width * lax.axis_size(TP)
    value_cells = fs_rows * lax.axis_size(FS) * width * lax.axis_size(TP)
    key_update = key_raw / jnp.sqrt(squares[0] / key_cells + 0.01)
    value_update = value_raw / jnp.sqrt(squares[1] / value_cells + 0.01)
    key_new = 0.998 * key_master - 0.02 * key_update
    value_new = 0.998 * value_master - 0.02 * value_update
    halves = jnp.concatenate([key_new, value_new], axis=1).astype(jnp.bfloat16)
    copies = collect(halves, FS, 0)
    return (
        key_new,
        value_new,
        copies[:, :key_width],
        copies[:, key_width:],
        first_new[:, :key_width],
        second_new[:, :key_width],
        first_new[:, key_width:],
        second_new[:, key_width:],
    )


def solution(mesh):
    split = Mesh(mesh.devices.reshape(4, 4, 16, 2), ("fs_0", "fs_1", "tp_0", "tp_1"))
    placed = (
        P(TP, FS),
        P(TP, FS),
        P(TP, FS),
        P(TP, FS),
        P(),
        P(),
        P(FS, TP),
        P(FS, TP),
        P(FS, TP),
        P(FS, TP),
        P(FS, TP),
        P(FS, TP),
    )
    return jax.shard_map(
        local,
        mesh=split,
        in_specs=placed,
        out_specs=(
            P(FS, TP),
            P(FS, TP),
            P(None, TP),
            P(None, TP),
            P(FS, TP),
            P(FS, TP),
            P(FS, TP),
            P(FS, TP),
        ),
        check_vma=False,
    )
```

profile of v0, /device:TPU:1, one launch (start us, length us, event | category | flops | bytes accessed | tf_op | source)
XLA Modules:
  0.0 239.1 jit_solution(16993545285375096101)
XLA Ops:
  7.2 0.0 copy-start
  7.2 0.0 copy-start.3
  7.2 0.0 copy-start.5
  7.2 0.0 copy-start.4
  7.2 0.0 copy-start.6
  7.2 0.0 copy-start.1
  7.2 0.0 copy-start.2
  7.2 0.0 all-gather.2.cloned.1.call-start
  7.3 0.7 all-gather.2.cloned.1.call-update
  8.0 0.7 select_reduce_fusion
  8.7 1.3 subtract_convert_fusion
  10.0 92.9 %all-gather.2.cloned.1.call-done = bf16[2048,3072]{1,0:T(8,128)(2,1)} async-done(((bf16[64,3072]{1,0:T(8,128)(2,1)}), bf16[2048,3072]{1,0:T(8,128)(2,1)}) %all-gather.2.cloned.1.call-update) | async-done | bytes 12582928 | tf_op jit(solution)/shard_map/all_gather | solution.py:83
  103.0 9.0 %convolution_bitcast_fusion = f32[16,16,8,128]{3,2,1,0:T(8,128)S(1)} fusion(bf16[2048,3072]{1,0:T(8,128)(2,1)} %all-gather.2.cloned.1.call-done, bf16[64,3072]{1,0:T(8,128)(2,1)S(1)} %subtract_convert_fusion, bf16[64,3072]{1,0:T(8,128)(2,1)} %param.13), kind=kOutput, calls=%fused_computation | convolution fusion | flops 1612185600 | bytes 14417920 | tf_op jit(solution)/shard_map/dot_general | solution.py:82
  112.0 1.1 copy.35
  113.1 6.5 %all-to-all-start = ((f32[16,128,128]{1,2,0:T(8,128)}), f32[16,128,128]{1,2,0:T(8,128)S(1)}, u32[]{:S(2)}, u32[]{:S(2)}) async-start(f32[16,128,128]{1,2,0:T(8,128)} %bitcast.10), calls=%async_computation | async-start | bytes 2097152 | tf_op jit(solution)/shard_map/all_to_all | solution.py:23
  119.6 16.4 %all-to-all-done = f32[16,128,128]{1,2,0:T(8,128)S(1)} async-done(((f32[16,128,128]{1,2,0:T(8,128)}), f32[16,128,128]{1,2,0:T(8,128)S(1)}, u32[]{:S(2)}, u32[]{:S(2)}) %all-to-all-start) | async-done | bytes 1048608 | tf_op jit(solution)/shard_map/all_to_all | solution.py:23
  136.1 0.1 reduce_sum.46
  136.1 0.0 copy-done
  136.1 0.3 fusion.3
  136.4 11.1 %all_to_all.20 = f32[16,16,128]{2,1,0:T(8,128)S(1)} all-to-all(f32[16,16,128]{2,1,0:T(8,128)S(1)} %bitcast.13), channel_id=1, replica_groups=mesh['fs_0'=4,'fs_1'=4,'tp_0'=16,'tp_1'=2] {'fs_0','fs_1'}, dimensions={0} | all-to-all | bytes 262144 | tf_op jit(solution)/shard_map/all_to_all | solution.py:23
  147.6 0.0 copy-done.3
  147.6 0.0 copy-done.5
  147.6 0.0 copy-done.4
  147.6 0.0 copy-done.6
  147.6 0.1 add_divide_fusion
  147.7 9.9 %all_to_all.21 = f32[16,16,128]{2,1,0:T(8,128)S(1)} all-to-all(f32[16,16,128]{2,1,0:T(8,128)S(1)} %broadcast_in_dim.4), channel_id=1, replica_groups=mesh['fs_0'=4,'fs_1'=4,'tp_0'=16,'tp_1'=2] {'fs_0','fs_1'}, dimensions={0} | all-to-all | bytes 262144 | tf_op jit(solution)/shard_map/all_to_all | solution.py:29
  157.6 0.3 fusion.5
  157.9 0.6 multiply_reduce_fusion
  158.5 7.3 %all-reduce.2 = (f32[]{:T(128)}, f32[]{:T(128)}) all-reduce(f32[]{:T(128)} %get-tuple-element.25, f32[]{:T(128)} %get-tuple-element.24), channel_id=1, replica_groups=mesh['fs_0'=4,'fs_1'=4,'tp_0'=16,'tp_1'=2] {'fs_0'}, use_global_device_ids=true, to_apply=%region_4.5 | all-reduce | flops 2 | bytes 16 | tf_op jit(solution)/shard_map/psum | solution.py:47
  165.8 7.5 %all-reduce.1 = (f32[]{:T(128)}, f32[]{:T(128)}) all-reduce(f32[]{:T(128)} %get-tuple-element.30, f32[]{:T(128)} %get-tuple-element.31), channel_id=1, replica_groups=mesh['fs_0'=4,'fs_1'=4,'tp_0'=16,'tp_1'=2] {'fs_1'}, use_global_device_ids=true, to_apply=%region_5.6 | all-reduce | flops 2 | bytes 16 | tf_op jit(solution)/shard_map/psum | solution.py:47
  173.3 22.4 %all-reduce = (f32[]{:T(128)}, f32[]{:T(128)}) all-reduce(f32[]{:T(128)} %get-tuple-element.28, f32[]{:T(128)} %get-tuple-element.29), channel_id=1, replica_groups=mesh['fs_0'=4,'fs_1'=4,'tp_0'=16,'tp_1'=2] {'tp_0'}, use_global_device_ids=true, to_apply=%region_6.7 | all-reduce | flops 2 | bytes 16 | tf_op jit(solution)/shard_map/psum | solution.py:47
  195.6 16.8 %all-reduce.3 = (f32[]{:T(128)}, f32[]{:T(128)}) all-reduce(f32[]{:T(128)} %get-tuple-element.26, f32[]{:T(128)} %get-tuple-element.27), channel_id=1, replica_groups=mesh['fs_0'=4,'fs_1'=4,'tp_0'=16,'tp_1'=2] {'tp_1'}, use_global_device_ids=true, to_apply=%region_7.8 | all-reduce | flops 2 | bytes 16 | tf_op jit(solution)/shard_map/psum | solution.py:47
  213.8 0.0 copy-done.1
  213.8 0.0 copy-done.2
  213.8 0.6 fusion.16
  214.5 0.9 broadcast_in_dim.5
  215.4 3.6 %all-to-all-start.3 = ((bf16[16,128,128]{1,2,0:T(8,128)(2,1)}), bf16[16,128,128]{1,2,0:T(8,128)(2,1)S(1)}, u32[]{:S(2)}, u32[]{:S(2)}) async-start(bf16[16,128,128]{1,2,0:T(8,128)(2,1)} %broadcast_in_dim.5), calls=%async_computation.3 | async-start | bytes 1048576 | tf_op jit(solution)/shard_map/all_to_all | solution.py:29
  219.0 0.7 fusion.20
  219.6 10.3 %all-to-all-done.3 = bf16[16,128,128]{1,2,0:T(8,128)(2,1)S(1)} async-done(((bf16[16,128,128]{1,2,0:T(8,128)(2,1)}), bf16[16,128,128]{1,2,0:T(8,128)(2,1)S(1)}, u32[]{:S(2)}, u32[]{:S(2)}) %all-to-all-start.3) | async-done | bytes 524320 | tf_op jit(solution)/shard_map/all_to_all | solution.py:29
  229.9 0.3 copy.29
  230.2 0.2 fusion.19
  230.4 0.9 copy.31
  231.3 0.9 copy.30
  (4 shorter events, 0.0 us)
Async XLA Ops:
  7.2 129.0 %copy-start = (bf16[2048,256]{1,0:T(8,128)(2,1)S(1)}, bf16[2048,256]{1,0:T(8,128)(2,1)}, u32[]{:S(2)}) copy-start(bf16[2048,256]{1,0:T(8,128)(2,1)} %param.17) | copy-start | bytes 3145732
  7.2 140.4 %copy-start.3 = (f32[16,64]{1,0:T(8,128)S(1)}, f32[16,64]{1,0:T(8,128)}, u32[]{:S(2)}) copy-start(f32[16,64]{1,0:T(8,128)} %param.23) | copy-start | bytes 12292
  7.2 140.4 %copy-start.5 = (f32[16,64]{1,0:T(8,128)S(1)}, f32[16,64]{1,0:T(8,128)}, u32[]{:S(2)}) copy-start(f32[16,64]{1,0:T(8,128)} %param.22) | copy-start | bytes 12292
  7.2 140.4 %copy-start.4 = (f32[16,64]{1,0:T(8,128)S(1)}, f32[16,64]{1,0:T(8,128)}, u32[]{:S(2)}) copy-start(f32[16,64]{1,0:T(8,128)} %param.21) | copy-start | bytes 12292
  7.2 140.4 %copy-start.6 = (f32[16,64]{1,0:T(8,128)S(1)}, f32[16,64]{1,0:T(8,128)}, u32[]{:S(2)}) copy-start(f32[16,64]{1,0:T(8,128)} %param.20) | copy-start | bytes 12292
  7.2 206.6 %copy-start.1 = (f32[128,64]{0,1:T(8,128)S(1)}, f32[128,64]{0,1:T(8,128)}, u32[]{:S(2)}) copy-start(f32[128,64]{0,1:T(8,128)} %param.19) | copy-start | bytes 98308
  7.2 206.6 %copy-start.2 = (f32[128,64]{0,1:T(8,128)S(1)}, f32[128,64]{0,1:T(8,128)}, u32[]{:S(2)}) copy-start(f32[128,64]{0,1:T(8,128)} %param.18) | copy-start | bytes 98308
  7.2 95.7 %all-gather.2.cloned.1.call-start = ((), (), s32[]{:S(2)}) async-start(), calls=%async_computation.4 | async-start | bytes 12976128 | tf_op jit(solution)/shard_map/all_gather | solution.py:83
  113.1 23.0 %all-to-all-start = ((f32[16,128,128]{1,2,0:T(8,128)}), f32[16,128,128]{1,2,0:T(8,128)S(1)}, u32[]{:S(2)}, u32[]{:S(2)}) async-start(f32[16,128,128]{1,2,0:T(8,128)} %bitcast.10), calls=%async_computation | async-start | bytes 2097152 | tf_op jit(solution)/shard_map/all_to_all | solution.py:23
  215.4 14.5 %all-to-all-start.3 = ((bf16[16,128,128]{1,2,0:T(8,128)(2,1)}), bf16[16,128,128]{1,2,0:T(8,128)(2,1)S(1)}, u32[]{:S(2)}, u32[]{:S(2)}) async-start(bf16[16,128,128]{1,2,0:T(8,128)(2,1)} %broadcast_in_dim.5), calls=%async_computation.3 | async-start | bytes 1048576 | tf_op jit(solution)/shard_map/all_to_all | solution.py:29
Sparse Core Ops, SparseCore 0:
  10.2 92.7 all-gather.1
where the time goes:
time: 240 us; the launch traced here: 239 us
  waiting for transfers between devices  120 us (50%)
  blocking collectives  74.9 us (31%)
  between operations  15.6 us (6%)
  starting transfers between devices  10.1 us (4%)
  matrix products  9.54 us (4%)
  local copies, waits for them, and re-layouts  5 us (2%)
  other arithmetic  3.48 us (1%)
    all_gather x1, waiting for transfers between devices, local(): lax.all_gather(normed, TP, axis=0, tiled=True)  92.9 us
    psum x4, blocking collectives, over_axes(): shard = lax.psum(shard, axis)  53.9 us
    all_to_all x1, waiting for transfers between devices, summed_on_arrival(): pieces = lax.all_to_all(cut_along(shard, dim, size), axis, 0, 0, tiled=True)  16.4 us
    all_to_all x1, blocking collectives, summed_on_arrival(): pieces = lax.all_to_all(cut_along(shard, dim, size), axis, 0, 0, tiled=True)  11.1 us
    all_to_all x1, waiting for transfers between devices, sent_to_all(): lax.all_to_all(jnp.broadcast_to(shard[None], (size, *shard.shape)), axis,...  10.3 us
    all_to_all x1, blocking collectives, sent_to_all(): lax.all_to_all(jnp.broadcast_to(shard[None], (size, *shard.shape)), axis,...  9.93 us
    dot_general x1, matrix products, local(): lax.dot_general(lax.all_gather(normed, TP, axis=0, tiled=True), cotangent...  8.99 us
    all_to_all x1, starting transfers between devices, summed_on_arrival(): pieces = lax.all_to_all(cut_along(shard, dim, size), axis, 0, 0, tiled=True)  6.53 us
  transfers between devices with their start and end apart: 3, of which 3 were waited for; matrix products, arithmetic and copies ran while one was open for 1% of the time, Pallas kernels for 0%

commit v1 on v0

v1 whole, which is shorter than its diff:
```python
import math

import jax
import jax.numpy as jnp
from jax import lax
from jax.sharding import Mesh
from jax.sharding import PartitionSpec as P

VALUE_DIM = 256
TP = ("tp_0", "tp_1")
FS = ("fs_0", "fs_1")
FS_CORE = ("fs_0", "fs_1", "tp_1")
LINK_SCALE = 32.0


def swap(pieces, axes):
    return lax.all_to_all(pieces, axes, 0, 0, tiled=True)


def to_all(shard, axes):
    size = lax.axis_size(axes)
    return swap(jnp.broadcast_to(shard[None], (size, *shard.shape)), axes)


def in_bf16_parts(values, count):
    parts = []
    for _ in range(count):
        part = lax.reduce_precision(values, 8, 7)
        parts.append(part.astype(jnp.bfloat16))
        values = values - part
    return parts


def local(
    normed,
    key_cot,
    first_map,
    second_map,
    lambdas,
    factor,
    key_master,
    value_master,
    key_first,
    key_second,
    value_first,
    value_second,
):
    width, tokens = normed.shape
    cores = lax.axis_size("tp_1")
    chips = lax.axis_size("tp_0")
    fs_size = lax.axis_size(FS)
    rank = factor.shape[1]
    rows = factor.shape[0]
    heads = lambdas.shape[0]
    fs_rows = key_master.shape[0]
    fs_at = lax.axis_index(FS)
    half = tokens // cores
    share = half // chips

    rows_here = lax.axis_index(TP) * width + lax.iota(jnp.int32, width)
    owners = rows_here // VALUE_DIM
    picked = (owners[:, None] == lax.iota(jnp.int32, heads)[None, :]).astype(jnp.float32)
    row_lambda = jnp.sum(picked * lambdas[None, :], axis=1)
    value_cot = (
        first_map.astype(jnp.float32) - row_lambda[:, None] * second_map.astype(jnp.float32)
    ).astype(jnp.bfloat16)

    stacked = jnp.stack([normed, key_cot, value_cot])
    halves = jnp.stack([stacked[:, :, c * half : (c + 1) * half] for c in range(cores)])
    halves = swap(halves, "tp_1")
    features = halves[:, 0].reshape(cores * width, half)
    cots = halves[:, 1:].reshape(cores * 2 * width, half)

    by_token = features.T.reshape(chips, share, cores * width)
    by_token = swap(by_token, "tp_0")
    product = lax.dot_general(
        by_token.transpose(1, 0, 2).reshape(share, rows),
        factor,
        (((1,), (0,)), ((), ())),
        preferred_element_type=jnp.float32,
    )
    masters_here = jnp.concatenate([key_master.T, value_master.T], axis=0)
    masters, product = lax.optimization_barrier((masters_here, product))
    masters = to_all(masters, FS)
    link = (product * LINK_SCALE).astype(jnp.float16)
    link = lax.all_gather(link, "tp_0", axis=0, tiled=True)

    high, low = in_bf16_parts(link.astype(jnp.float32), 2)
    dims = (((0,), (1,)), ((), ()))
    partial = lax.dot_general(high, cots, dims, preferred_element_type=jnp.float32)
    partial = partial + lax.dot_general(low, cots, dims, preferred_element_type=jnp.float32)
    pieces = partial.reshape(fs_size, rank // fs_size, cores, 2 * width)
    pieces = pieces.transpose(0, 2, 1, 3).reshape(fs_size * cores, rank // fs_size, 2 * width)
    masters, pieces = lax.optimization_barrier((masters, pieces))
    norm_scale = 1.0 / (LINK_SCALE * math.sqrt(tokens * fs_size))
    small = jnp.sum(swap(pieces, FS_CORE), axis=0) * norm_scale

    first = jnp.concatenate([key_first, value_first], axis=1)
    second = jnp.concatenate([key_second, value_second], axis=1)
    first_new = 0.8 * first + 0.2 * small
    second_new = 0.9 * second + 0.1 * small * small
    direction = first_new / (jnp.sqrt(second_new) + 1e-06)
    directions = to_all(direction, FS).reshape(rank, 2 * width)

    raw = sum(
        lax.dot_general(part, factor, (((0,), (1,)), ((), ())), preferred_element_type=jnp.float32)
        for part in in_bf16_parts(directions, 3)
    )
    squares = jnp.stack([jnp.sum(raw[:width] * raw[:width]), jnp.sum(raw[width:] * raw[width:])])
    squares = jnp.sum(to_all(squares.reshape(1, 2), TP), axis=(0, 1))
    cells = rows * width * cores * chips
    scales = 0.02 / jnp.sqrt(squares / cells + 0.01)
    row_scale = jnp.repeat(scales, width)[:, None]
    raw_here = lax.dynamic_slice_in_dim(raw, fs_at * fs_rows, fs_rows, 1)
    new_here = 0.998 * masters_here - row_scale * raw_here
    all_masters = masters.transpose(1, 0, 2).reshape(2 * width, rows)
    copies = (0.998 * all_masters - row_scale * raw).astype(jnp.bfloat16)
    return (
        new_here[:width].T,
        new_here[width:].T,
        copies[:width].T,
        copies[width:].T,
        first_new[:, :width],
        second_new[:, :width],
        first_new[:, width:],
        second_new[:, width:],
    )


def solution(mesh):
    split = Mesh(mesh.devices.reshape(4, 4, 16, 2), ("fs_0", "fs_1", "tp_0", "tp_1"))
    placed = (
        P(TP, FS),
        P(TP, FS),
        P(TP, FS),
        P(TP, FS),
        P(),
        P(),
        P(FS, TP),
        P(FS, TP),
        P(FS, TP),
        P(FS, TP),
        P(FS, TP),
        P(FS, TP),
    )
    return jax.shard_map(
        local,
        mesh=split,
        in_specs=placed,
        out_specs=(
            P(FS, TP),
            P(FS, TP),
            P(None, TP),
            P(None, TP),
            P(FS, TP),
            P(FS, TP),
            P(FS, TP),
            P(FS, TP),
        ),
        check_vma=False,
    )
```

time: 240 us -> 146 us (0.61)
  waiting for transfers between devices: 120 us -> 34.6 us
  starting transfers between devices: 10.1 us -> 26.5 us
  between operations: 15.6 us -> 0.92 us
  matrix products: 9.54 us -> 2.57 us
  blocking collectives: 74.9 us -> 68.9 us
    all_gather x1 -> x0, waiting for transfers between devices: 92.9 us -> none  [local(): lax.all_gather(normed, TP, axis=0, tiled=True)]
    psum x4 -> x0, blocking collectives: 53.9 us -> none  [over_axes(): shard = lax.psum(shard, axis)]
    all_gather x0 -> x1, blocking collectives: none -> 32.3 us  [local(): link = lax.all_gather(link, 'tp_0', axis=0, tiled=True)]
    all_to_all x2 -> x4, starting transfers between devices: 10.1 us -> 26.5 us  [swap(): return lax.all_to_all(pieces, axes, 0, 0, tiled=True)]
    all_to_all x2, blocking collectives: 21 us -> 36.6 us  [swap(): return lax.all_to_all(pieces, axes, 0, 0, tiled=True)]
    all_to_all x2 -> x4, waiting for transfers between devices: 26.7 us -> 34.6 us  [swap(): return lax.all_to_all(pieces, axes, 0, 0, tiled=True)]
    dot_general x3 -> x6, matrix products: 9.54 us -> 2.57 us  [the longest x3 1.43 us: local(): lax.dot_general(part, factor, (((0,), (1,)), ((), ())), preferred_element...]
  transfers between devices with their start and end apart: 3 -> 4, of which waited for: 3 -> 3; matrix products, arithmetic and copies ran while one was open for 1% -> 2% of each run, Pallas kernels for 0% -> 0%
where the time goes in v1:
time: 146 us
  blocking collectives  68.9 us (47%)
  waiting for transfers between devices  34.6 us (24%)
  starting transfers between devices  26.5 us (18%)
  local copies, waits for them, and re-layouts  6.93 us (5%)
  other arithmetic  5.04 us (3%)
  matrix products  2.57 us (2%)
    all_to_all x2, blocking collectives, swap(): return lax.all_to_all(pieces, axes, 0, 0, tiled=True)  36.6 us
    all_to_all x4, waiting for transfers between devices, swap(): return lax.all_to_all(pieces, axes, 0, 0, tiled=True)  34.6 us
    all_gather x1, blocking collectives, local(): link = lax.all_gather(link, 'tp_0', axis=0, tiled=True)  32.3 us
    all_to_all x4, starting transfers between devices, swap(): return lax.all_to_all(pieces, axes, 0, 0, tiled=True)  26.5 us
  transfers between devices with their start and end apart: 4, of which 3 were waited for; matrix products, arithmetic and copies ran while one was open for 2% of the time, Pallas kernels for 0%

profile of v1, /device:TPU:1, one launch (start us, length us, event | category | flops | bytes accessed | tf_op | source)
XLA Modules:
  0.0 145.5 jit_solution(858612690182567524)
XLA Ops:
  0.6 0.0 copy-start
  0.6 0.0 copy-start.2
  0.7 0.0 copy-start.3
  0.7 0.9 select_reduce_fusion
  1.6 1.3 fusion.7
  2.9 0.0 copy-done.2
  2.9 0.0 copy-done.3
  2.9 0.1 pad_maximum_fusion
  3.0 0.1 slice_bitcast_fusion.1
  3.1 0.1 pad_maximum_fusion.1
  3.2 11.1 %all_to_all.30 = bf16[2,3,64,1536]{3,2,1,0:T(8,128)(2,1)S(1)} all-to-all(bf16[2,3,64,1536]{3,2,1,0:T(8,128)(2,1)S(1)} %pad_maximum_fusion.1), channel_id=1, replica_groups=mesh['fs_0'=4,'fs_1'=4,'tp_0'=16,'tp_1'=2] {'tp_1'}, dimensions={0} | all-to-all | bytes 2359296 | tf_op jit(solution)/shard_map/all_to_all | solution.py:17
  14.4 0.9 copy.43
  15.3 0.0 copy-start.4
  15.3 0.0 copy-start.5
  15.3 9.7 %all-to-all-start.1 = ((bf16[16,96,128]{2,1,0:T(8,128)(2,1)}), bf16[16,96,128]{2,1,0:T(8,128)(2,1)S(1)}, u32[]{:S(2)}, u32[]{:S(2)}) async-start(bf16[16,96,128]{2,1,0:T(8,128)(2,1)} %bitcast.9), calls=%async_computation.1 | async-start | bytes 786432 | tf_op jit(solution)/shard_map/all_to_all | solution.py:17
  25.1 1.0 slice.61
  26.1 0.0 copy-done.4
  26.1 0.0 copy-done.5
  26.1 16.5 %all-to-all-done.1 = bf16[16,96,128]{2,1,0:T(8,128)(2,1)S(1)} async-done(((bf16[16,96,128]{2,1,0:T(8,128)(2,1)}), bf16[16,96,128]{2,1,0:T(8,128)(2,1)S(1)}, u32[]{:S(2)}, u32[]{:S(2)}) %all-to-all-start.1) | async-done | bytes 393248 | tf_op jit(solution)/shard_map/all_to_all | solution.py:17
  42.5 0.0 copy-done
  42.5 0.3 fusion.8
  42.9 1.1 broadcast_in_dim.8
  43.9 0.0 copy-start.1
  43.9 6.9 %all-to-all-start.2 = ((f32[16,128,128]{2,1,0:T(8,128)}), f32[16,128,128]{2,1,0:T(8,128)S(1)}, u32[]{:S(2)}, u32[]{:S(2)}) async-start(f32[16,128,128]{2,1,0:T(8,128)} %broadcast_in_dim.8), calls=%async_computation.2 | async-start | bytes 2097152 | tf_op jit(solution)/shard_map/all_to_all | solution.py:17
  50.8 32.3 %all_gather.3 = f16[1536,256]{1,0:T(8,128)(2,1)S(1)} all-gather(f16[96,256]{1,0:T(8,128)(2,1)S(1)} %multiply_convert_fusion), channel_id=1, replica_groups=mesh['fs_0'=4,'fs_1'=4,'tp_0'=16,'tp_1'=2] {'tp_0'}, dimensions={0}, use_global_device_ids=true | all-gather | bytes 835584 | tf_op jit(solution)/shard_map/all_gather | solution.py:86
  83.2 0.0 copy-done.1
  83.2 0.4 fusion.4
  83.6 0.4 convolution_add_fusion.2
  84.0 0.0 copy-start.6
  84.0 0.0 copy-start.7
  84.0 0.0 copy-start.8
  84.1 0.0 copy-start.9
  84.1 0.1 reshape.107
  84.2 0.0 all-to-all-done.2
  84.2 25.4 %all_to_all.31 = f32[32,16,128]{2,1,0:T(8,128)S(1)} all-to-all(f32[32,16,128]{2,1,0:T(8,128)S(1)} %bitcast.63), channel_id=1, replica_groups=mesh['fs_0'=4,'fs_1'=4,'tp_0'=16,'tp_1'=2] {'fs_0','fs_1','tp_1'}, dimensions={0} | all-to-all | bytes 524288 | tf_op jit(solution)/shard_map/all_to_all | solution.py:17
  109.7 0.0 copy-done.6
  109.7 0.0 copy-done.7
  109.7 0.0 copy-done.8
  109.7 0.0 copy-done.9
  109.7 0.1 add_divide_fusion
  109.8 0.7 broadcast_in_dim.9
  110.5 3.5 %all-to-all-start.4 = ((f32[16,16,128]{2,1,0:T(8,128)}), f32[16,16,128]{2,1,0:T(8,128)S(1)}, u32[]{:S(2)}, u32[]{:S(2)}) async-start(f32[16,16,128]{2,1,0:T(8,128)} %broadcast_in_dim.9), calls=%async_computation.4 | async-start | bytes 262144 | tf_op jit(solution)/shard_map/all_to_all | solution.py:17
  114.0 7.1 %all-to-all-done.4 = f32[16,16,128]{2,1,0:T(8,128)S(1)} async-done(((f32[16,16,128]{2,1,0:T(8,128)}), f32[16,16,128]{2,1,0:T(8,128)S(1)}, u32[]{:S(2)}, u32[]{:S(2)}) %all-to-all-start.4) | async-done | bytes 131104 | tf_op jit(solution)/shard_map/all_to_all | solution.py:17
  121.2 0.5 fusion.19
  121.7 0.5 convolution_add_fusion.1
  122.1 0.5 convolution_add_fusion
  122.6 0.7 fusion.6
  123.4 1.4 pad_maximum_fusion.3
  124.7 0.6 broadcast_in_dim.10
  125.4 6.4 %all-to-all-start.5 = ((f32[32,1,2]{2,1,0:T(1,128)}), f32[32,1,2]{2,1,0:T(1,128)S(1)}, u32[]{:S(2)}, u32[]{:S(2)}) async-start(f32[32,1,2]{2,1,0:T(1,128)} %broadcast_in_dim.10), calls=%async_computation.5 | async-start | bytes 32768 | tf_op jit(solution)/shard_map/all_to_all | solution.py:17
  131.8 0.7 fusion.17
  132.5 11.1 %all-to-all-done.5 = f32[32,1,2]{2,1,0:T(1,128)S(1)} async-done(((f32[32,1,2]{2,1,0:T(1,128)}), f32[32,1,2]{2,1,0:T(1,128)S(1)}, u32[]{:S(2)}, u32[]{:S(2)}) %all-to-all-start.5) | async-done | bytes 288 | tf_op jit(solution)/shard_map/all_to_all | solution.py:17
  143.5 0.1 reduce_sum.49
  143.6 0.1 broadcast_in_dim.11
  143.7 0.1 mul.156
  143.8 0.2 fusion.2
  144.0 0.1 multiply_subtract_fusion
  144.1 0.6 slice_bitcast_fusion.4
  144.7 0.8 slice_bitcast_fusion.2
  (8 shorter events, 0.2 us)
Async XLA Ops:
  0.6 41.9 %copy-start = (bf16[2048,256]{1,0:T(8,128)(2,1)S(1)}, bf16[2048,256]{1,0:T(8,128)(2,1)}, u32[]{:S(2)}) copy-start(bf16[2048,256]{1,0:T(8,128)(2,1)} %param.17) | copy-start | bytes 3145732
  0.6 2.2 %copy-start.2 = (bf16[64,3072]{1,0:T(8,128)(2,1)S(1)}, bf16[64,3072]{1,0:T(8,128)(2,1)}, u32[]{:S(2)}) copy-start(bf16[64,3072]{1,0:T(8,128)(2,1)} %param.13) | copy-start | bytes 1179652
  0.7 2.2 %copy-start.3 = (bf16[64,3072]{1,0:T(8,128)(2,1)S(1)}, bf16[64,3072]{1,0:T(8,128)(2,1)}, u32[]{:S(2)}) copy-start(bf16[64,3072]{1,0:T(8,128)(2,1)} %param.12) | copy-start | bytes 1179652
  15.3 10.7 %copy-start.4 = (f32[128,64]{0,1:T(8,128)S(1)}, f32[128,64]{0,1:T(8,128)}, u32[]{:S(2)}) copy-start(f32[128,64]{0,1:T(8,128)} %param.19) | copy-start | bytes 98308
  15.3 10.7 %copy-start.5 = (f32[128,64]{0,1:T(8,128)S(1)}, f32[128,64]{0,1:T(8,128)}, u32[]{:S(2)}) copy-start(f32[128,64]{0,1:T(8,128)} %param.18) | copy-start | bytes 98308
  15.3 27.2 %all-to-all-start.1 = ((bf16[16,96,128]{2,1,0:T(8,128)(2,1)}), bf16[16,96,128]{2,1,0:T(8,128)(2,1)S(1)}, u32[]{:S(2)}, u32[]{:S(2)}) async-start(bf16[16,96,128]{2,1,0:T(8,128)(2,1)} %bitcast.9), calls=%async_computation.1 | async-start | bytes 786432 | tf_op jit(solution)/shard_map/all_to_all | solution.py:17
  43.9 39.2 %copy-start.1 = (bf16[2,2,64,1536]{3,2,1,0:T(8,128)(2,1)S(1)}, bf16[2,2,64,1536]{3,2,1,0:T(8,128)(2,1)}, u32[]{:S(2)}) copy-start(bf16[2,2,64,1536]{3,2,1,0:T(8,128)(2,1)} %slice.61) | copy-start | bytes 2359300
  43.9 40.3 %all-to-all-start.2 = ((f32[16,128,128]{2,1,0:T(8,128)}), f32[16,128,128]{2,1,0:T(8,128)S(1)}, u32[]{:S(2)}, u32[]{:S(2)}) async-start(f32[16,128,128]{2,1,0:T(8,128)} %broadcast_in_dim.8), calls=%async_computation.2 | async-start | bytes 2097152 | tf_op jit(solution)/shard_map/all_to_all | solution.py:17
  84.0 25.7 %copy-start.6 = (f32[16,64]{1,0:T(8,128)S(1)}, f32[16,64]{1,0:T(8,128)}, u32[]{:S(2)}) copy-start(f32[16,64]{1,0:T(8,128)} %param.23) | copy-start | bytes 12292
  84.0 25.7 %copy-start.7 = (f32[16,64]{1,0:T(8,128)S(1)}, f32[16,64]{1,0:T(8,128)}, u32[]{:S(2)}) copy-start(f32[16,64]{1,0:T(8,128)} %param.21) | copy-start | bytes 12292
  84.0 25.7 %copy-start.8 = (f32[16,64]{1,0:T(8,128)S(1)}, f32[16,64]{1,0:T(8,128)}, u32[]{:S(2)}) copy-start(f32[16,64]{1,0:T(8,128)} %param.22) | copy-start | bytes 12292
  84.1 25.7 %copy-start.9 = (f32[16,64]{1,0:T(8,128)S(1)}, f32[16,64]{1,0:T(8,128)}, u32[]{:S(2)}) copy-start(f32[16,64]{1,0:T(8,128)} %param.20) | copy-start | bytes 12292
  110.5 10.6 %all-to-all-start.4 = ((f32[16,16,128]{2,1,0:T(8,128)}), f32[16,16,128]{2,1,0:T(8,128)S(1)}, u32[]{:S(2)}, u32[]{:S(2)}) async-start(f32[16,16,128]{2,1,0:T(8,128)} %broadcast_in_dim.9), calls=%async_computation.4 | async-start | bytes 262144 | tf_op jit(solution)/shard_map/all_to_all | solution.py:17
  125.4 18.2 %all-to-all-start.5 = ((f32[32,1,2]{2,1,0:T(1,128)}), f32[32,1,2]{2,1,0:T(1,128)S(1)}, u32[]{:S(2)}, u32[]{:S(2)}) async-start(f32[32,1,2]{2,1,0:T(1,128)} %broadcast_in_dim.10), calls=%async_computation.5 | async-start | bytes 32768 | tf_op jit(solution)/shard_map/all_to_all | solution.py:17

commit v2 on v1

--- a/solution.py
+++ b/solution.py
@@ -3,6 +3,8 @@
 import jax
 import jax.numpy as jnp
 from jax import lax
+from jax.experimental import pallas as pl
+from jax.experimental.pallas import tpu as pltpu
 from jax.sharding import Mesh
 from jax.sharding import PartitionSpec as P
 
@@ -29,6 +31,65 @@
         parts.append(part.astype(jnp.bfloat16))
         values = values - part
     return parts
+
+
+def raw_kernel(directions, factor, raw, squares):
+    values = directions[...].T
+    total = None
+    for _ in range(3):
+        part = values.astype(jnp.bfloat16)
+        values = values - part.astype(jnp.float32)
+        term = lax.dot_general(
+            part, factor[...], (((1,), (1,)), ((), ())), preferred_element_type=jnp.float32
+        )
+        total = term if total is None else total + term
+    raw[...] = total
+    width = total.shape[0] // 2
+    peers = squares.shape[0]
+    for half in range(2):
+        own = total[half * width : (half + 1) * width]
+        block = jnp.full((peers, 4, 128), jnp.sum(own * own), jnp.float32)
+        squares[:, 4 * half : 4 * half + 4, :] = block
+
+
+def raw_and_squares(directions, factor, peers):
+    columns = directions.shape[1]
+    return pl.pallas_call(
+        raw_kernel,
+        out_shape=(
+            jax.ShapeDtypeStruct((columns, factor.shape[0]), jnp.float32),
+            jax.ShapeDtypeStruct((peers, 8, 128), jnp.float32),
+        ),
+        name="raw_and_squares",
+    )(directions, factor)
+
+
+def updated(raw, squares, all_masters, masters_here, fs_at, cells):
+    columns, rows = raw.shape
+    width = columns // 2
+    fs_rows = masters_here.shape[1]
+
+    def kernel(at, raw, squares, all_masters, masters_here, key_new, value_new, key_copy, value_copy):
+        sums = jnp.sum(squares[...], axis=0)
+        start = pl.multiple_of(at[0] * fs_rows, fs_rows)
+        for half, (new, copy) in enumerate(((key_new, key_copy), (value_new, value_copy))):
+            span = slice(half * width, (half + 1) * width)
+            scale = 0.02 / jnp.sqrt(sums[4 * half : 4 * half + 1, 0:1] / cells + 0.01)
+            copy[...] = (0.998 * all_masters[span, :] - scale * raw[span, :]).astype(jnp.bfloat16)
+            new[...] = 0.998 * masters_here[span, :] - scale * raw[span, pl.ds(start, fs_rows)]
+
+    vmem = pl.BlockSpec(memory_space=pltpu.VMEM)
+    return pl.pallas_call(
+        kernel,
+        in_specs=[pl.BlockSpec(memory_space=pltpu.SMEM), vmem, vmem, vmem, vmem],
+        out_shape=(
+            jax.ShapeDtypeStruct((width, fs_rows), jnp.float32),
+            jax.ShapeDtypeStruct((width, fs_rows), jnp.float32),
+            jax.ShapeDtypeStruct((width, rows), jnp.bfloat16),
+            jax.ShapeDtypeStruct((width, rows), jnp.bfloat16),
+        ),
+        name="updated",
+    )(fs_at.reshape(1), raw, squares, all_masters, masters_here)
 
 
 def local(
@@ -61,27 +122,34 @@
     owners = rows_here // VALUE_DIM
     picked = (owners[:, None] == lax.iota(jnp.int32, heads)[None, :]).astype(jnp.float32)
     row_lambda = jnp.sum(picked * lambdas[None, :], axis=1)
+    features = jnp.stack([normed[:, c * half : (c + 1) * half] for c in range(cores)])
+    features = swap(features, "tp_1").reshape(cores * width, half)
+
+    by_token = features.T.reshape(chips, share, cores * width)
+    by_token, first_map, second_map = lax.optimization_barrier((by_token, first_map, second_map))
+    by_token = swap(by_token, "tp_0")
+
     value_cot = (
         first_map.astype(jnp.float32) - row_lambda[:, None] * second_map.astype(jnp.float32)
     ).astype(jnp.bfloat16)
-
-    stacked = jnp.stack([normed, key_cot, value_cot])
-    halves = jnp.stack([stacked[:, :, c * half : (c + 1) * half] for c in range(cores)])
-    halves = swap(halves, "tp_1")
-    features = halves[:, 0].reshape(cores * width, half)
-    cots = halves[:, 1:].reshape(cores * 2 * width, half)
-
-    by_token = features.T.reshape(chips, share, cores * width)
-    by_token = swap(by_token, "tp_0")
+    core = lax.axis_index("tp_1")
+    stacked = jnp.concatenate([key_cot, value_cot], axis=0)
+    kept = lax.dynamic_slice_in_dim(stacked, core * half, half, 1)
+    sent = lax.dynamic_slice_in_dim(stacked, (1 - core) * half, half, 1)
+    masters_here = jnp.concatenate([key_master.T, value_master.T], axis=0)
+    masters = jnp.broadcast_to(masters_here[None], (fs_size, *masters_here.shape))
+    masters, sent = lax.optimization_barrier((masters, sent))
+    came = lax.ppermute(sent, "tp_1", [(0, 1), (1, 0)])
+    cots = jnp.concatenate([jnp.where(core == 0, kept, came), jnp.where(core == 0, came, kept)])
+    cots, by_token = lax.optimization_barrier((cots, by_token))
     product = lax.dot_general(
         by_token.transpose(1, 0, 2).reshape(share, rows),
         factor,
         (((1,), (0,)), ((), ())),
         preferred_element_type=jnp.float32,
     )
-    masters_here = jnp.concatenate([key_master.T, value_master.T], axis=0)
-    masters, product = lax.optimization_barrier((masters_here, product))
-    masters = to_all(masters, FS)
+    masters, product = lax.optimization_barrier((masters, product))
+    masters = swap(masters, FS)
     link = (product * LINK_SCALE).astype(jnp.float16)
     link = lax.all_gather(link, "tp_0", axis=0, tiled=True)
 
@@ -102,24 +170,18 @@
     direction = first_new / (jnp.sqrt(second_new) + 1e-06)
     directions = to_all(direction, FS).reshape(rank, 2 * width)
 
-    raw = sum(
-        lax.dot_general(part, factor, (((0,), (1,)), ((), ())), preferred_element_type=jnp.float32)
-        for part in in_bf16_parts(directions, 3)
-    )
-    squares = jnp.stack([jnp.sum(raw[:width] * raw[:width]), jnp.sum(raw[width:] * raw[width:])])
-    squares = jnp.sum(to_all(squares.reshape(1, 2), TP), axis=(0, 1))
+    raw, squares = raw_and_squares(directions, factor, cores * chips)
+    squares = swap(squares, TP)
     cells = rows * width * cores * chips
-    scales = 0.02 / jnp.sqrt(squares / cells + 0.01)
-    row_scale = jnp.repeat(scales, width)[:, None]
-    raw_here = lax.dynamic_slice_in_dim(raw, fs_at * fs_rows, fs_rows, 1)
-    new_here = 0.998 * masters_here - row_scale * raw_here
     all_masters = masters.transpose(1, 0, 2).reshape(2 * width, rows)
-    copies = (0.998 * all_masters - row_scale * raw).astype(jnp.bfloat16)
+    key_new, value_new, key_copy, value_copy = updated(
+        raw, squares, all_masters, masters_here, fs_at, cells
+    )
     return (
-        new_here[:width].T,
-        new_here[width:].T,
-        copies[:width].T,
-        copies[width:].T,
+        key_new.T,
+        value_new.T,
+        key_copy.T,
+        value_copy.T,
         first_new[:, :width],
         second_new[:, :width],
         first_new[:, width:],

time: 146 us -> 148 us (1.014)
  Pallas kernels: 0 us -> 6.12 us
  other arithmetic: 5.04 us -> 0.71 us
  starting transfers between devices: 26.5 us -> 29 us
    pallas_call x0 -> x2, Pallas kernels: none -> 6.12 us  [the longest x1 3.47 us: raw_and_squares(): pl.pallas_call(raw_kernel, out_shape=(jax.ShapeDtypeStruct((columns, fact...]
    another operation x4 -> x1, other arithmetic: 2.91 us -> 0.04 us  [local(): jnp.stack([normed[:, c * half:(c + 1) * half] for c in range(cores)])]
    ppermute x0 -> x1, starting transfers between devices: none -> 2.55 us  [local(): came = lax.ppermute(sent, 'tp_1', [(0, 1), (1, 0)])]
    broadcast_in_dim x3 -> x1, local copies, waits for them, and re-layouts: 2.37 us -> 0.67 us  [to_all(): return swap(jnp.broadcast_to(shard[None], (size, *shard.shape)), axes)]
    all_to_all x4, waiting for transfers between devices: 34.6 us -> 33.1 us  [swap(): return lax.all_to_all(pieces, axes, 0, 0, tiled=True)]
  transfers between devices with their start and end apart: 4 -> 5, of which waited for: 3 -> 4; matrix products, arithmetic and copies ran while one was open for 2% -> 3% of each run, Pallas kernels for 0% -> 0%
where the time goes in v2:
time: 148 us
  blocking collectives  68.4 us (46%)
  waiting for transfers between devices  34.4 us (23%)
  starting transfers between devices  29 us (20%)
  local copies, waits for them, and re-layouts  7.03 us (5%)
  Pallas kernels  6.12 us (4%)
    all_to_all x2, blocking collectives, swap(): return lax.all_to_all(pieces, axes, 0, 0, tiled=True)  36.1 us
    all_to_all x4, waiting for transfers between devices, swap(): return lax.all_to_all(pieces, axes, 0, 0, tiled=True)  33.1 us
    all_gather x1, blocking collectives, local(): link = lax.all_gather(link, 'tp_0', axis=0, tiled=True)  32.3 us
    all_to_all x4, starting transfers between devices, swap(): return lax.all_to_all(pieces, axes, 0, 0, tiled=True)  26.4 us
    pallas_call x1, Pallas kernels, raw_and_squares(): pl.pallas_call(raw_kernel, out_shape=(jax.ShapeDtypeStruct((columns, fact...  3.47 us
  transfers between devices with their start and end apart: 5, of which 4 were waited for; matrix products, arithmetic and copies ran while one was open for 3% of the time, Pallas kernels for 0%

profile of v2, /device:TPU:1, one launch (start us, length us, event | category | flops | bytes accessed | tf_op | source)
XLA Modules:
  0.0 147.7 jit_solution(14701991101052887948)
XLA Ops:
  0.6 1.0 slice_bitcast_fusion.1
  1.7 0.0 copy-start.13
  1.7 0.0 copy-start.5
  1.8 0.0 copy-start.6
  1.8 10.6 %all_to_all.30 = bf16[2,64,1536]{2,1,0:T(8,128)(2,1)S(1)} all-to-all(bf16[2,64,1536]{2,1,0:T(8,128)(2,1)S(1)} %pad_maximum_fusion.1), channel_id=1, replica_groups=mesh['fs_0'=4,'fs_1'=4,'tp_0'=16,'tp_1'=2] {'tp_1'}, dimensions={0} | all-to-all | bytes 786432 | tf_op jit(solution)/shard_map/all_to_all | solution.py:19
  12.4 0.9 copy.30
  13.4 0.0 copy-start.7
  13.4 0.0 copy-start.8
  13.4 0.0 copy-start.1
  13.4 9.7 %all-to-all-start.1 = ((bf16[16,96,128]{2,1,0:T(8,128)(2,1)}), bf16[16,96,128]{2,1,0:T(8,128)(2,1)S(1)}, u32[]{:S(2)}, u32[]{:S(2)}) async-start(bf16[16,96,128]{2,1,0:T(8,128)(2,1)} %bitcast.7), calls=%async_computation.1 | async-start | bytes 786432 | tf_op jit(solution)/shard_map/all_to_all | solution.py:19
  23.1 0.0 copy-done.13
  23.1 0.1 select_reduce_fusion
  23.2 0.0 copy-done.5
  23.2 0.0 copy-done.6
  23.2 0.2 subtract_convert_fusion
  23.4 0.0 copy-done.7
  23.4 0.0 copy-done.8
  23.4 0.0 copy-done.1
  23.4 0.0 copy-start.2
  23.5 1.1 broadcast_in_dim.4
  24.6 0.0 copy-done.2
  24.6 2.6 %collective-permute-start = (bf16[128,1536]{1,0:T(8,128)(2,1)S(1)}, bf16[128,1536]{1,0:T(8,128)(2,1)S(1)}, u32[]{:S(2)}, u32[]{:S(2)}) collective-permute-start(bf16[128,1536]{1,0:T(8,128)(2,1)S(1)} %fusion.5), channel_id=1, source_target_pairs={{0,1},{1,0},{2,3},{3,2},{4,5},{5,4},{6,7},{7,6},{8,9},{9,8},{10,11... | collective-permute-start | bytes 1179656 | tf_op jit(solution)/shard_map/ppermute | solution.py:142
  27.1 1.3 collective-permute-done
  28.5 0.2 broadcast_select_fusion.1
  28.6 0.0 copy-start
  28.6 0.1 pad_maximum_fusion
  28.7 11.9 %all-to-all-done.1 = bf16[16,96,128]{2,1,0:T(8,128)(2,1)S(1)} async-done(((bf16[16,96,128]{2,1,0:T(8,128)(2,1)}), bf16[16,96,128]{2,1,0:T(8,128)(2,1)S(1)}, u32[]{:S(2)}, u32[]{:S(2)}) %all-to-all-start.1) | async-done | bytes 393248 | tf_op jit(solution)/shard_map/all_to_all | solution.py:19
  40.6 0.0 copy-done
  40.6 0.3 fusion.6
  40.9 6.8 %all-to-all-start.2 = ((f32[16,128,128]{2,1,0:T(8,128)}), f32[16,128,128]{2,1,0:T(8,128)S(1)}, u32[]{:S(2)}, u32[]{:S(2)}) async-start(f32[16,128,128]{2,1,0:T(8,128)} %broadcast_in_dim.4), calls=%async_computation.2 | async-start | bytes 2097152 | tf_op jit(solution)/shard_map/all_to_all | solution.py:19
  47.7 32.3 %all_gather.3 = f16[1536,256]{1,0:T(8,128)(2,1)S(1)} all-gather(f16[96,256]{1,0:T(8,128)(2,1)S(1)} %multiply_convert_fusion), channel_id=1, replica_groups=mesh['fs_0'=4,'fs_1'=4,'tp_0'=16,'tp_1'=2] {'tp_0'}, dimensions={0}, use_global_device_ids=true | all-gather | bytes 835584 | tf_op jit(solution)/shard_map/all_gather | solution.py:154
  80.0 0.4 fusion.3
  80.4 0.4 convolution_add_fusion
  80.8 0.0 copy-start.9
  80.8 0.0 copy-start.10
  80.8 0.0 copy-start.11
  80.8 0.0 copy-start.12
  80.9 0.1 reshape.107
  81.0 0.0 all-to-all-done.2
  81.0 25.4 %all_to_all.31 = f32[32,16,128]{2,1,0:T(8,128)S(1)} all-to-all(f32[32,16,128]{2,1,0:T(8,128)S(1)} %bitcast.37), channel_id=1, replica_groups=mesh['fs_0'=4,'fs_1'=4,'tp_0'=16,'tp_1'=2] {'fs_0','fs_1','tp_1'}, dimensions={0} | all-to-all | bytes 524288 | tf_op jit(solution)/shard_map/all_to_all | solution.py:19
  106.5 0.0 copy-done.9
  106.5 0.0 copy-done.10
  106.5 0.0 copy-done.11
  106.5 0.0 copy-done.12
  106.6 0.1 add_divide_fusion
  106.6 0.7 broadcast_in_dim.5
  107.3 3.5 %all-to-all-start.4 = ((f32[16,16,128]{2,1,0:T(8,128)}), f32[16,16,128]{2,1,0:T(8,128)S(1)}, u32[]{:S(2)}, u32[]{:S(2)}) async-start(f32[16,16,128]{2,1,0:T(8,128)} %broadcast_in_dim.5), calls=%async_computation.4 | async-start | bytes 262144 | tf_op jit(solution)/shard_map/all_to_all | solution.py:19
  110.8 7.1 %all-to-all-done.4 = f32[16,16,128]{2,1,0:T(8,128)S(1)} async-done(((f32[16,16,128]{2,1,0:T(8,128)}), f32[16,16,128]{2,1,0:T(8,128)S(1)}, u32[]{:S(2)}, u32[]{:S(2)}) %all-to-all-start.4) | async-done | bytes 131104 | tf_op jit(solution)/shard_map/all_to_all | solution.py:19
  117.9 0.0 copy-start.3
  117.9 0.7 copy-done.3
  118.6 3.5 %raw_and_squares.1 = (f32[128,2048]{1,0:T(8,128)}, f32[32,8,128]{2,1,0:T(8,128)}) custom-call(f32[256,128]{1,0:T(8,128)} %bitcast.38, bf16[2048,256]{1,0:T(8,128)(2,1)} %factor.1), custom_call_target="tpu_custom_call" | custom-call | tf_op jit(solution)/shard_map/raw_and_squares/pallas_call | solution.py:57
  122.1 6.4 %all-to-all-start.5 = ((f32[32,8,128]{2,1,0:T(8,128)}), f32[32,8,128]{2,1,0:T(8,128)S(1)}, u32[]{:S(2)}, u32[]{:S(2)}) async-start(f32[32,8,128]{2,1,0:T(8,128)} %get-tuple-element.36), calls=%async_computation.5 | async-start | bytes 262144 | tf_op jit(solution)/shard_map/all_to_all | solution.py:19
  128.5 1.1 copy_bitcast_fusion.all_masters
  129.6 0.7 fusion.13
  130.2 14.1 %all-to-all-done.5.squares = f32[32,8,128]{2,1,0:T(8,128)S(1)} async-done(((f32[32,8,128]{2,1,0:T(8,128)}), f32[32,8,128]{2,1,0:T(8,128)S(1)}, u32[]{:S(2)}, u32[]{:S(2)}) %all-to-all-start.5) | async-done | bytes 131104 | tf_op jit(solution)/shard_map/all_to_all | solution.py:19
  144.4 0.0 copy-start.4
  144.4 0.7 copy-done.4
  145.0 2.7 %updated.1 = (f32[64,128]{1,0:T(8,128)}, f32[64,128]{1,0:T(8,128)}, bf16[64,2048]{1,0:T(8,128)(2,1)}, bf16[64,2048]{1,0:T(8,128)(2,1)}) custom-call(s32[1]{0:T(128)} %bitcast.at, f32[128,2048]{1,0:T(8,128)} %get-tuple-element.35.raw, f32[32,8,128]{2,1,0:T(8,128)} %copy-done.4, f32[128,2048]{1,0:T(8,128)} %copy_bitcast_fusion.all_masters, f32[128,128]{1,0:T(8,128)} %copy-done.2), custom_call_target="tpu_custom_call" | custom-call | tf_op jit(solution)/shard_map/updated/pallas_call | solution.py:82
  (7 shorter events, 0.2 us)
Async XLA Ops:
  1.7 21.4 %copy-start.13 = (f32[8]{0:T(128)S(1)}, f32[8]{0:T(128)}, u32[]{:S(2)}) copy-start(f32[8]{0:T(128)} %param.16) | copy-start | bytes 100
  1.7 21.4 %copy-start.5 = (bf16[64,3072]{1,0:T(8,128)(2,1)S(1)}, bf16[64,3072]{1,0:T(8,128)(2,1)}, u32[]{:S(2)}) copy-start(bf16[64,3072]{1,0:T(8,128)(2,1)} %param.15) | copy-start | bytes 1179652
  1.8 21.4 %copy-start.6 = (bf16[64,3072]{1,0:T(8,128)(2,1)S(1)}, bf16[64,3072]{1,0:T(8,128)(2,1)}, u32[]{:S(2)}) copy-start(bf16[64,3072]{1,0:T(8,128)(2,1)} %param.14) | copy-start | bytes 1179652
  13.4 10.0 %copy-start.7 = (f32[128,64]{0,1:T(8,128)S(1)}, f32[128,64]{0,1:T(8,128)}, u32[]{:S(2)}) copy-start(f32[128,64]{0,1:T(8,128)} %param.19) | copy-start | bytes 98308
  13.4 10.0 %copy-start.8 = (f32[128,64]{0,1:T(8,128)S(1)}, f32[128,64]{0,1:T(8,128)}, u32[]{:S(2)}) copy-start(f32[128,64]{0,1:T(8,128)} %param.18) | copy-start | bytes 98308
  13.4 10.1 %copy-start.1 = (bf16[64,3072]{1,0:T(8,128)(2,1)S(1)}, bf16[64,3072]{1,0:T(8,128)(2,1)}, u32[]{:S(2)}) copy-start(bf16[64,3072]{1,0:T(8,128)(2,1)} %param.13) | copy-start | bytes 1179652
  13.4 27.2 %all-to-all-start.1 = ((bf16[16,96,128]{2,1,0:T(8,128)(2,1)}), bf16[16,96,128]{2,1,0:T(8,128)(2,1)S(1)}, u32[]{:S(2)}, u32[]{:S(2)}) async-start(bf16[16,96,128]{2,1,0:T(8,128)(2,1)} %bitcast.7), calls=%async_computation.1 | async-start | bytes 786432 | tf_op jit(solution)/shard_map/all_to_all | solution.py:19
  23.4 1.2 copy-start.2
  24.6 3.9 %collective-permute-start = (bf16[128,1536]{1,0:T(8,128)(2,1)S(1)}, bf16[128,1536]{1,0:T(8,128)(2,1)S(1)}, u32[]{:S(2)}, u32[]{:S(2)}) collective-permute-start(bf16[128,1536]{1,0:T(8,128)(2,1)S(1)} %fusion.5), channel_id=1, source_target_pairs={{0,1},{1,0},{2,3},{3,2},{4,5},{5,4},{6,7},{7,6},{8,9},{9,8},{10,11... | collective-permute-start | bytes 1179656 | tf_op jit(solution)/shard_map/ppermute | solution.py:142
  28.6 11.9 %copy-start = (bf16[2048,256]{1,0:T(8,128)(2,1)S(1)}, bf16[2048,256]{1,0:T(8,128)(2,1)}, u32[]{:S(2)}) copy-start(bf16[2048,256]{1,0:T(8,128)(2,1)} %factor.1) | copy-start | bytes 3145732
  40.9 40.2 %all-to-all-start.2 = ((f32[16,128,128]{2,1,0:T(8,128)}), f32[16,128,128]{2,1,0:T(8,128)S(1)}, u32[]{:S(2)}, u32[]{:S(2)}) async-start(f32[16,128,128]{2,1,0:T(8,128)} %broadcast_in_dim.4), calls=%async_computation.2 | async-start | bytes 2097152 | tf_op jit(solution)/shard_map/all_to_all | solution.py:19
  80.8 25.7 %copy-start.9 = (f32[16,64]{1,0:T(8,128)S(1)}, f32[16,64]{1,0:T(8,128)}, u32[]{:S(2)}) copy-start(f32[16,64]{1,0:T(8,128)} %param.23) | copy-start | bytes 12292
  80.8 25.7 %copy-start.10 = (f32[16,64]{1,0:T(8,128)S(1)}, f32[16,64]{1,0:T(8,128)}, u32[]{:S(2)}) copy-start(f32[16,64]{1,0:T(8,128)} %param.21) | copy-start | bytes 12292
  80.8 25.7 %copy-start.11 = (f32[16,64]{1,0:T(8,128)S(1)}, f32[16,64]{1,0:T(8,128)}, u32[]{:S(2)}) copy-start(f32[16,64]{1,0:T(8,128)} %param.22) | copy-start | bytes 12292
  80.8 25.7 %copy-start.12 = (f32[16,64]{1,0:T(8,128)S(1)}, f32[16,64]{1,0:T(8,128)}, u32[]{:S(2)}) copy-start(f32[16,64]{1,0:T(8,128)} %param.20) | copy-start | bytes 12292
  107.3 10.6 %all-to-all-start.4 = ((f32[16,16,128]{2,1,0:T(8,128)}), f32[16,16,128]{2,1,0:T(8,128)S(1)}, u32[]{:S(2)}, u32[]{:S(2)}) async-start(f32[16,16,128]{2,1,0:T(8,128)} %broadcast_in_dim.5), calls=%async_computation.4 | async-start | bytes 262144 | tf_op jit(solution)/shard_map/all_to_all | solution.py:19
  117.9 0.7 copy-start.3
  122.1 22.3 %all-to-all-start.5 = ((f32[32,8,128]{2,1,0:T(8,128)}), f32[32,8,128]{2,1,0:T(8,128)S(1)}, u32[]{:S(2)}, u32[]{:S(2)}) async-start(f32[32,8,128]{2,1,0:T(8,128)} %get-tuple-element.36), calls=%async_computation.5 | async-start | bytes 262144 | tf_op jit(solution)/shard_map/all_to_all | solution.py:19
  144.4 0.7 copy-start.4

commit v3 on v1

--- a/solution.py
+++ b/solution.py
@@ -3,6 +3,7 @@
 import jax
 import jax.numpy as jnp
 from jax import lax
+from jax.experimental import pallas as pl
 from jax.sharding import Mesh
 from jax.sharding import PartitionSpec as P
 
@@ -31,6 +32,26 @@
     return parts
 
 
+def squares_kernel(directions, gram, squares):
+    values = directions[...]
+    seen = jnp.dot(
+        gram[...], values, precision=lax.Precision.HIGHEST, preferred_element_type=jnp.float32
+    )
+    columns = jnp.sum(values * seen, axis=0, keepdims=True)
+    is_key = lax.broadcasted_iota(jnp.int32, columns.shape, 1) < columns.shape[1] // 2
+    key = jnp.sum(jnp.where(is_key, columns, 0.0))
+    value = jnp.sum(jnp.where(is_key, 0.0, columns))
+    squares[...] = jnp.broadcast_to(jnp.where(is_key, key, value)[None], squares.shape)
+
+
+def squares_of(directions, gram, peers):
+    return pl.pallas_call(
+        squares_kernel,
+        out_shape=jax.ShapeDtypeStruct((peers, 1, directions.shape[1]), jnp.float32),
+        name="squares",
+    )(directions, gram)
+
+
 def local(
     normed,
     key_cot,
@@ -53,7 +74,6 @@
     rows = factor.shape[0]
     heads = lambdas.shape[0]
     fs_rows = key_master.shape[0]
-    fs_at = lax.axis_index(FS)
     half = tokens // cores
     share = half // chips
 
@@ -61,27 +81,38 @@
     owners = rows_here // VALUE_DIM
     picked = (owners[:, None] == lax.iota(jnp.int32, heads)[None, :]).astype(jnp.float32)
     row_lambda = jnp.sum(picked * lambdas[None, :], axis=1)
+    features = jnp.stack([normed[:, c * half : (c + 1) * half] for c in range(cores)])
+    features = swap(features, "tp_1").reshape(cores * width, half)
+
+    by_token = features.T.reshape(chips, share, cores * width)
+    by_token, first_map, second_map = lax.optimization_barrier((by_token, first_map, second_map))
+    by_token = swap(by_token, "tp_0")
+
     value_cot = (
         first_map.astype(jnp.float32) - row_lambda[:, None] * second_map.astype(jnp.float32)
     ).astype(jnp.bfloat16)
-
-    stacked = jnp.stack([normed, key_cot, value_cot])
-    halves = jnp.stack([stacked[:, :, c * half : (c + 1) * half] for c in range(cores)])
-    halves = swap(halves, "tp_1")
-    features = halves[:, 0].reshape(cores * width, half)
-    cots = halves[:, 1:].reshape(cores * 2 * width, half)
-
-    by_token = features.T.reshape(chips, share, cores * width)
-    by_token = swap(by_token, "tp_0")
+    core = lax.axis_index("tp_1")
+    stacked = jnp.concatenate([key_cot, value_cot], axis=0)
+    kept = lax.dynamic_slice_in_dim(stacked, core * half, half, 1)
+    sent = lax.dynamic_slice_in_dim(stacked, (1 - core) * half, half, 1)
+    masters_here = jnp.concatenate([key_master.T, value_master.T], axis=0)
+    masters = jnp.broadcast_to(masters_here[None], (fs_size, *masters_here.shape))
+    gram = lax.dot_general(
+        factor, factor, (((0,), (0,)), ((), ())), preferred_element_type=jnp.float32
+    )
+    fs_at = lax.axis_index(FS) * fs_rows
+    masters, gram, fs_at, sent = lax.optimization_barrier((masters, gram, fs_at, sent))
+    came = lax.ppermute(sent, "tp_1", [(0, 1), (1, 0)])
+    cots = jnp.concatenate([jnp.where(core == 0, kept, came), jnp.where(core == 0, came, kept)])
+    cots, by_token = lax.optimization_barrier((cots, by_token))
     product = lax.dot_general(
         by_token.transpose(1, 0, 2).reshape(share, rows),
         factor,
         (((1,), (0,)), ((), ())),
         preferred_element_type=jnp.float32,
     )
-    masters_here = jnp.concatenate([key_master.T, value_master.T], axis=0)
-    masters, product = lax.optimization_barrier((masters_here, product))
-    masters = to_all(masters, FS)
+    masters, product = lax.optimization_barrier((masters, product))
+    masters = swap(masters, FS)
     link = (product * LINK_SCALE).astype(jnp.float16)
     link = lax.all_gather(link, "tp_0", axis=0, tiled=True)
 
@@ -102,24 +133,26 @@
     direction = first_new / (jnp.sqrt(second_new) + 1e-06)
     directions = to_all(direction, FS).reshape(rank, 2 * width)
 
+    squares = squares_of(directions, gram, cores * chips)
+    squares = jnp.sum(swap(squares, TP), axis=(0, 1))
+    cells = rows * width * cores * chips
+    scales = 0.02 / jnp.sqrt(squares / cells + 0.01)
+
     raw = sum(
         lax.dot_general(part, factor, (((0,), (1,)), ((), ())), preferred_element_type=jnp.float32)
         for part in in_bf16_parts(directions, 3)
     )
-    squares = jnp.stack([jnp.sum(raw[:width] * raw[:width]), jnp.sum(raw[width:] * raw[width:])])
-    squares = jnp.sum(to_all(squares.reshape(1, 2), TP), axis=(0, 1))
-    cells = rows * width * cores * chips
-    scales = 0.02 / jnp.sqrt(squares / cells + 0.01)
-    row_scale = jnp.repeat(scales, width)[:, None]
-    raw_here = lax.dynamic_slice_in_dim(raw, fs_at * fs_rows, fs_rows, 1)
-    new_here = 0.998 * masters_here - row_scale * raw_here
+    raw_here = lax.dynamic_slice_in_dim(raw, fs_at, fs_rows, 1)
     all_masters = masters.transpose(1, 0, 2).reshape(2 * width, rows)
-    copies = (0.998 * all_masters - row_scale * raw).astype(jnp.bfloat16)
+    key_new = 0.998 * key_master.T - scales[0] * raw_here[:width]
+    value_new = 0.998 * value_master.T - scales[width] * raw_here[width:]
+    key_copy = 0.998 * all_masters[:width] - scales[0] * raw[:width]
+    value_copy = 0.998 * all_masters[width:] - scales[width] * raw[width:]
     return (
-        new_here[:width].T,
-        new_here[width:].T,
-        copies[:width].T,
-        copies[width:].T,
+        key_new.T,
+        value_new.T,
+        key_copy.astype(jnp.bfloat16).T,
+        value_copy.astype(jnp.bfloat16).T,
         first_new[:, :width],
         second_new[:, :width],
         first_new[:, width:],

time: 146 us -> 146 us (level)
  blocking collectives: 68.9 us -> 43 us
  starting transfers between devices: 26.5 us -> 45.7 us
  matrix products: 2.57 us -> 4.72 us
  Pallas kernels: 0 us -> 2.14 us
  waiting for transfers between devices: 34.6 us -> 36.4 us
    all_to_all x2 -> x1, blocking collectives: 36.6 us -> 10.6 us  [swap(): return lax.all_to_all(pieces, axes, 0, 0, tiled=True)]
    all_to_all x4 -> x5, starting transfers between devices: 26.5 us -> 43.2 us  [swap(): return lax.all_to_all(pieces, axes, 0, 0, tiled=True)]
    transpose x0 -> x2, other arithmetic: none -> 4.14 us  [the longest x1 2.17 us: local(): value_copy.astype(jnp.bfloat16)]
    another operation x4 -> x1, other arithmetic: 2.91 us -> 0.04 us  [local(): jnp.stack([normed[:, c * half:(c + 1) * half] for c in range(cores)])]
    ppermute x0 -> x1, starting transfers between devices: none -> 2.55 us  [local(): came = lax.ppermute(sent, 'tp_1', [(0, 1), (1, 0)])]
    pallas_call x0 -> x1, Pallas kernels: none -> 2.14 us  [squares_of(): pl.pallas_call(squares_kernel, out_shape=jax.ShapeDtypeStruct((peers, 1,...]
    broadcast_in_dim x3 -> x1, local copies, waits for them, and re-layouts: 2.37 us -> 0.67 us  [to_all(): return swap(jnp.broadcast_to(shard[None], (size, *shard.shape)), axes)]
    transpose x2 -> x0, local copies, waits for them, and re-layouts: 1.47 us -> none  [the longest x1 0.83 us: local(): copies[width:]]
  transfers between devices with their start and end apart: 4 -> 6, of which waited for: 3 -> 5; matrix products, arithmetic and copies ran while one was open for 2% -> 5% of each run, Pallas kernels for 0% -> 0%
where the time goes in v3:
time: 146 us; the launch traced here: 145 us
  starting transfers between devices  45.7 us (31%)
  blocking collectives  43 us (29%)
  waiting for transfers between devices  36.4 us (25%)
  local copies, waits for them, and re-layouts  6.81 us (5%)
  other arithmetic  5.06 us (3%)
  matrix products  4.72 us (3%)
  Pallas kernels  2.14 us (1%)
    all_to_all x5, starting transfers between devices, swap(): return lax.all_to_all(pieces, axes, 0, 0, tiled=True)  43.2 us
    all_to_all x5, waiting for transfers between devices, swap(): return lax.all_to_all(pieces, axes, 0, 0, tiled=True)  35 us
    all_gather x1, blocking collectives, local(): link = lax.all_gather(link, 'tp_0', axis=0, tiled=True)  32.3 us
    all_to_all x1, blocking collectives, swap(): return lax.all_to_all(pieces, axes, 0, 0, tiled=True)  10.6 us
  transfers between devices with their start and end apart: 6, of which 5 were waited for; matrix products, arithmetic and copies ran while one was open for 5% of the time, Pallas kernels for 0%

profile of v3, /device:TPU:1, one launch (start us, length us, event | category | flops | bytes accessed | tf_op | source)
XLA Modules:
  0.0 144.8 jit_solution(13558804343714124789)
XLA Ops:
  0.6 0.0 copy-start
  0.6 1.1 slice_bitcast_fusion.1
  1.8 0.0 copy-start.14
  1.8 0.0 copy-start.4
  1.9 0.0 copy-start.5
  1.9 10.6 %all_to_all.30 = bf16[2,64,1536]{2,1,0:T(8,128)(2,1)S(1)} all-to-all(bf16[2,64,1536]{2,1,0:T(8,128)(2,1)S(1)} %pad_maximum_fusion.1), channel_id=1, replica_groups=mesh['fs_0'=4,'fs_1'=4,'tp_0'=16,'tp_1'=2] {'tp_1'}, dimensions={0} | all-to-all | bytes 786432 | tf_op jit(solution)/shard_map/all_to_all | solution.py:18
  12.5 0.9 copy.31
  13.4 9.7 %all-to-all-start.1 = ((bf16[16,96,128]{2,1,0:T(8,128)(2,1)}), bf16[16,96,128]{2,1,0:T(8,128)(2,1)S(1)}, u32[]{:S(2)}, u32[]{:S(2)}) async-start(bf16[16,96,128]{2,1,0:T(8,128)(2,1)} %bitcast.6), calls=%async_computation.1 | async-start | bytes 786432 | tf_op jit(solution)/shard_map/all_to_all | solution.py:18
  23.2 0.0 copy-done.14
  23.2 0.1 select_reduce_fusion
  23.3 0.0 copy-done.4
  23.3 0.0 copy-done.5
  23.3 0.0 copy-start.8
  23.3 0.2 subtract_convert_fusion
  23.5 0.0 copy-done.3
  23.5 0.5 copy-done.6
  24.0 0.0 copy-done.8
  24.1 0.0 copy-done
  24.1 1.2 fusion.30.gram
  25.3 1.1 broadcast_in_dim.4
  26.4 2.5 %collective-permute-start = (bf16[128,1536]{1,0:T(8,128)(2,1)S(1)}, bf16[128,1536]{1,0:T(8,128)(2,1)S(1)}, u32[]{:S(2)}, u32[]{:S(2)}) collective-permute-start(bf16[128,1536]{1,0:T(8,128)(2,1)S(1)} %fusion.9), channel_id=1, source_target_pairs={{0,1},{1,0},{2,3},{3,2},{4,5},{5,4},{6,7},{7,6},{8,9},{9,8},{10,11... | collective-permute-start | bytes 1179656 | tf_op jit(solution)/shard_map/ppermute | solution.py:105
  28.9 1.3 collective-permute-done
  30.2 0.2 broadcast_select_fusion.1
  30.4 0.1 pad_maximum_fusion
  30.5 10.2 %all-to-all-done.1 = bf16[16,96,128]{2,1,0:T(8,128)(2,1)S(1)} async-done(((bf16[16,96,128]{2,1,0:T(8,128)(2,1)}), bf16[16,96,128]{2,1,0:T(8,128)(2,1)S(1)}, u32[]{:S(2)}, u32[]{:S(2)}) %all-to-all-start.1) | async-done | bytes 393248 | tf_op jit(solution)/shard_map/all_to_all | solution.py:18
  40.6 0.3 fusion.10
  40.9 6.8 %all-to-all-start.2 = ((f32[16,128,128]{2,1,0:T(8,128)}), f32[16,128,128]{2,1,0:T(8,128)S(1)}, u32[]{:S(2)}, u32[]{:S(2)}) async-start(f32[16,128,128]{2,1,0:T(8,128)} %broadcast_in_dim.4), calls=%async_computation.2 | async-start | bytes 2097152 | tf_op jit(solution)/shard_map/all_to_all | solution.py:18
  47.7 32.3 %all_gather.3 = f16[1536,256]{1,0:T(8,128)(2,1)S(1)} all-gather(f16[96,256]{1,0:T(8,128)(2,1)S(1)} %multiply_convert_fusion), channel_id=1, replica_groups=mesh['fs_0'=4,'fs_1'=4,'tp_0'=16,'tp_1'=2] {'tp_0'}, dimensions={0}, use_global_device_ids=true | all-gather | bytes 835584 | tf_op jit(solution)/shard_map/all_gather | solution.py:117
  80.1 0.4 fusion.3
  80.5 0.4 convolution_add_fusion.2
  80.9 0.1 reshape.107
  81.0 0.7 copy.33
  81.8 0.0 all-to-all-done.2
  81.8 16.7 %all-to-all-start.3 = ((f32[32,16,128]{2,1,0:T(8,128)}), f32[32,16,128]{2,1,0:T(8,128)S(1)}, u32[]{:S(2)}, u32[]{:S(2)}) async-start(f32[32,16,128]{2,1,0:T(8,128)} %bitcast.9), calls=%async_computation.3 | async-start | bytes 524288 | tf_op jit(solution)/shard_map/all_to_all | solution.py:18
  98.5 0.0 copy-start.10
  98.5 0.0 copy-start.11
  98.5 0.0 copy-start.12
  98.6 0.0 copy-start.13
  98.6 0.1 fusion.6
  98.7 8.7 %all-to-all-done.3 = f32[32,16,128]{2,1,0:T(8,128)S(1)} async-done(((f32[32,16,128]{2,1,0:T(8,128)}), f32[32,16,128]{2,1,0:T(8,128)S(1)}, u32[]{:S(2)}, u32[]{:S(2)}) %all-to-all-start.3) | async-done | bytes 262176 | tf_op jit(solution)/shard_map/all_to_all | solution.py:18
  107.4 0.0 copy-done.10
  107.4 0.0 copy-done.11
  107.5 0.0 copy-done.12
  107.5 0.0 copy-done.13
  107.5 0.1 add_divide_fusion
  107.6 0.7 broadcast_in_dim.5
  108.2 3.5 %all-to-all-start.4 = ((f32[16,16,128]{2,1,0:T(8,128)}), f32[16,16,128]{2,1,0:T(8,128)S(1)}, u32[]{:S(2)}, u32[]{:S(2)}) async-start(f32[16,16,128]{2,1,0:T(8,128)} %broadcast_in_dim.5), calls=%async_computation.4 | async-start | bytes 262144 | tf_op jit(solution)/shard_map/all_to_all | solution.py:18
  111.8 0.7 fusion.27
  112.4 6.4 %all-to-all-done.4 = f32[16,16,128]{2,1,0:T(8,128)S(1)} async-done(((f32[16,16,128]{2,1,0:T(8,128)}), f32[16,16,128]{2,1,0:T(8,128)S(1)}, u32[]{:S(2)}, u32[]{:S(2)}) %all-to-all-start.4) | async-done | bytes 131104 | tf_op jit(solution)/shard_map/all_to_all | solution.py:18
  118.9 0.5 fusion.18
  119.3 0.2 copy-done.1
  119.5 2.1 %squares.1 = f32[32,1,128]{2,1,0:T(1,128)} custom-call(f32[256,128]{1,0:T(8,128)} %bitcast.61, f32[256,256]{1,0:T(8,128)} %fusion.30.gram), custom_call_target="tpu_custom_call" | custom-call | tf_op jit(solution)/shard_map/squares/pallas_call | solution.py:48
  121.7 6.4 %all-to-all-start.5 = ((f32[32,1,128]{2,1,0:T(1,128)}), f32[32,1,128]{2,1,0:T(1,128)S(1)}, u32[]{:S(2)}, u32[]{:S(2)}) async-start(f32[32,1,128]{2,1,0:T(1,128)} %squares.1), calls=%async_computation.5 | async-start | bytes 32768 | tf_op jit(solution)/shard_map/all_to_all | solution.py:18
  128.1 0.0 copy-start.2
  128.1 1.5 %convolution_add_fusion.1 = f32[128,2048]{1,0:T(8,128)S(1)} fusion(f32[128,2048]{1,0:T(8,128)S(1)} %fusion.18, bf16[2048,256]{1,0:T(8,128)(2,1)S(1)} %copy-done, f32[256,128]{1,0:T(8,128)} %bitcast.62), kind=kOutput, calls=%fused_computation.1 | convolution fusion | flops 134610944 | bytes 3276800 | tf_op jit(solution)/shard_map/dot_general | solution.py:142
  129.6 0.0 copy-done.2
  129.6 0.5 convolution_add_fusion
  130.1 9.8 %all-to-all-done.5 = f32[32,1,128]{2,1,0:T(1,128)S(1)} async-done(((f32[32,1,128]{2,1,0:T(1,128)}), f32[32,1,128]{2,1,0:T(1,128)S(1)}, u32[]{:S(2)}, u32[]{:S(2)}) %all-to-all-start.5) | async-done | bytes 16416 | tf_op jit(solution)/shard_map/all_to_all | solution.py:18
  139.9 0.1 reduce_sum.29
  139.9 0.7 fusion.29
  140.6 2.2 %fusion.14 = (bf16[2048,64]{0,1:T(8,128)(2,1)}, bf16[2048,64]{0,1:T(8,128)(2,1)}) fusion(f32[128,2048]{1,0:T(8,128)S(1)} %convolution_add_fusion, f32[16,8,8,128]{3,2,1,0:T(8,128)S(1)} %get-tuple-element.41, f32[]{:T(128)} %bitcast.13, f32[]{:T(128)} %bitcast.11, f32[16,8,8,128]{3,2,1,0:T(8,128)S(1)} %get-tuple-element.42), kind=kLoop, calls=%fused_computation.33 | loop fusion | flops 786432 | bytes 2621448 | tf_op jit(solution)/shard_map/transpose | solution.py:155
  142.8 0.0 copy-done.7
  142.8 0.0 copy-done.9
  142.8 2.0 %fusion.20 = (f32[128,64]{0,1:T(8,128)}, f32[128,64]{0,1:T(8,128)}) fusion(f32[128,2048]{1,0:T(8,128)S(1)} %convolution_add_fusion, s32[]{:T(128)S(6)} %add.85, s32[]{:T(128)S(6)} %select_n.36, f32[]{:T(128)} %bitcast.13, f32[128,64]{0,1:T(8,128)S(1)} %copy-done.7, f32[]{:T(128)} %bitcast.11, f32[128,64]{0,1:T(8,128)S(1)} %copy-done.9), kind=kLoop, calls=%fused_computation.47 | loop fusion | flops 49152 | bytes 196624 | tf_op jit(solution)/shard_map/transpose | solution.py:153
  (12 shorter events, 0.2 us)
Async XLA Ops:
  0.6 23.4 %copy-start = (bf16[2048,256]{1,0:T(8,128)(2,1)S(1)}, bf16[2048,256]{1,0:T(8,128)(2,1)}, u32[]{:S(2)}) copy-start(bf16[2048,256]{1,0:T(8,128)(2,1)} %param.17) | copy-start | bytes 3145732
  1.8 21.4 %copy-start.14 = (f32[8]{0:T(128)S(1)}, f32[8]{0:T(128)}, u32[]{:S(2)}) copy-start(f32[8]{0:T(128)} %param.16) | copy-start | bytes 100
  1.8 21.4 %copy-start.4 = (bf16[64,3072]{1,0:T(8,128)(2,1)S(1)}, bf16[64,3072]{1,0:T(8,128)(2,1)}, u32[]{:S(2)}) copy-start(bf16[64,3072]{1,0:T(8,128)(2,1)} %param.15) | copy-start | bytes 1179652
  1.9 21.4 %copy-start.5 = (bf16[64,3072]{1,0:T(8,128)(2,1)S(1)}, bf16[64,3072]{1,0:T(8,128)(2,1)}, u32[]{:S(2)}) copy-start(bf16[64,3072]{1,0:T(8,128)(2,1)} %param.14) | copy-start | bytes 1179652
  13.4 10.1 %copy-start.3 = (bf16[64,3072]{1,0:T(8,128)(2,1)S(1)}, bf16[64,3072]{1,0:T(8,128)(2,1)}, u32[]{:S(2)}) copy-start(bf16[64,3072]{1,0:T(8,128)(2,1)} %param.13) | copy-start | bytes 1179652
  13.4 27.2 %all-to-all-start.1 = ((bf16[16,96,128]{2,1,0:T(8,128)(2,1)}), bf16[16,96,128]{2,1,0:T(8,128)(2,1)S(1)}, u32[]{:S(2)}, u32[]{:S(2)}) async-start(bf16[16,96,128]{2,1,0:T(8,128)(2,1)} %bitcast.6), calls=%async_computation.1 | async-start | bytes 786432 | tf_op jit(solution)/shard_map/all_to_all | solution.py:18
  23.3 0.8 copy-start.6
  23.3 0.8 copy-start.8
  26.4 3.9 %collective-permute-start = (bf16[128,1536]{1,0:T(8,128)(2,1)S(1)}, bf16[128,1536]{1,0:T(8,128)(2,1)S(1)}, u32[]{:S(2)}, u32[]{:S(2)}) collective-permute-start(bf16[128,1536]{1,0:T(8,128)(2,1)S(1)} %fusion.9), channel_id=1, source_target_pairs={{0,1},{1,0},{2,3},{3,2},{4,5},{5,4},{6,7},{7,6},{8,9},{9,8},{10,11... | collective-permute-start | bytes 1179656 | tf_op jit(solution)/shard_map/ppermute | solution.py:105
  40.9 40.8 %all-to-all-start.2 = ((f32[16,128,128]{2,1,0:T(8,128)}), f32[16,128,128]{2,1,0:T(8,128)S(1)}, u32[]{:S(2)}, u32[]{:S(2)}) async-start(f32[16,128,128]{2,1,0:T(8,128)} %broadcast_in_dim.4), calls=%async_computation.2 | async-start | bytes 2097152 | tf_op jit(solution)/shard_map/all_to_all | solution.py:18
  81.8 25.6 %all-to-all-start.3 = ((f32[32,16,128]{2,1,0:T(8,128)}), f32[32,16,128]{2,1,0:T(8,128)S(1)}, u32[]{:S(2)}, u32[]{:S(2)}) async-start(f32[32,16,128]{2,1,0:T(8,128)} %bitcast.9), calls=%async_computation.3 | async-start | bytes 524288 | tf_op jit(solution)/shard_map/all_to_all | solution.py:18
  98.5 8.9 %copy-start.10 = (f32[16,64]{1,0:T(8,128)S(1)}, f32[16,64]{1,0:T(8,128)}, u32[]{:S(2)}) copy-start(f32[16,64]{1,0:T(8,128)} %param.23) | copy-start | bytes 12292
  98.5 8.9 %copy-start.11 = (f32[16,64]{1,0:T(8,128)S(1)}, f32[16,64]{1,0:T(8,128)}, u32[]{:S(2)}) copy-start(f32[16,64]{1,0:T(8,128)} %param.21) | copy-start | bytes 12292
  98.5 8.9 %copy-start.12 = (f32[16,64]{1,0:T(8,128)S(1)}, f32[16,64]{1,0:T(8,128)}, u32[]{:S(2)}) copy-start(f32[16,64]{1,0:T(8,128)} %param.22) | copy-start | bytes 12292
  98.6 8.9 %copy-start.13 = (f32[16,64]{1,0:T(8,128)S(1)}, f32[16,64]{1,0:T(8,128)}, u32[]{:S(2)}) copy-start(f32[16,64]{1,0:T(8,128)} %param.20) | copy-start | bytes 12292
  108.2 10.6 %all-to-all-start.4 = ((f32[16,16,128]{2,1,0:T(8,128)}), f32[16,16,128]{2,1,0:T(8,128)S(1)}, u32[]{:S(2)}, u32[]{:S(2)}) async-start(f32[16,16,128]{2,1,0:T(8,128)} %broadcast_in_dim.5), calls=%async_computation.4 | async-start | bytes 262144 | tf_op jit(solution)/shard_map/all_to_all | solution.py:18
  118.9 0.7 copy-start.1
  121.7 18.2 %all-to-all-start.5 = ((f32[32,1,128]{2,1,0:T(1,128)}), f32[32,1,128]{2,1,0:T(1,128)S(1)}, u32[]{:S(2)}, u32[]{:S(2)}) async-start(f32[32,1,128]{2,1,0:T(1,128)} %squares.1), calls=%async_computation.5 | async-start | bytes 32768 | tf_op jit(solution)/shard_map/all_to_all | solution.py:18
  128.1 1.5 %copy-start.2 = (f32[16,16,128]{2,1,0:T(8,128)S(1)}, f32[16,16,128]{2,1,0:T(8,128)}, u32[]{:S(2)}) copy-start(f32[16,16,128]{2,1,0:T(8,128)} %copy-done.1) | copy-start | bytes 393220
  140.6 2.2 %copy-start.7 = (f32[128,64]{0,1:T(8,128)S(1)}, f32[128,64]{0,1:T(8,128)}, u32[]{:S(2)}) copy-start(f32[128,64]{0,1:T(8,128)} %param.19) | copy-start | bytes 98308
  140.6 2.2 %copy-start.9 = (f32[128,64]{0,1:T(8,128)S(1)}, f32[128,64]{0,1:T(8,128)}, u32[]{:S(2)}) copy-start(f32[128,64]{0,1:T(8,128)} %param.18) | copy-start | bytes 98308

commit v4 on v1

--- a/solution.py
+++ b/solution.py
@@ -3,6 +3,7 @@
 import jax
 import jax.numpy as jnp
 from jax import lax
+from jax.experimental.layout import Layout, with_layout_constraint
 from jax.sharding import Mesh
 from jax.sharding import PartitionSpec as P
 
@@ -53,7 +54,6 @@
     rows = factor.shape[0]
     heads = lambdas.shape[0]
     fs_rows = key_master.shape[0]
-    fs_at = lax.axis_index(FS)
     half = tokens // cores
     share = half // chips
 
@@ -61,28 +61,56 @@
     owners = rows_here // VALUE_DIM
     picked = (owners[:, None] == lax.iota(jnp.int32, heads)[None, :]).astype(jnp.float32)
     row_lambda = jnp.sum(picked * lambdas[None, :], axis=1)
+    core = lax.axis_index("tp_1")
+    kept = lax.dynamic_slice_in_dim(normed, core * half, half, 1)
+    sent = lax.dynamic_slice_in_dim(normed, (1 - core) * half, half, 1)
+    sent = with_layout_constraint(sent, Layout(major_to_minor=(0, 1)))
+    came = lax.ppermute(sent, "tp_1", [(0, 1), (1, 0)])
+    came = with_layout_constraint(came, Layout(major_to_minor=(0, 1)))
+    features = jnp.concatenate([kept, came], axis=0)
+
+    by_token = features.T.reshape(chips, share, cores * width)
+    by_token, first_map, second_map, blocks, key_master, value_master = lax.optimization_barrier(
+        (
+            by_token,
+            first_map,
+            second_map,
+            factor.reshape(chips, cores, width, rank),
+            key_master,
+            value_master,
+        )
+    )
+    by_token = swap(by_token, "tp_0")
+
     value_cot = (
         first_map.astype(jnp.float32) - row_lambda[:, None] * second_map.astype(jnp.float32)
     ).astype(jnp.bfloat16)
-
-    stacked = jnp.stack([normed, key_cot, value_cot])
-    halves = jnp.stack([stacked[:, :, c * half : (c + 1) * half] for c in range(cores)])
-    halves = swap(halves, "tp_1")
-    features = halves[:, 0].reshape(cores * width, half)
-    cots = halves[:, 1:].reshape(cores * 2 * width, half)
-
-    by_token = features.T.reshape(chips, share, cores * width)
-    by_token = swap(by_token, "tp_0")
+    stacked = jnp.concatenate([key_cot, value_cot], axis=0)
+    kept = lax.dynamic_slice_in_dim(stacked, core * half, half, 1)
+    sent = lax.dynamic_slice_in_dim(stacked, (1 - core) * half, half, 1)
+    masters_here = jnp.concatenate([key_master.T, value_master.T], axis=0)
+    masters = jnp.broadcast_to(masters_here[None], (fs_size, *masters_here.shape))
+    late_factor = blocks.reshape(rows, rank)
+    gram = lax.dot_general(
+        late_factor, late_factor, (((0,), (0,)), ((), ())), preferred_element_type=jnp.float32
+    )
+    own_first = jnp.where(core == 0, blocks, blocks[:, ::-1]).reshape(rows, rank)
+    fs_at = lax.axis_index(FS) * fs_rows
+    masters, gram, own_first, fs_at, sent = lax.optimization_barrier(
+        (masters, gram, own_first, fs_at, sent)
+    )
+    came = lax.ppermute(sent, "tp_1", [(0, 1), (1, 0)])
+    cots = jnp.concatenate([jnp.where(core == 0, kept, came), jnp.where(core == 0, came, kept)])
+    cots, by_token = lax.optimization_barrier((cots, by_token))
     product = lax.dot_general(
         by_token.transpose(1, 0, 2).reshape(share, rows),
-        factor,
+        own_first,
         (((1,), (0,)), ((), ())),
         preferred_element_type=jnp.float32,
     )
-    masters_here = jnp.concatenate([key_master.T, value_master.T], axis=0)
-    masters, product = lax.optimization_barrier((masters_here, product))
-    masters = to_all(masters, FS)
     link = (product * LINK_SCALE).astype(jnp.float16)
+    masters, link = lax.optimization_barrier((masters, link))
+    masters = swap(masters, FS)
     link = lax.all_gather(link, "tp_0", axis=0, tiled=True)
 
     high, low = in_bf16_parts(link.astype(jnp.float32), 2)
@@ -102,18 +130,24 @@
     direction = first_new / (jnp.sqrt(second_new) + 1e-06)
     directions = to_all(direction, FS).reshape(rank, 2 * width)
 
+    seen = jnp.dot(gram, directions, precision=lax.Precision.HIGHEST)
+    squares = jnp.sum(directions * seen, axis=0, keepdims=True)
+    squares = jnp.broadcast_to(squares[None], (cores * chips, 1, 2 * width))
+    directions, squares, masters, first_new, second_new = lax.optimization_barrier(
+        (directions, squares, masters, first_new, second_new)
+    )
+    squares = jnp.sum(swap(squares, TP).reshape(cores * chips, 2, width), axis=(0, 2))
+    cells = rows * width * cores * chips
+    scales = 0.02 / jnp.sqrt(squares / cells + 0.01)
+    row_scale = jnp.repeat(scales, width)[:, None]
+
     raw = sum(
         lax.dot_general(part, factor, (((0,), (1,)), ((), ())), preferred_element_type=jnp.float32)
         for part in in_bf16_parts(directions, 3)
     )
-    squares = jnp.stack([jnp.sum(raw[:width] * raw[:width]), jnp.sum(raw[width:] * raw[width:])])
-    squares = jnp.sum(to_all(squares.reshape(1, 2), TP), axis=(0, 1))
-    cells = rows * width * cores * chips
-    scales = 0.02 / jnp.sqrt(squares / cells + 0.01)
-    row_scale = jnp.repeat(scales, width)[:, None]
-    raw_here = lax.dynamic_slice_in_dim(raw, fs_at * fs_rows, fs_rows, 1)
+    raw_here = lax.dynamic_slice_in_dim(raw, fs_at, fs_rows, 1, allow_negative_indices=False)
+    all_masters = masters.transpose(1, 0, 2).reshape(2 * width, rows)
     new_here = 0.998 * masters_here - row_scale * raw_here
-    all_masters = masters.transpose(1, 0, 2).reshape(2 * width, rows)
     copies = (0.998 * all_masters - row_scale * raw).astype(jnp.bfloat16)
     return (
         new_here[:width].T,

time: 146 us -> 139 us (0.952)
  waiting for transfers between devices: 34.6 us -> 21.5 us
  starting transfers between devices: 26.5 us -> 34.8 us
  other arithmetic: 5.04 us -> 1.87 us
  matrix products: 2.57 us -> 4.08 us
    all_to_all x4 -> x3, waiting for transfers between devices: 34.6 us -> 19.9 us  [swap(): return lax.all_to_all(pieces, axes, 0, 0, tiled=True)]
    ppermute x0 -> x2, starting transfers between devices: none -> 11.3 us  [local(): came = lax.ppermute(sent, 'tp_1', [(0, 1), (1, 0)])]
    all_to_all x4 -> x3, starting transfers between devices: 26.5 us -> 23.5 us  [swap(): return lax.all_to_all(pieces, axes, 0, 0, tiled=True)]
    another operation x4 -> x0, other arithmetic: 2.91 us -> none  [the longest x2 1.43 us: local(): stacked = jnp.stack([normed, key_cot, value_cot])]
    broadcast_in_dim x3 -> x1, local copies, waits for them, and re-layouts: 2.37 us -> 0.01 us  [to_all(): return swap(jnp.broadcast_to(shard[None], (size, *shard.shape)), axes)]
    broadcast_in_dim x0 -> x2, local copies, waits for them, and re-layouts: none -> 1.7 us  [the longest x1 1.08 us: local(): jnp.broadcast_to(masters_here[None], (fs_size, *masters_here.shape))]
    ppermute x0 -> x2, waiting for transfers between devices: none -> 1.6 us  [local(): came = lax.ppermute(sent, 'tp_1', [(0, 1), (1, 0)])]
    dot_general x1 -> x3, matrix products: 0.3 us -> 1.79 us  [the longest x1 0.93 us: local(): lax.dot_general(by_token.transpose(1, 0, 2).reshape(share, rows), own_fir...]
  transfers between devices with their start and end apart: 4 -> 5, of which waited for: 3 -> 4; matrix products, arithmetic and copies ran while one was open for 2% -> 4% of each run, Pallas kernels for 0% -> 0%
where the time goes in v4:
time: 139 us
  blocking collectives  67.5 us (49%)
  starting transfers between devices  34.8 us (25%)
  waiting for transfers between devices  21.5 us (15%)
  local copies, waits for them, and re-layouts  7.72 us (6%)
  matrix products  4.08 us (3%)
  other arithmetic  1.87 us (1%)
    all_to_all x2, blocking collectives, swap(): return lax.all_to_all(pieces, axes, 0, 0, tiled=True)  35.2 us
    all_gather x1, blocking collectives, local(): link = lax.all_gather(link, 'tp_0', axis=0, tiled=True)  32.3 us
    all_to_all x3, starting transfers between devices, swap(): return lax.all_to_all(pieces, axes, 0, 0, tiled=True)  23.5 us
    all_to_all x3, waiting for transfers between devices, swap(): return lax.all_to_all(pieces, axes, 0, 0, tiled=True)  19.9 us
    ppermute x2, starting transfers between devices, local(): came = lax.ppermute(sent, 'tp_1', [(0, 1), (1, 0)])  11.3 us
  transfers between devices with their start and end apart: 5, of which 4 were waited for; matrix products, arithmetic and copies ran while one was open for 4% of the time, Pallas kernels for 0%

profile of v4, /device:TPU:1, one launch (start us, length us, event | category | flops | bytes accessed | tf_op | source)
XLA Modules:
  0.0 138.5 jit_solution(3345263262611823748)
XLA Ops:
  0.6 1.1 constant_dynamic-slice_fusion.1
  1.7 8.7 %collective-permute-start = (bf16[64,1536]{1,0:T(8,128)(2,1)S(1)}, bf16[64,1536]{1,0:T(8,128)(2,1)S(1)}, u32[]{:S(2)}, u32[]{:S(2)}) collective-permute-start(bf16[64,1536]{1,0:T(8,128)(2,1)S(1)} %get-tuple-element.60), channel_id=1, source_target_pairs={{0,1},{1,0},{2,3},{3,2},{4,5},{5,4},{6,7},{7,6},{8,9},{9,8},{10,11... | collective-permute-start | bytes 589832 | tf_op jit(solution)/shard_map/ppermute | solution.py:68
  10.5 0.7 select_reduce_fusion
  11.2 0.3 collective-permute-done
  11.5 0.0 copy-start
  11.5 0.9 copy.31
  12.5 9.6 %all-to-all-start = ((bf16[16,96,128]{2,1,0:T(8,128)(2,1)}), bf16[16,96,128]{2,1,0:T(8,128)(2,1)S(1)}, u32[]{:S(2)}, u32[]{:S(2)}) async-start(bf16[16,96,128]{2,1,0:T(8,128)(2,1)} %bitcast.1), calls=%async_computation | async-start | bytes 786432 | tf_op jit(solution)/shard_map/all_to_all | solution.py:18
  22.0 0.0 copy-done
  22.1 0.0 copy-start.2
  22.1 0.0 copy-start.3
  22.1 0.5 convolution_bitcast_fusion
  22.6 0.5 copy-done.2
  23.1 0.1 copy-done.3
  23.2 0.0 copy-start.1
  23.2 0.0 copy-start.5
  23.2 0.2 subtract_convert_fusion
  23.4 0.8 copy-done.1
  24.2 0.0 copy-done.5
  24.2 0.0 copy-done.7
  24.2 0.3 reverse_select_fusion
  24.5 1.1 broadcast_in_dim.8
  25.6 2.5 %collective-permute-start.1 = (bf16[128,1536]{1,0:T(8,128)(2,1)S(1)}, bf16[128,1536]{1,0:T(8,128)(2,1)S(1)}, u32[]{:S(2)}, u32[]{:S(2)}) collective-permute-start(bf16[128,1536]{1,0:T(8,128)(2,1)S(1)} %fusion.8), channel_id=1, source_target_pairs={{0,1},{1,0},{2,3},{3,2},{4,5},{5,4},{6,7},{7,6},{8,9},{9,8},{10,11... | collective-permute-start | bytes 1179656 | tf_op jit(solution)/shard_map/ppermute | solution.py:102
  28.2 1.3 collective-permute-done.1
  29.5 0.2 broadcast_select_fusion.1
  29.6 0.1 pad_maximum_fusion
  29.7 9.8 %all-to-all-done = bf16[16,96,128]{2,1,0:T(8,128)(2,1)S(1)} async-done(((bf16[16,96,128]{2,1,0:T(8,128)(2,1)}), bf16[16,96,128]{2,1,0:T(8,128)(2,1)S(1)}, u32[]{:S(2)}, u32[]{:S(2)}) %all-to-all-start) | async-done | bytes 393248 | tf_op jit(solution)/shard_map/all_to_all | solution.py:18
  39.5 0.9 fusion.2
  40.5 6.9 %all-to-all-start.1 = ((f32[16,128,128]{2,1,0:T(8,128)}), f32[16,128,128]{2,1,0:T(8,128)S(1)}, u32[]{:S(2)}, u32[]{:S(2)}) async-start(f32[16,128,128]{2,1,0:T(8,128)} %broadcast_in_dim.8), calls=%async_computation.1 | async-start | bytes 2097152 | tf_op jit(solution)/shard_map/all_to_all | solution.py:18
  47.4 0.0 copy-done.4
  47.4 32.3 %all_gather.3 = f16[1536,256]{1,0:T(8,128)(2,1)S(1)} all-gather(f16[96,256]{1,0:T(8,128)(2,1)S(1)} %copy-done.4), channel_id=1, replica_groups=mesh['fs_0'=4,'fs_1'=4,'tp_0'=16,'tp_1'=2] {'tp_0'}, dimensions={0}, use_global_device_ids=true | all-gather | bytes 835584 | tf_op jit(solution)/shard_map/all_gather | solution.py:114
  79.7 0.4 fusion.6
  80.1 0.4 convolution_add_fusion.2
  80.5 0.0 copy-start.9
  80.5 0.0 copy-start.10
  80.5 0.0 copy-start.11
  80.5 0.0 copy-start.12
  80.6 0.1 reshape.114
  80.7 0.0 all-to-all-done.1
  80.7 25.5 %all_to_all.25 = f32[32,16,128]{2,1,0:T(8,128)S(1)} all-to-all(f32[32,16,128]{2,1,0:T(8,128)S(1)} %bitcast.57), channel_id=1, replica_groups=mesh['fs_0'=4,'fs_1'=4,'tp_0'=16,'tp_1'=2] {'fs_0','fs_1','tp_1'}, dimensions={0} | all-to-all | bytes 524288 | tf_op jit(solution)/shard_map/all_to_all | solution.py:18
  106.2 0.0 copy-done.9
  106.2 0.0 copy-done.10
  106.3 0.0 copy-done.11
  106.3 0.0 copy-done.12
  106.3 0.1 add_divide_fusion
  106.4 9.8 %all_to_all.26 = f32[16,16,128]{2,1,0:T(8,128)S(1)} all-to-all(f32[16,16,128]{2,1,0:T(8,128)S(1)} %broadcast_in_dim.9), channel_id=1, replica_groups=mesh['fs_0'=4,'fs_1'=4,'tp_0'=16,'tp_1'=2] {'fs_0','fs_1'}, dimensions={0} | all-to-all | bytes 262144 | tf_op jit(solution)/shard_map/all_to_all | solution.py:18
  116.1 0.4 fusion.3
  116.5 0.6 broadcast_in_dim.10
  117.2 7.1 %all-to-all-start.4 = ((f32[32,1,128]{2,1,0:T(1,128)}), f32[32,1,128]{2,1,0:T(1,128)S(1)}, u32[]{:S(2)}, u32[]{:S(2)}) async-start(f32[32,1,128]{2,1,0:T(1,128)} %broadcast_in_dim.10), calls=%async_computation.4 | async-start | bytes 32768 | tf_op jit(solution)/shard_map/all_to_all | solution.py:18
  124.2 0.5 fusion.14
  124.7 0.5 convolution_add_fusion.1
  125.2 0.7 fusion.19
  125.9 10.1 %all-to-all-done.4 = f32[32,1,128]{2,1,0:T(1,128)S(1)} async-done(((f32[32,1,128]{2,1,0:T(1,128)}), f32[32,1,128]{2,1,0:T(1,128)S(1)}, u32[]{:S(2)}, u32[]{:S(2)}) %all-to-all-start.4) | async-done | bytes 16416 | tf_op jit(solution)/shard_map/all_to_all | solution.py:18
  136.0 0.1 reduce_sum.47
  136.1 0.1 reduce_sum.48
  136.2 0.1 broadcast_in_dim.11
  136.3 0.1 mul.164
  136.4 0.5 fusion.4
  136.9 0.0 copy-start.6
  136.9 0.0 copy-start.8
  136.9 0.8 slice_bitcast_fusion
  137.8 0.0 copy-done.6
  137.8 0.0 copy-done.8
  137.8 0.1 multiply_subtract_fusion
  137.9 0.6 slice_bitcast_fusion.2
  (11 shorter events, 0.2 us)
Async XLA Ops:
  1.7 9.8 %collective-permute-start = (bf16[64,1536]{1,0:T(8,128)(2,1)S(1)}, bf16[64,1536]{1,0:T(8,128)(2,1)S(1)}, u32[]{:S(2)}, u32[]{:S(2)}) collective-permute-start(bf16[64,1536]{1,0:T(8,128)(2,1)S(1)} %get-tuple-element.60), channel_id=1, source_target_pairs={{0,1},{1,0},{2,3},{3,2},{4,5},{5,4},{6,7},{7,6},{8,9},{9,8},{10,11... | collective-permute-start | bytes 589832 | tf_op jit(solution)/shard_map/ppermute | solution.py:68
  11.5 10.5 %copy-start = (bf16[2048,256]{1,0:T(8,128)(2,1)S(1)}, bf16[2048,256]{1,0:T(8,128)(2,1)}, u32[]{:S(2)}) copy-start(bf16[2048,256]{1,0:T(8,128)(2,1)} %param.17) | copy-start | bytes 3145732
  12.5 27.1 %all-to-all-start = ((bf16[16,96,128]{2,1,0:T(8,128)(2,1)}), bf16[16,96,128]{2,1,0:T(8,128)(2,1)S(1)}, u32[]{:S(2)}, u32[]{:S(2)}) async-start(bf16[16,96,128]{2,1,0:T(8,128)(2,1)} %bitcast.1), calls=%async_computation | async-start | bytes 786432 | tf_op jit(solution)/shard_map/all_to_all | solution.py:18
  22.1 1.0 copy-start.2
  22.1 1.1 copy-start.3
  23.2 1.0 copy-start.1
  23.2 1.0 copy-start.5
  23.2 1.0 copy-start.7
  25.6 3.9 %collective-permute-start.1 = (bf16[128,1536]{1,0:T(8,128)(2,1)S(1)}, bf16[128,1536]{1,0:T(8,128)(2,1)S(1)}, u32[]{:S(2)}, u32[]{:S(2)}) collective-permute-start(bf16[128,1536]{1,0:T(8,128)(2,1)S(1)} %fusion.8), channel_id=1, source_target_pairs={{0,1},{1,0},{2,3},{3,2},{4,5},{5,4},{6,7},{7,6},{8,9},{9,8},{10,11... | collective-permute-start | bytes 1179656 | tf_op jit(solution)/shard_map/ppermute | solution.py:102
  40.5 6.9 %copy-start.4 = (f16[96,256]{1,0:T(8,128)(2,1)S(1)}, f16[96,256]{1,0:T(8,128)(2,1)}, u32[]{:S(2)}) copy-start(f16[96,256]{1,0:T(8,128)(2,1)} %fusion.2) | copy-start | bytes 147460
  40.5 40.3 %all-to-all-start.1 = ((f32[16,128,128]{2,1,0:T(8,128)}), f32[16,128,128]{2,1,0:T(8,128)S(1)}, u32[]{:S(2)}, u32[]{:S(2)}) async-start(f32[16,128,128]{2,1,0:T(8,128)} %broadcast_in_dim.8), calls=%async_computation.1 | async-start | bytes 2097152 | tf_op jit(solution)/shard_map/all_to_all | solution.py:18
  80.5 25.7 %copy-start.9 = (f32[16,64]{1,0:T(8,128)S(1)}, f32[16,64]{1,0:T(8,128)}, u32[]{:S(2)}) copy-start(f32[16,64]{1,0:T(8,128)} %param.23) | copy-start | bytes 12292
  80.5 25.7 %copy-start.10 = (f32[16,64]{1,0:T(8,128)S(1)}, f32[16,64]{1,0:T(8,128)}, u32[]{:S(2)}) copy-start(f32[16,64]{1,0:T(8,128)} %param.21) | copy-start | bytes 12292
  80.5 25.7 %copy-start.11 = (f32[16,64]{1,0:T(8,128)S(1)}, f32[16,64]{1,0:T(8,128)}, u32[]{:S(2)}) copy-start(f32[16,64]{1,0:T(8,128)} %param.22) | copy-start | bytes 12292
  80.5 25.7 %copy-start.12 = (f32[16,64]{1,0:T(8,128)S(1)}, f32[16,64]{1,0:T(8,128)}, u32[]{:S(2)}) copy-start(f32[16,64]{1,0:T(8,128)} %param.20) | copy-start | bytes 12292
  117.2 18.8 %all-to-all-start.4 = ((f32[32,1,128]{2,1,0:T(1,128)}), f32[32,1,128]{2,1,0:T(1,128)S(1)}, u32[]{:S(2)}, u32[]{:S(2)}) async-start(f32[32,1,128]{2,1,0:T(1,128)} %broadcast_in_dim.10), calls=%async_computation.4 | async-start | bytes 32768 | tf_op jit(solution)/shard_map/all_to_all | solution.py:18
  136.9 0.9 copy-start.6
  136.9 0.9 copy-start.8

commit v5 on v4

--- a/solution.py
+++ b/solution.py
@@ -62,11 +62,12 @@
     picked = (owners[:, None] == lax.iota(jnp.int32, heads)[None, :]).astype(jnp.float32)
     row_lambda = jnp.sum(picked * lambdas[None, :], axis=1)
     core = lax.axis_index("tp_1")
-    kept = lax.dynamic_slice_in_dim(normed, core * half, half, 1)
-    sent = lax.dynamic_slice_in_dim(normed, (1 - core) * half, half, 1)
-    sent = with_layout_constraint(sent, Layout(major_to_minor=(0, 1)))
-    came = lax.ppermute(sent, "tp_1", [(0, 1), (1, 0)])
+    came = lax.ppermute(normed, "tp_1", [(0, 1), (1, 0)])
     came = with_layout_constraint(came, Layout(major_to_minor=(0, 1)))
+    kept, came = (
+        lax.dynamic_slice_in_dim(side, core * half, half, 1, allow_negative_indices=False)
+        for side in (normed, came)
+    )
     features = jnp.concatenate([kept, came], axis=0)
 
     by_token = features.T.reshape(chips, share, cores * width)
@@ -101,7 +102,7 @@
     )
     came = lax.ppermute(sent, "tp_1", [(0, 1), (1, 0)])
     cots = jnp.concatenate([jnp.where(core == 0, kept, came), jnp.where(core == 0, came, kept)])
-    cots, by_token = lax.optimization_barrier((cots, by_token))
+    cots, masters, by_token = lax.optimization_barrier((cots, masters, by_token))
     product = lax.dot_general(
         by_token.transpose(1, 0, 2).reshape(share, rows),
         own_first,
@@ -109,7 +110,6 @@
         preferred_element_type=jnp.float32,
     )
     link = (product * LINK_SCALE).astype(jnp.float16)
-    masters, link = lax.optimization_barrier((masters, link))
     masters = swap(masters, FS)
     link = lax.all_gather(link, "tp_0", axis=0, tiled=True)
 
@@ -139,7 +139,6 @@
     squares = jnp.sum(swap(squares, TP).reshape(cores * chips, 2, width), axis=(0, 2))
     cells = rows * width * cores * chips
     scales = 0.02 / jnp.sqrt(squares / cells + 0.01)
-    row_scale = jnp.repeat(scales, width)[:, None]
 
     raw = sum(
         lax.dot_general(part, factor, (((0,), (1,)), ((), ())), preferred_element_type=jnp.float32)
@@ -147,13 +146,17 @@
     )
     raw_here = lax.dynamic_slice_in_dim(raw, fs_at, fs_rows, 1, allow_negative_indices=False)
     all_masters = masters.transpose(1, 0, 2).reshape(2 * width, rows)
-    new_here = 0.998 * masters_here - row_scale * raw_here
-    copies = (0.998 * all_masters - row_scale * raw).astype(jnp.bfloat16)
+    raw, raw_here, all_masters = lax.optimization_barrier((raw, raw_here, all_masters))
+    row_scale = lax.optimization_barrier(jnp.repeat(scales, width)[:, None])
+    new, copies = [], []
+    for at in (0, width):
+        span = slice(at, at + width)
+        scale = row_scale[span]
+        new.append((0.998 * masters_here[span] - scale * raw_here[span]).T)
+        copies.append((0.998 * all_masters[span] - scale * raw[span]).astype(jnp.bfloat16).T)
     return (
-        new_here[:width].T,
-        new_here[width:].T,
-        copies[:width].T,
-        copies[width:].T,
+        *new,
+        *copies,
         first_new[:, :width],
         second_new[:, :width],
         first_new[:, width:],

time: 139 us -> 137 us (0.986)
  other arithmetic: 1.87 us -> 6.14 us
  local copies, waits for them, and re-layouts: 7.72 us -> 5.82 us
  waiting for transfers between devices: 21.5 us -> 19.6 us
  blocking collectives: 67.5 us -> 65.9 us
    ppermute x2 -> x1, starting transfers between devices: 11.3 us -> 2.34 us  [local(): came = lax.ppermute(sent, 'tp_1', [(0, 1), (1, 0)])]
    ppermute x0 -> x1, starting transfers between devices: none -> 8.75 us  [local(): came = lax.ppermute(normed, 'tp_1', [(0, 1), (1, 0)])]
    all_to_all x3, waiting for transfers between devices: 19.9 us -> 17.9 us  [swap(): return lax.all_to_all(pieces, axes, 0, 0, tiled=True)]
    transpose x0 -> x2, other arithmetic: none -> 1.68 us  [the longest x1 0.97 us: local(): (0.998 * all_masters[span] - scale * raw[span]).astype(jnp.bfloat16)]
    transpose x2 -> x0, local copies, waits for them, and re-layouts: 1.47 us -> none  [the longest x1 0.84 us: local(): copies[width:]]
    all_gather x1, blocking collectives: 32.3 us -> 30.9 us  [local(): link = lax.all_gather(link, 'tp_0', axis=0, tiled=True)]
  transfers between devices with their start and end apart: 5 -> 5, of which waited for: 4 -> 3; matrix products, arithmetic and copies ran while one was open for 4% -> 8% of each run, Pallas kernels for 0% -> 0%
where the time goes in v5:
time: 137 us
  blocking collectives  65.9 us (48%)
  starting transfers between devices  34.2 us (25%)
  waiting for transfers between devices  19.6 us (14%)
  other arithmetic  6.14 us (4%)
  local copies, waits for them, and re-layouts  5.82 us (4%)
  matrix products  4.15 us (3%)
    all_to_all x2, blocking collectives, swap(): return lax.all_to_all(pieces, axes, 0, 0, tiled=True)  35 us
    all_gather x1, blocking collectives, local(): link = lax.all_gather(link, 'tp_0', axis=0, tiled=True)  30.9 us
    all_to_all x3, starting transfers between devices, swap(): return lax.all_to_all(pieces, axes, 0, 0, tiled=True)  23.1 us
    all_to_all x3, waiting for transfers between devices, swap(): return lax.all_to_all(pieces, axes, 0, 0, tiled=True)  17.9 us
    ppermute x1, starting transfers between devices, local(): came = lax.ppermute(normed, 'tp_1', [(0, 1), (1, 0)])  8.75 us
  transfers between devices with their start and end apart: 5, of which 3 were waited for; matrix products, arithmetic and copies ran while one was open for 8% of the time, Pallas kernels for 0%

profile of v5, /device:TPU:1, one launch (start us, length us, event | category | flops | bytes accessed | tf_op | source)
XLA Modules:
  0.0 136.9 jit_solution(17517048318877147163)
XLA Ops:
  0.6 8.7 %collective-permute-start = (bf16[64,3072]{1,0:T(8,128)(2,1)}, bf16[64,3072]{1,0:T(8,128)(2,1)S(1)}, u32[]{:S(2)}, u32[]{:S(2)}) collective-permute-start(bf16[64,3072]{1,0:T(8,128)(2,1)} %param.12), channel_id=1, source_target_pairs={{0,1},{1,0},{2,3},{3,2},{4,5},{5,4},{6,7},{7,6},{8,9},{9,8},{10,11... | collective-permute-start | bytes 1179656 | tf_op jit(solution)/shard_map/ppermute | solution.py:65
  9.4 0.7 select_reduce_fusion
  10.2 0.9 constant_dynamic-slice_fusion.2
  11.1 0.0 collective-permute-done
  11.2 0.0 copy-start
  11.2 1.0 copy.31
  12.2 9.6 %all-to-all-start = ((bf16[16,96,128]{2,1,0:T(8,128)(2,1)}), bf16[16,96,128]{2,1,0:T(8,128)(2,1)S(1)}, u32[]{:S(2)}, u32[]{:S(2)}) async-start(bf16[16,96,128]{2,1,0:T(8,128)(2,1)} %bitcast.1), calls=%async_computation | async-start | bytes 786432 | tf_op jit(solution)/shard_map/all_to_all | solution.py:18
  21.7 0.0 copy-done
  21.7 0.0 copy-start.4
  21.8 0.0 copy-start.5
  21.8 1.2 convolution_bitcast_fusion
  22.9 0.0 copy-done.4
  22.9 0.0 copy-done.5
  23.0 0.0 copy-start.8
  23.0 0.2 subtract_convert_fusion
  23.2 0.8 copy-done.1
  23.9 0.8 fusion.6
  24.7 0.0 copy-done.6
  24.7 0.0 copy-done.8
  24.7 0.3 reverse_select_fusion
  25.0 1.1 broadcast_in_dim.8
  26.1 2.3 %collective-permute-start.1 = (bf16[128,1536]{1,0:T(8,128)(2,1)}, bf16[128,1536]{1,0:T(8,128)(2,1)}, u32[]{:S(2)}, u32[]{:S(2)}) collective-permute-start(bf16[128,1536]{1,0:T(8,128)(2,1)} %fusion.6), channel_id=1, source_target_pairs={{0,1},{1,0},{2,3},{3,2},{4,5},{5,4},{6,7},{7,6},{8,9},{9,8},{10,11... | collective-permute-start | bytes 1179656 | tf_op jit(solution)/shard_map/ppermute | solution.py:103
  28.5 1.7 %collective-permute-done.1 = bf16[128,1536]{1,0:T(8,128)(2,1)} collective-permute-done((bf16[128,1536]{1,0:T(8,128)(2,1)}, bf16[128,1536]{1,0:T(8,128)(2,1)}, u32[]{:S(2)}, u32[]{:S(2)}) %collective-permute-start.1) | collective-permute-done | bytes 393248 | tf_op jit(solution)/shard_map/ppermute | solution.py:103
  30.1 1.1 broadcast_select_fusion.1
  31.3 1.0 pad_maximum_fusion
  32.3 8.5 %all-to-all-done = bf16[16,96,128]{2,1,0:T(8,128)(2,1)S(1)} async-done(((bf16[16,96,128]{2,1,0:T(8,128)(2,1)}), bf16[16,96,128]{2,1,0:T(8,128)(2,1)S(1)}, u32[]{:S(2)}, u32[]{:S(2)}) %all-to-all-start) | async-done | bytes 393248 | tf_op jit(solution)/shard_map/all_to_all | solution.py:18
  40.8 6.8 %all-to-all-start.1 = ((f32[16,128,128]{2,1,0:T(8,128)}), f32[16,128,128]{2,1,0:T(8,128)S(1)}, u32[]{:S(2)}, u32[]{:S(2)}) async-start(f32[16,128,128]{2,1,0:T(8,128)} %broadcast_in_dim.8), calls=%async_computation.1 | async-start | bytes 2097152 | tf_op jit(solution)/shard_map/all_to_all | solution.py:18
  47.6 0.0 copy-start.3
  47.6 0.3 fusion.2
  47.9 30.9 %all_gather.3 = f16[1536,256]{1,0:T(8,128)(2,1)S(1)} all-gather(f16[96,256]{1,0:T(8,128)(2,1)S(1)} %fusion.2), channel_id=1, replica_groups=mesh['fs_0'=4,'fs_1'=4,'tp_0'=16,'tp_1'=2] {'tp_0'}, dimensions={0}, use_global_device_ids=true | all-gather | bytes 835584 | tf_op jit(solution)/shard_map/all_gather | solution.py:114
  78.8 0.0 copy-done.3
  78.8 0.4 fusion.5
  79.2 0.4 convolution_add_fusion.2
  79.6 0.0 copy-start.10
  79.7 0.0 copy-start.11
  79.7 0.0 copy-start.12
  79.7 0.0 copy-start.13
  79.7 0.0 copy-start.2
  79.7 0.1 reshape.113
  79.9 0.0 all-to-all-done.1
  79.9 25.3 %all_to_all.25 = f32[32,16,128]{2,1,0:T(8,128)S(1)} all-to-all(f32[32,16,128]{2,1,0:T(8,128)S(1)} %bitcast.61), channel_id=1, replica_groups=mesh['fs_0'=4,'fs_1'=4,'tp_0'=16,'tp_1'=2] {'fs_0','fs_1','tp_1'}, dimensions={0} | all-to-all | bytes 524288 | tf_op jit(solution)/shard_map/all_to_all | solution.py:18
  105.2 0.0 copy-done.10
  105.2 0.1 add_divide_fusion
  105.3 9.8 %all_to_all.26 = f32[16,16,128]{2,1,0:T(8,128)S(1)} all-to-all(f32[16,16,128]{2,1,0:T(8,128)S(1)} %broadcast_in_dim.9), channel_id=1, replica_groups=mesh['fs_0'=4,'fs_1'=4,'tp_0'=16,'tp_1'=2] {'fs_0','fs_1'}, dimensions={0} | all-to-all | bytes 262144 | tf_op jit(solution)/shard_map/all_to_all | solution.py:18
  115.1 0.0 copy-done.2
  115.1 0.4 fusion.3
  115.5 0.6 broadcast_in_dim.10
  116.1 6.8 %all-to-all-start.4 = ((f32[32,1,128]{2,1,0:T(1,128)}), f32[32,1,128]{2,1,0:T(1,128)S(1)}, u32[]{:S(2)}, u32[]{:S(2)}) async-start(f32[32,1,128]{2,1,0:T(1,128)} %broadcast_in_dim.10), calls=%async_computation.4 | async-start | bytes 32768 | tf_op jit(solution)/shard_map/all_to_all | solution.py:18
  122.9 0.1 copy_bitcast_fusion
  123.1 0.5 fusion.15
  123.5 0.5 convolution_add_fusion.1
  124.0 0.0 copy-start.7
  124.0 0.0 copy-start.9
  124.0 0.5 convolution_add_fusion
  124.5 0.7 fusion.20
  125.2 0.1 constant_dynamic-slice_fusion
  125.3 9.4 %all-to-all-done.4 = f32[32,1,128]{2,1,0:T(1,128)S(1)} async-done(((f32[32,1,128]{2,1,0:T(1,128)}), f32[32,1,128]{2,1,0:T(1,128)S(1)}, u32[]{:S(2)}, u32[]{:S(2)}) %all-to-all-start.4) | async-done | bytes 16416 | tf_op jit(solution)/shard_map/all_to_all | solution.py:18
  134.7 0.1 reduce_sum.47
  134.8 0.1 reduce_sum.48
  134.9 0.1 broadcast_in_dim.11
  135.0 0.1 broadcast_in_dim_reshape.3
  135.1 0.1 slice_bitcast_fusion
  135.2 0.7 subtract_bitcast_fusion
  135.9 1.0 fusion.11
  (16 shorter events, 0.2 us)
Async XLA Ops:
  0.6 10.5 %collective-permute-start = (bf16[64,3072]{1,0:T(8,128)(2,1)}, bf16[64,3072]{1,0:T(8,128)(2,1)S(1)}, u32[]{:S(2)}, u32[]{:S(2)}) collective-permute-start(bf16[64,3072]{1,0:T(8,128)(2,1)} %param.12), channel_id=1, source_target_pairs={{0,1},{1,0},{2,3},{3,2},{4,5},{5,4},{6,7},{7,6},{8,9},{9,8},{10,11... | collective-permute-start | bytes 1179656 | tf_op jit(solution)/shard_map/ppermute | solution.py:65
  11.2 10.6 %copy-start = (bf16[2048,256]{1,0:T(8,128)(2,1)S(1)}, bf16[2048,256]{1,0:T(8,128)(2,1)}, u32[]{:S(2)}) copy-start(bf16[2048,256]{1,0:T(8,128)(2,1)} %param.17) | copy-start | bytes 3145732
  12.2 28.6 %all-to-all-start = ((bf16[16,96,128]{2,1,0:T(8,128)(2,1)}), bf16[16,96,128]{2,1,0:T(8,128)(2,1)S(1)}, u32[]{:S(2)}, u32[]{:S(2)}) async-start(bf16[16,96,128]{2,1,0:T(8,128)(2,1)} %bitcast.1), calls=%async_computation | async-start | bytes 786432 | tf_op jit(solution)/shard_map/all_to_all | solution.py:18
  21.7 1.2 copy-start.4
  21.8 1.2 copy-start.5
  22.9 1.0 copy-start.1
  23.0 1.8 %copy-start.6 = (f32[128,64]{0,1:T(8,128)S(1)}, f32[128,64]{0,1:T(8,128)}, u32[]{:S(2)}) copy-start(f32[128,64]{0,1:T(8,128)} %param.19) | copy-start | bytes 98308
  23.0 1.8 %copy-start.8 = (f32[128,64]{0,1:T(8,128)S(1)}, f32[128,64]{0,1:T(8,128)}, u32[]{:S(2)}) copy-start(f32[128,64]{0,1:T(8,128)} %param.18) | copy-start | bytes 98308
  26.1 4.0 %collective-permute-start.1 = (bf16[128,1536]{1,0:T(8,128)(2,1)}, bf16[128,1536]{1,0:T(8,128)(2,1)}, u32[]{:S(2)}, u32[]{:S(2)}) collective-permute-start(bf16[128,1536]{1,0:T(8,128)(2,1)} %fusion.6), channel_id=1, source_target_pairs={{0,1},{1,0},{2,3},{3,2},{4,5},{5,4},{6,7},{7,6},{8,9},{9,8},{10,11... | collective-permute-start | bytes 1179656 | tf_op jit(solution)/shard_map/ppermute | solution.py:103
  40.8 39.1 %all-to-all-start.1 = ((f32[16,128,128]{2,1,0:T(8,128)}), f32[16,128,128]{2,1,0:T(8,128)S(1)}, u32[]{:S(2)}, u32[]{:S(2)}) async-start(f32[16,128,128]{2,1,0:T(8,128)} %broadcast_in_dim.8), calls=%async_computation.1 | async-start | bytes 2097152 | tf_op jit(solution)/shard_map/all_to_all | solution.py:18
  47.6 31.2 %copy-start.3 = (bf16[256,1536]{1,0:T(8,128)(2,1)S(1)}, bf16[256,1536]{1,0:T(8,128)(2,1)}, u32[]{:S(2)}) copy-start(bf16[256,1536]{1,0:T(8,128)(2,1)} %pad_maximum_fusion) | copy-start | bytes 2359300
  79.6 25.6 %copy-start.10 = (f32[16,64]{1,0:T(8,128)S(1)}, f32[16,64]{1,0:T(8,128)}, u32[]{:S(2)}) copy-start(f32[16,64]{1,0:T(8,128)} %param.23) | copy-start | bytes 12292
  79.7 25.6 %copy-start.11 = (f32[16,64]{1,0:T(8,128)S(1)}, f32[16,64]{1,0:T(8,128)}, u32[]{:S(2)}) copy-start(f32[16,64]{1,0:T(8,128)} %param.21) | copy-start | bytes 12292
  79.7 25.6 %copy-start.12 = (f32[16,64]{1,0:T(8,128)S(1)}, f32[16,64]{1,0:T(8,128)}, u32[]{:S(2)}) copy-start(f32[16,64]{1,0:T(8,128)} %param.22) | copy-start | bytes 12292
  79.7 25.6 %copy-start.13 = (f32[16,64]{1,0:T(8,128)S(1)}, f32[16,64]{1,0:T(8,128)}, u32[]{:S(2)}) copy-start(f32[16,64]{1,0:T(8,128)} %param.20) | copy-start | bytes 12292
  79.7 35.4 %copy-start.2 = (f32[256,256]{1,0:T(8,128)S(1)}, f32[256,256]{1,0:T(8,128)}, u32[]{:S(2)}) copy-start(f32[256,256]{1,0:T(8,128)} %convolution_bitcast_fusion) | copy-start | bytes 786436
  116.1 18.6 %all-to-all-start.4 = ((f32[32,1,128]{2,1,0:T(1,128)}), f32[32,1,128]{2,1,0:T(1,128)S(1)}, u32[]{:S(2)}, u32[]{:S(2)}) async-start(f32[32,1,128]{2,1,0:T(1,128)} %broadcast_in_dim.10), calls=%async_computation.4 | async-start | bytes 32768 | tf_op jit(solution)/shard_map/all_to_all | solution.py:18
  124.0 11.1 %copy-start.7 = (f32[128,64]{0,1:T(8,128)S(1)}, f32[128,64]{0,1:T(8,128)}, u32[]{:S(2)}) copy-start(f32[128,64]{0,1:T(8,128)} %param.19) | copy-start | bytes 98308
  124.0 11.1 %copy-start.9 = (f32[128,64]{0,1:T(8,128)S(1)}, f32[128,64]{0,1:T(8,128)}, u32[]{:S(2)}) copy-start(f32[128,64]{0,1:T(8,128)} %param.18) | copy-start | bytes 98308

commit v6 on v5

--- a/solution.py
+++ b/solution.py
@@ -12,6 +12,7 @@
 FS = ("fs_0", "fs_1")
 FS_CORE = ("fs_0", "fs_1", "tp_1")
 LINK_SCALE = 32.0
+MASTER_SCALE = 1024.0
 
 
 def swap(pieces, axes):
@@ -30,6 +31,15 @@
         parts.append(part.astype(jnp.bfloat16))
         values = values - part
     return parts
+
+
+def coded(masters):
+    return (masters * jnp.abs(masters) * MASTER_SCALE**2).astype(jnp.float16)
+
+
+def decoded(codes):
+    values = codes.astype(jnp.float32)
+    return jnp.sign(values) * jnp.sqrt(jnp.abs(values)) * (1.0 / MASTER_SCALE)
 
 
 def local(
@@ -90,7 +100,8 @@
     kept = lax.dynamic_slice_in_dim(stacked, core * half, half, 1)
     sent = lax.dynamic_slice_in_dim(stacked, (1 - core) * half, half, 1)
     masters_here = jnp.concatenate([key_master.T, value_master.T], axis=0)
-    masters = jnp.broadcast_to(masters_here[None], (fs_size, *masters_here.shape))
+    masters = coded(masters_here)
+    masters = jnp.broadcast_to(masters[None], (fs_size, *masters.shape))
     late_factor = blocks.reshape(rows, rank)
     gram = lax.dot_general(
         late_factor, late_factor, (((0,), (0,)), ((), ())), preferred_element_type=jnp.float32
@@ -145,7 +156,7 @@
         for part in in_bf16_parts(directions, 3)
     )
     raw_here = lax.dynamic_slice_in_dim(raw, fs_at, fs_rows, 1, allow_negative_indices=False)
-    all_masters = masters.transpose(1, 0, 2).reshape(2 * width, rows)
+    all_masters = decoded(masters).transpose(1, 0, 2).reshape(2 * width, rows)
     raw, raw_here, all_masters = lax.optimization_barrier((raw, raw_here, all_masters))
     row_scale = lax.optimization_barrier(jnp.repeat(scales, width)[:, None])
     new, copies = [], []

time: 137 us -> 138 us (level)
  no operation moved by 1% of the time
where the time goes in v6:
time: 138 us; the launch traced here: 137 us
  blocking collectives  66.2 us (48%)
  starting transfers between devices  34.2 us (25%)
  waiting for transfers between devices  19.4 us (14%)
  other arithmetic  6.69 us (5%)
  local copies, waits for them, and re-layouts  6.15 us (4%)
  matrix products  3.43 us (2%)
    all_to_all x2, blocking collectives, swap(): return lax.all_to_all(pieces, axes, 0, 0, tiled=True)  36.1 us
    all_gather x1, blocking collectives, local(): link = lax.all_gather(link, 'tp_0', axis=0, tiled=True)  30.1 us
    all_to_all x3, starting transfers between devices, swap(): return lax.all_to_all(pieces, axes, 0, 0, tiled=True)  23.1 us
    all_to_all x3, waiting for transfers between devices, swap(): return lax.all_to_all(pieces, axes, 0, 0, tiled=True)  17.7 us
    ppermute x1, starting transfers between devices, local(): came = lax.ppermute(normed, 'tp_1', [(0, 1), (1, 0)])  8.75 us
  transfers between devices with their start and end apart: 5, of which 3 were waited for; matrix products, arithmetic and copies ran while one was open for 8% of the time, Pallas kernels for 0%

profile of v6, /device:TPU:1, one launch (start us, length us, event | category | flops | bytes accessed | tf_op | source)
XLA Modules:
  0.0 137.0 jit_solution(3933963086586227247)
XLA Ops:
  0.6 8.7 %collective-permute-start = (bf16[64,3072]{1,0:T(8,128)(2,1)}, bf16[64,3072]{1,0:T(8,128)(2,1)S(1)}, u32[]{:S(2)}, u32[]{:S(2)}) collective-permute-start(bf16[64,3072]{1,0:T(8,128)(2,1)} %param.12), channel_id=1, source_target_pairs={{0,1},{1,0},{2,3},{3,2},{4,5},{5,4},{6,7},{7,6},{8,9},{9,8},{10,11... | collective-permute-start | bytes 1179656 | tf_op jit(solution)/shard_map/ppermute | solution.py:75
  9.4 0.7 select_reduce_fusion
  10.2 0.9 constant_dynamic-slice_fusion.2
  11.1 0.0 collective-permute-done
  11.2 0.0 copy-start
  11.2 0.9 copy.31
  12.1 9.6 %all-to-all-start = ((bf16[16,96,128]{2,1,0:T(8,128)(2,1)}), bf16[16,96,128]{2,1,0:T(8,128)(2,1)S(1)}, u32[]{:S(2)}, u32[]{:S(2)}) async-start(bf16[16,96,128]{2,1,0:T(8,128)(2,1)} %bitcast.1), calls=%async_computation | async-start | bytes 786432 | tf_op jit(solution)/shard_map/all_to_all | solution.py:19
  21.7 0.0 copy-done
  21.7 0.0 copy-start.3
  21.7 0.0 copy-start.4
  21.7 0.5 convolution_bitcast_fusion
  22.2 0.5 copy-done.3
  22.7 0.1 copy-done.4
  22.8 0.2 subtract_convert_fusion
  23.0 0.8 copy-done.1
  23.8 0.8 fusion.10
  24.6 0.0 copy-done.5
  24.6 0.0 copy-done.7
  24.6 0.3 reverse_select_fusion
  24.9 0.9 broadcast_in_dim.8
  25.8 2.3 %collective-permute-start.1 = (bf16[128,1536]{1,0:T(8,128)(2,1)}, bf16[128,1536]{1,0:T(8,128)(2,1)}, u32[]{:S(2)}, u32[]{:S(2)}) collective-permute-start(bf16[128,1536]{1,0:T(8,128)(2,1)} %fusion.10), channel_id=1, source_target_pairs={{0,1},{1,0},{2,3},{3,2},{4,5},{5,4},{6,7},{7,6},{8,9},{9,8},{10,11... | collective-permute-start | bytes 1179656 | tf_op jit(solution)/shard_map/ppermute | solution.py:114
  28.2 1.7 %collective-permute-done.1 = bf16[128,1536]{1,0:T(8,128)(2,1)} collective-permute-done((bf16[128,1536]{1,0:T(8,128)(2,1)}, bf16[128,1536]{1,0:T(8,128)(2,1)}, u32[]{:S(2)}, u32[]{:S(2)}) %collective-permute-start.1) | collective-permute-done | bytes 393248 | tf_op jit(solution)/shard_map/ppermute | solution.py:114
  29.9 1.1 broadcast_select_fusion.1
  31.0 0.9 pad_maximum_fusion
  31.9 8.8 %all-to-all-done = bf16[16,96,128]{2,1,0:T(8,128)(2,1)S(1)} async-done(((bf16[16,96,128]{2,1,0:T(8,128)(2,1)}), bf16[16,96,128]{2,1,0:T(8,128)(2,1)S(1)}, u32[]{:S(2)}, u32[]{:S(2)}) %all-to-all-start) | async-done | bytes 393248 | tf_op jit(solution)/shard_map/all_to_all | solution.py:19
  40.8 6.8 %all-to-all-start.1 = ((f16[16,128,128]{2,1,0:T(8,128)(2,1)}), f16[16,128,128]{2,1,0:T(8,128)(2,1)S(1)}, u32[]{:S(2)}, u32[]{:S(2)}) async-start(f16[16,128,128]{2,1,0:T(8,128)(2,1)} %broadcast_in_dim.8), calls=%async_computation.1 | async-start | bytes 1048576 | tf_op jit(solution)/shard_map/all_to_all | solution.py:19
  47.5 0.0 copy-start.2
  47.5 0.3 fusion.2
  47.8 30.1 %all_gather.3 = f16[1536,256]{1,0:T(8,128)(2,1)S(1)} all-gather(f16[96,256]{1,0:T(8,128)(2,1)S(1)} %fusion.2), channel_id=1, replica_groups=mesh['fs_0'=4,'fs_1'=4,'tp_0'=16,'tp_1'=2] {'tp_0'}, dimensions={0}, use_global_device_ids=true | all-gather | bytes 835584 | tf_op jit(solution)/shard_map/all_gather | solution.py:125
  77.9 0.0 copy-done.2
  77.9 0.4 fusion.9
  78.3 0.4 convolution_add_fusion.2
  78.8 0.0 copy-start.9
  78.8 0.0 copy-start.10
  78.8 0.0 copy-start.11
  78.8 0.0 copy-start.12
  78.8 0.1 reshape.142
  79.0 0.0 all-to-all-done.1
  79.0 26.4 %all_to_all.25 = f32[32,16,128]{2,1,0:T(8,128)S(1)} all-to-all(f32[32,16,128]{2,1,0:T(8,128)S(1)} %bitcast.61), channel_id=1, replica_groups=mesh['fs_0'=4,'fs_1'=4,'tp_0'=16,'tp_1'=2] {'fs_0','fs_1','tp_1'}, dimensions={0} | all-to-all | bytes 524288 | tf_op jit(solution)/shard_map/all_to_all | solution.py:19
  105.4 0.0 copy-done.9
  105.4 0.0 copy-done.10
  105.4 0.0 copy-done.11
  105.4 0.0 copy-done.12
  105.5 0.1 add_divide_fusion
  105.6 9.8 %all_to_all.26 = f32[16,16,128]{2,1,0:T(8,128)S(1)} all-to-all(f32[16,16,128]{2,1,0:T(8,128)S(1)} %broadcast_in_dim.9), channel_id=1, replica_groups=mesh['fs_0'=4,'fs_1'=4,'tp_0'=16,'tp_1'=2] {'fs_0','fs_1'}, dimensions={0} | all-to-all | bytes 262144 | tf_op jit(solution)/shard_map/all_to_all | solution.py:19
  115.3 0.4 fusion.3
  115.7 0.6 broadcast_in_dim.10
  116.3 6.8 %all-to-all-start.4 = ((f32[32,1,128]{2,1,0:T(1,128)}), f32[32,1,128]{2,1,0:T(1,128)S(1)}, u32[]{:S(2)}, u32[]{:S(2)}) async-start(f32[32,1,128]{2,1,0:T(1,128)} %broadcast_in_dim.10), calls=%async_computation.4 | async-start | bytes 32768 | tf_op jit(solution)/shard_map/all_to_all | solution.py:19
  123.1 0.6 copy_bitcast_fusion
  123.7 0.5 fusion.21
  124.2 0.5 convolution_add_fusion.1
  124.7 0.0 copy-start.6
  124.7 0.0 copy-start.8
  124.7 0.5 convolution_add_fusion
  125.2 0.7 fusion.26
  125.9 0.1 constant_dynamic-slice_fusion
  126.0 8.9 %all-to-all-done.4 = f32[32,1,128]{2,1,0:T(1,128)S(1)} async-done(((f32[32,1,128]{2,1,0:T(1,128)}), f32[32,1,128]{2,1,0:T(1,128)S(1)}, u32[]{:S(2)}, u32[]{:S(2)}) %all-to-all-start.4) | async-done | bytes 16416 | tf_op jit(solution)/shard_map/all_to_all | solution.py:19
  134.9 0.1 reduce_sum.47
  135.0 0.1 reduce_sum.48
  135.1 0.1 broadcast_in_dim.11
  135.2 0.1 broadcast_in_dim_reshape.3
  135.2 0.1 slice_bitcast_fusion
  135.3 0.7 subtract_bitcast_fusion
  136.0 1.0 fusion.15
  (14 shorter events, 0.2 us)
Async XLA Ops:
  0.6 10.5 %collective-permute-start = (bf16[64,3072]{1,0:T(8,128)(2,1)}, bf16[64,3072]{1,0:T(8,128)(2,1)S(1)}, u32[]{:S(2)}, u32[]{:S(2)}) collective-permute-start(bf16[64,3072]{1,0:T(8,128)(2,1)} %param.12), channel_id=1, source_target_pairs={{0,1},{1,0},{2,3},{3,2},{4,5},{5,4},{6,7},{7,6},{8,9},{9,8},{10,11... | collective-permute-start | bytes 1179656 | tf_op jit(solution)/shard_map/ppermute | solution.py:75
  11.2 10.5 %copy-start = (bf16[2048,256]{1,0:T(8,128)(2,1)S(1)}, bf16[2048,256]{1,0:T(8,128)(2,1)}, u32[]{:S(2)}) copy-start(bf16[2048,256]{1,0:T(8,128)(2,1)} %param.17) | copy-start | bytes 3145732
  12.1 28.6 %all-to-all-start = ((bf16[16,96,128]{2,1,0:T(8,128)(2,1)}), bf16[16,96,128]{2,1,0:T(8,128)(2,1)S(1)}, u32[]{:S(2)}, u32[]{:S(2)}) async-start(bf16[16,96,128]{2,1,0:T(8,128)(2,1)} %bitcast.1), calls=%async_computation | async-start | bytes 786432 | tf_op jit(solution)/shard_map/all_to_all | solution.py:19
  21.7 1.0 copy-start.3
  21.7 1.1 copy-start.4
  22.8 1.0 copy-start.1
  22.8 1.8 %copy-start.5 = (f32[128,64]{0,1:T(8,128)S(1)}, f32[128,64]{0,1:T(8,128)}, u32[]{:S(2)}) copy-start(f32[128,64]{0,1:T(8,128)} %param.19) | copy-start | bytes 98308
  22.8 1.8 %copy-start.7 = (f32[128,64]{0,1:T(8,128)S(1)}, f32[128,64]{0,1:T(8,128)}, u32[]{:S(2)}) copy-start(f32[128,64]{0,1:T(8,128)} %param.18) | copy-start | bytes 98308
  25.8 4.0 %collective-permute-start.1 = (bf16[128,1536]{1,0:T(8,128)(2,1)}, bf16[128,1536]{1,0:T(8,128)(2,1)}, u32[]{:S(2)}, u32[]{:S(2)}) collective-permute-start(bf16[128,1536]{1,0:T(8,128)(2,1)} %fusion.10), channel_id=1, source_target_pairs={{0,1},{1,0},{2,3},{3,2},{4,5},{5,4},{6,7},{7,6},{8,9},{9,8},{10,11... | collective-permute-start | bytes 1179656 | tf_op jit(solution)/shard_map/ppermute | solution.py:114
  40.8 38.2 %all-to-all-start.1 = ((f16[16,128,128]{2,1,0:T(8,128)(2,1)}), f16[16,128,128]{2,1,0:T(8,128)(2,1)S(1)}, u32[]{:S(2)}, u32[]{:S(2)}) async-start(f16[16,128,128]{2,1,0:T(8,128)(2,1)} %broadcast_in_dim.8), calls=%async_computation.1 | async-start | bytes 1048576 | tf_op jit(solution)/shard_map/all_to_all | solution.py:19
  47.5 30.4 %copy-start.2 = (bf16[256,1536]{1,0:T(8,128)(2,1)S(1)}, bf16[256,1536]{1,0:T(8,128)(2,1)}, u32[]{:S(2)}) copy-start(bf16[256,1536]{1,0:T(8,128)(2,1)} %pad_maximum_fusion) | copy-start | bytes 2359300
  78.8 26.7 %copy-start.9 = (f32[16,64]{1,0:T(8,128)S(1)}, f32[16,64]{1,0:T(8,128)}, u32[]{:S(2)}) copy-start(f32[16,64]{1,0:T(8,128)} %param.23) | copy-start | bytes 12292
  78.8 26.7 %copy-start.10 = (f32[16,64]{1,0:T(8,128)S(1)}, f32[16,64]{1,0:T(8,128)}, u32[]{:S(2)}) copy-start(f32[16,64]{1,0:T(8,128)} %param.21) | copy-start | bytes 12292
  78.8 26.7 %copy-start.11 = (f32[16,64]{1,0:T(8,128)S(1)}, f32[16,64]{1,0:T(8,128)}, u32[]{:S(2)}) copy-start(f32[16,64]{1,0:T(8,128)} %param.22) | copy-start | bytes 12292
  78.8 26.7 %copy-start.12 = (f32[16,64]{1,0:T(8,128)S(1)}, f32[16,64]{1,0:T(8,128)}, u32[]{:S(2)}) copy-start(f32[16,64]{1,0:T(8,128)} %param.20) | copy-start | bytes 12292
  116.3 18.5 %all-to-all-start.4 = ((f32[32,1,128]{2,1,0:T(1,128)}), f32[32,1,128]{2,1,0:T(1,128)S(1)}, u32[]{:S(2)}, u32[]{:S(2)}) async-start(f32[32,1,128]{2,1,0:T(1,128)} %broadcast_in_dim.10), calls=%async_computation.4 | async-start | bytes 32768 | tf_op jit(solution)/shard_map/all_to_all | solution.py:19
  124.7 10.6 %copy-start.6 = (f32[128,64]{0,1:T(8,128)S(1)}, f32[128,64]{0,1:T(8,128)}, u32[]{:S(2)}) copy-start(f32[128,64]{0,1:T(8,128)} %param.19) | copy-start | bytes 98308
  124.7 10.6 %copy-start.8 = (f32[128,64]{0,1:T(8,128)S(1)}, f32[128,64]{0,1:T(8,128)}, u32[]{:S(2)}) copy-start(f32[128,64]{0,1:T(8,128)} %param.18) | copy-start | bytes 98308

commit v7 on v5

--- a/solution.py
+++ b/solution.py
@@ -12,15 +12,25 @@
 FS = ("fs_0", "fs_1")
 FS_CORE = ("fs_0", "fs_1", "tp_1")
 LINK_SCALE = 32.0
-
-
-def swap(pieces, axes):
-    return lax.all_to_all(pieces, axes, 0, 0, tiled=True)
+FIRST_CHIP = 11
+FIRST_CORE = 1
+
+
+def swap(pieces, axes, groups=None):
+    return lax.all_to_all(pieces, axes, 0, 0, tiled=True, axis_index_groups=groups)
 
 
 def to_all(shard, axes):
     size = lax.axis_size(axes)
     return swap(jnp.broadcast_to(shard[None], (size, *shard.shape)), axes)
+
+
+def core_order(cores):
+    return [(FIRST_CORE + c) % cores for c in range(cores)]
+
+
+def chip_order(chips):
+    return [(FIRST_CHIP + z) % chips for z in range(chips)]
 
 
 def in_bf16_parts(values, count):
@@ -55,6 +65,9 @@
     heads = lambdas.shape[0]
     fs_rows = key_master.shape[0]
     half = tokens // cores
+    rings = [[z * cores + c for z in chip_order(chips)] for c in range(cores)]
+    whole = [[z * cores + c for z in chip_order(chips) for c in core_order(cores)]]
+    planes = [[f * cores + c for f in range(fs_size) for c in core_order(cores)]]
     share = half // chips
 
     rows_here = lax.axis_index(TP) * width + lax.iota(jnp.int32, width)
@@ -81,7 +94,7 @@
             value_master,
         )
     )
-    by_token = swap(by_token, "tp_0")
+    by_token = swap(by_token, TP, rings)
 
     value_cot = (
         first_map.astype(jnp.float32) - row_lambda[:, None] * second_map.astype(jnp.float32)
@@ -95,13 +108,15 @@
     gram = lax.dot_general(
         late_factor, late_factor, (((0,), (0,)), ((), ())), preferred_element_type=jnp.float32
     )
-    own_first = jnp.where(core == 0, blocks, blocks[:, ::-1]).reshape(rows, rank)
+    own_first = jnp.where(core == 0, blocks, blocks[:, ::-1])
+    own_first = jnp.roll(own_first, -FIRST_CHIP, axis=0).reshape(rows, rank)
     fs_at = lax.axis_index(FS) * fs_rows
     masters, gram, own_first, fs_at, sent = lax.optimization_barrier(
         (masters, gram, own_first, fs_at, sent)
     )
     came = lax.ppermute(sent, "tp_1", [(0, 1), (1, 0)])
-    cots = jnp.concatenate([jnp.where(core == 0, kept, came), jnp.where(core == 0, came, kept)])
+    is_first = core == FIRST_CORE
+    cots = jnp.concatenate([jnp.where(is_first, kept, came), jnp.where(is_first, came, kept)])
     cots, masters, by_token = lax.optimization_barrier((cots, masters, by_token))
     product = lax.dot_general(
         by_token.transpose(1, 0, 2).reshape(share, rows),
@@ -111,7 +126,7 @@
     )
     link = (product * LINK_SCALE).astype(jnp.float16)
     masters = swap(masters, FS)
-    link = lax.all_gather(link, "tp_0", axis=0, tiled=True)
+    link = lax.all_gather(link, TP, axis=0, tiled=True, axis_index_groups=rings)
 
     high, low = in_bf16_parts(link.astype(jnp.float32), 2)
     dims = (((0,), (1,)), ((), ()))
@@ -121,7 +136,7 @@
     pieces = pieces.transpose(0, 2, 1, 3).reshape(fs_size * cores, rank // fs_size, 2 * width)
     masters, pieces = lax.optimization_barrier((masters, pieces))
     norm_scale = 1.0 / (LINK_SCALE * math.sqrt(tokens * fs_size))
-    small = jnp.sum(swap(pieces, FS_CORE), axis=0) * norm_scale
+    small = jnp.sum(swap(pieces, FS_CORE, planes), axis=0) * norm_scale
 
     first = jnp.concatenate([key_first, value_first], axis=1)
     second = jnp.concatenate([key_second, value_second], axis=1)
@@ -136,16 +151,17 @@
     directions, squares, masters, first_new, second_new = lax.optimization_barrier(
         (directions, squares, masters, first_new, second_new)
     )
-    squares = jnp.sum(swap(squares, TP).reshape(cores * chips, 2, width), axis=(0, 2))
-    cells = rows * width * cores * chips
-    scales = 0.02 / jnp.sqrt(squares / cells + 0.01)
-
+    squares = swap(squares, TP, whole)
     raw = sum(
         lax.dot_general(part, factor, (((0,), (1,)), ((), ())), preferred_element_type=jnp.float32)
         for part in in_bf16_parts(directions, 3)
     )
     raw_here = lax.dynamic_slice_in_dim(raw, fs_at, fs_rows, 1, allow_negative_indices=False)
     all_masters = masters.transpose(1, 0, 2).reshape(2 * width, rows)
+    squares = jnp.sum(squares.reshape(cores * chips, 2, width), axis=(0, 2))
+    cells = rows * width * cores * chips
+    scales = 0.02 / jnp.sqrt(squares / cells + 0.01)
+
     raw, raw_here, all_masters = lax.optimization_barrier((raw, raw_here, all_masters))
     row_scale = lax.optimization_barrier(jnp.repeat(scales, width)[:, None])
     new, copies = [], []

time: 137 us -> 132 us (0.964)
  blocking collectives: 65.9 us -> 58.9 us
  starting transfers between devices: 34.2 us -> 39.4 us
  waiting for transfers between devices: 19.6 us -> 14.8 us
    all_gather x1, blocking collectives: 30.9 us -> 25.6 us  [local(): link = lax.all_gather(link, TP, axis=0, tiled=True, axis_index_groups=rings)]
    all_to_all x3, starting transfers between devices: 23.1 us -> 28.3 us  [swap(): lax.all_to_all(pieces, axes, 0, 0, tiled=True, axis_index_groups=groups)]
    all_to_all x3, waiting for transfers between devices: 17.9 us -> 13.2 us  [swap(): lax.all_to_all(pieces, axes, 0, 0, tiled=True, axis_index_groups=groups)]
    all_to_all x2, blocking collectives: 35 us -> 33.3 us  [swap(): lax.all_to_all(pieces, axes, 0, 0, tiled=True, axis_index_groups=groups)]
  transfers between devices with their start and end apart: 5 -> 5, of which waited for: 3 -> 3; matrix products, arithmetic and copies ran while one was open for 8% -> 7% of each run, Pallas kernels for 0% -> 0%
where the time goes in v7:
time: 132 us
  blocking collectives  58.9 us (45%)
  starting transfers between devices  39.4 us (30%)
  waiting for transfers between devices  14.8 us (11%)
  local copies, waits for them, and re-layouts  7.18 us (5%)
  other arithmetic  6.23 us (5%)
  matrix products  4.15 us (3%)
    all_to_all x2, blocking collectives, swap(): lax.all_to_all(pieces, axes, 0, 0, tiled=True, axis_index_groups=groups)  33.3 us
    all_to_all x3, starting transfers between devices, swap(): lax.all_to_all(pieces, axes, 0, 0, tiled=True, axis_index_groups=groups)  28.3 us
    all_gather x1, blocking collectives, local(): link = lax.all_gather(link, TP, axis=0, tiled=True, axis_index_groups=rings)  25.6 us
    all_to_all x3, waiting for transfers between devices, swap(): lax.all_to_all(pieces, axes, 0, 0, tiled=True, axis_index_groups=groups)  13.2 us
    ppermute x1, starting transfers between devices, local(): came = lax.ppermute(normed, 'tp_1', [(0, 1), (1, 0)])  8.75 us
  transfers between devices with their start and end apart: 5, of which 3 were waited for; matrix products, arithmetic and copies ran while one was open for 7% of the time, Pallas kernels for 0%

profile of v7, /device:TPU:1, one launch (start us, length us, event | category | flops | bytes accessed | tf_op | source)
XLA Modules:
  0.0 131.8 jit_solution(16971087409235075540)
XLA Ops:
  0.6 8.7 %collective-permute-start = (bf16[64,3072]{1,0:T(8,128)(2,1)}, bf16[64,3072]{1,0:T(8,128)(2,1)S(1)}, u32[]{:S(2)}, u32[]{:S(2)}) collective-permute-start(bf16[64,3072]{1,0:T(8,128)(2,1)} %param.12), channel_id=1, source_target_pairs={{0,1},{1,0},{2,3},{3,2},{4,5},{5,4},{6,7},{7,6},{8,9},{9,8},{10,11... | collective-permute-start | bytes 1179656 | tf_op jit(solution)/shard_map/ppermute | solution.py:78
  9.4 0.7 select_reduce_fusion
  10.2 0.9 constant_dynamic-slice_fusion.2
  11.1 0.0 copy-start
  11.1 0.0 collective-permute-done
  11.2 1.0 copy.31
  12.2 0.3 copy-done
  12.4 0.3 reverse_select_fusion
  12.7 0.1 slice.59
  12.8 10.3 %all-to-all-start = ((bf16[16,96,128]{2,1,0:T(8,128)(2,1)}), bf16[16,96,128]{2,1,0:T(8,128)(2,1)S(1)}, u32[]{:S(2)}, u32[]{:S(2)}) async-start(bf16[16,96,128]{2,1,0:T(8,128)(2,1)} %bitcast.1), calls=%async_computation | async-start | bytes 786432 | tf_op jit(solution)/shard_map/all_to_all | solution.py:20
  23.1 0.0 copy-start.5
  23.1 0.1 pad_maximum_fusion
  23.2 0.9 copy-done.4
  24.1 0.1 copy-done.5
  24.2 0.2 subtract_convert_fusion
  24.4 0.8 copy-done.1
  25.2 0.8 fusion.6
  26.0 0.0 copy-done.8
  26.0 1.2 convolution_bitcast_fusion
  27.2 1.1 broadcast_in_dim.8
  28.3 2.4 %collective-permute-start.1 = (bf16[128,1536]{1,0:T(8,128)(2,1)}, bf16[128,1536]{1,0:T(8,128)(2,1)}, u32[]{:S(2)}, u32[]{:S(2)}) collective-permute-start(bf16[128,1536]{1,0:T(8,128)(2,1)} %fusion.6), channel_id=1, source_target_pairs={{0,1},{1,0},{2,3},{3,2},{4,5},{5,4},{6,7},{7,6},{8,9},{9,8},{10,11... | collective-permute-start | bytes 1179656 | tf_op jit(solution)/shard_map/ppermute | solution.py:117
  30.6 1.7 %collective-permute-done.1 = bf16[128,1536]{1,0:T(8,128)(2,1)} collective-permute-done((bf16[128,1536]{1,0:T(8,128)(2,1)}, bf16[128,1536]{1,0:T(8,128)(2,1)}, u32[]{:S(2)}, u32[]{:S(2)}) %collective-permute-start.1) | collective-permute-done | bytes 393248 | tf_op jit(solution)/shard_map/ppermute | solution.py:117
  32.3 1.1 broadcast_select_fusion.1
  33.5 1.0 pad_maximum_fusion.1
  34.5 9.1 %all-to-all-done = bf16[16,96,128]{2,1,0:T(8,128)(2,1)S(1)} async-done(((bf16[16,96,128]{2,1,0:T(8,128)(2,1)}), bf16[16,96,128]{2,1,0:T(8,128)(2,1)S(1)}, u32[]{:S(2)}, u32[]{:S(2)}) %all-to-all-start) | async-done | bytes 393248 | tf_op jit(solution)/shard_map/all_to_all | solution.py:20
  43.5 6.8 %all-to-all-start.1 = ((f32[16,128,128]{2,1,0:T(8,128)}), f32[16,128,128]{2,1,0:T(8,128)S(1)}, u32[]{:S(2)}, u32[]{:S(2)}) async-start(f32[16,128,128]{2,1,0:T(8,128)} %broadcast_in_dim.8), calls=%async_computation.1 | async-start | bytes 2097152 | tf_op jit(solution)/shard_map/all_to_all | solution.py:20
  50.3 0.3 fusion.2
  50.6 25.6 %all_gather.3 = f16[1536,256]{1,0:T(8,128)(2,1)S(1)} all-gather(f16[96,256]{1,0:T(8,128)(2,1)S(1)} %fusion.2), channel_id=1, replica_groups={{22,24,26,28,30,0,2,4,6,8,10,12,14,16,18,20},{23,25,27,29,31,1,3,5,7,9,..., dimensions={0}, use_global_device_ids=true | all-gather | bytes 835584 | tf_op jit(solution)/shard_map/all_gather | solution.py:129
  76.3 0.4 fusion.5
  76.7 0.4 convolution_add_fusion.2
  77.1 0.0 copy-start.10
  77.1 0.0 copy-start.11
  77.1 0.0 copy-start.12
  77.1 0.0 copy-start.13
  77.2 0.0 copy-start.2
  77.2 0.1 reshape.113
  77.3 0.0 all-to-all-done.1
  77.3 23.6 %all_to_all.25 = f32[32,16,128]{2,1,0:T(8,128)S(1)} all-to-all(f32[32,16,128]{2,1,0:T(8,128)S(1)} %bitcast.61), channel_id=1, replica_groups={{1,0,33,32,65,64,97,96,129,128,161,160,193,192,225,224,257,256,289,288,..., dimensions={0} | all-to-all | bytes 524288 | tf_op jit(solution)/shard_map/all_to_all | solution.py:20
  100.9 0.0 copy-done.10
  100.9 0.0 copy-done.11
  101.0 0.0 copy-done.12
  101.0 0.0 copy-done.13
  101.0 0.1 add_divide_fusion
  101.1 9.7 %all_to_all.26 = f32[16,16,128]{2,1,0:T(8,128)S(1)} all-to-all(f32[16,16,128]{2,1,0:T(8,128)S(1)} %broadcast_in_dim.9), channel_id=1, replica_groups=mesh['fs_0'=4,'fs_1'=4,'tp_0'=16,'tp_1'=2] {'fs_0','fs_1'}, dimensions={0} | all-to-all | bytes 262144 | tf_op jit(solution)/shard_map/all_to_all | solution.py:20
  110.8 0.4 fusion.3
  111.2 0.6 broadcast_in_dim.10
  111.8 0.5 fusion.15
  112.3 0.5 convolution_add_fusion.1
  112.8 0.5 convolution_add_fusion
  113.3 0.0 copy-start.7
  113.3 0.0 copy-start.9
  113.3 0.1 copy_bitcast_fusion
  113.4 11.3 %all-to-all-start.4 = ((f32[32,1,128]{2,1,0:T(1,128)}), f32[32,1,128]{2,1,0:T(1,128)S(1)}, u32[]{:S(2)}, u32[]{:S(2)}) async-start(f32[32,1,128]{2,1,0:T(1,128)} %broadcast_in_dim.10), calls=%async_computation.4 | async-start | bytes 32768 | tf_op jit(solution)/shard_map/all_to_all | solution.py:20
  124.7 0.7 fusion.20
  125.4 0.1 constant_dynamic-slice_fusion
  125.5 4.1 %all-to-all-done.4 = f32[32,1,128]{2,1,0:T(1,128)S(1)} async-done(((f32[32,1,128]{2,1,0:T(1,128)}), f32[32,1,128]{2,1,0:T(1,128)S(1)}, u32[]{:S(2)}, u32[]{:S(2)}) %all-to-all-start.4) | async-done | bytes 16416 | tf_op jit(solution)/shard_map/all_to_all | solution.py:20
  129.6 0.1 reduce_sum.47
  129.7 0.1 reduce_sum.48
  129.8 0.1 broadcast_in_dim.11
  129.9 0.1 broadcast_in_dim_reshape.3
  130.0 0.1 slice_bitcast_fusion
  130.1 0.0 copy-done.9
  130.1 0.7 subtract_bitcast_fusion
  130.8 1.0 fusion.11
  (19 shorter events, 0.2 us)
Async XLA Ops:
  0.6 10.5 %collective-permute-start = (bf16[64,3072]{1,0:T(8,128)(2,1)}, bf16[64,3072]{1,0:T(8,128)(2,1)S(1)}, u32[]{:S(2)}, u32[]{:S(2)}) collective-permute-start(bf16[64,3072]{1,0:T(8,128)(2,1)} %param.12), channel_id=1, source_target_pairs={{0,1},{1,0},{2,3},{3,2},{4,5},{5,4},{6,7},{7,6},{8,9},{9,8},{10,11... | collective-permute-start | bytes 1179656 | tf_op jit(solution)/shard_map/ppermute | solution.py:78
  11.1 1.3 %copy-start = (bf16[2048,256]{1,0:T(8,128)(2,1)S(1)}, bf16[2048,256]{1,0:T(8,128)(2,1)}, u32[]{:S(2)}) copy-start(bf16[2048,256]{1,0:T(8,128)(2,1)} %param.17) | copy-start | bytes 3145732
  12.8 30.7 %all-to-all-start = ((bf16[16,96,128]{2,1,0:T(8,128)(2,1)}), bf16[16,96,128]{2,1,0:T(8,128)(2,1)S(1)}, u32[]{:S(2)}, u32[]{:S(2)}) async-start(bf16[16,96,128]{2,1,0:T(8,128)(2,1)} %bitcast.1), calls=%async_computation | async-start | bytes 786432 | tf_op jit(solution)/shard_map/all_to_all | solution.py:20
  23.1 1.0 copy-start.4
  23.1 1.1 copy-start.5
  24.2 1.0 copy-start.1
  24.2 1.8 %copy-start.6 = (f32[128,64]{0,1:T(8,128)S(1)}, f32[128,64]{0,1:T(8,128)}, u32[]{:S(2)}) copy-start(f32[128,64]{0,1:T(8,128)} %param.19) | copy-start | bytes 98308
  24.2 1.8 %copy-start.8 = (f32[128,64]{0,1:T(8,128)S(1)}, f32[128,64]{0,1:T(8,128)}, u32[]{:S(2)}) copy-start(f32[128,64]{0,1:T(8,128)} %param.18) | copy-start | bytes 98308
  28.3 4.1 %collective-permute-start.1 = (bf16[128,1536]{1,0:T(8,128)(2,1)}, bf16[128,1536]{1,0:T(8,128)(2,1)}, u32[]{:S(2)}, u32[]{:S(2)}) collective-permute-start(bf16[128,1536]{1,0:T(8,128)(2,1)} %fusion.6), channel_id=1, source_target_pairs={{0,1},{1,0},{2,3},{3,2},{4,5},{5,4},{6,7},{7,6},{8,9},{9,8},{10,11... | collective-permute-start | bytes 1179656 | tf_op jit(solution)/shard_map/ppermute | solution.py:117
  43.5 33.8 %all-to-all-start.1 = ((f32[16,128,128]{2,1,0:T(8,128)}), f32[16,128,128]{2,1,0:T(8,128)S(1)}, u32[]{:S(2)}, u32[]{:S(2)}) async-start(f32[16,128,128]{2,1,0:T(8,128)} %broadcast_in_dim.8), calls=%async_computation.1 | async-start | bytes 2097152 | tf_op jit(solution)/shard_map/all_to_all | solution.py:20
  50.3 26.0 %copy-start.3 = (bf16[256,1536]{1,0:T(8,128)(2,1)S(1)}, bf16[256,1536]{1,0:T(8,128)(2,1)}, u32[]{:S(2)}) copy-start(bf16[256,1536]{1,0:T(8,128)(2,1)} %pad_maximum_fusion.1) | copy-start | bytes 2359300
  77.1 23.8 %copy-start.10 = (f32[16,64]{1,0:T(8,128)S(1)}, f32[16,64]{1,0:T(8,128)}, u32[]{:S(2)}) copy-start(f32[16,64]{1,0:T(8,128)} %param.23) | copy-start | bytes 12292
  77.1 23.8 %copy-start.11 = (f32[16,64]{1,0:T(8,128)S(1)}, f32[16,64]{1,0:T(8,128)}, u32[]{:S(2)}) copy-start(f32[16,64]{1,0:T(8,128)} %param.21) | copy-start | bytes 12292
  77.1 23.8 %copy-start.12 = (f32[16,64]{1,0:T(8,128)S(1)}, f32[16,64]{1,0:T(8,128)}, u32[]{:S(2)}) copy-start(f32[16,64]{1,0:T(8,128)} %param.22) | copy-start | bytes 12292
  77.1 23.8 %copy-start.13 = (f32[16,64]{1,0:T(8,128)S(1)}, f32[16,64]{1,0:T(8,128)}, u32[]{:S(2)}) copy-start(f32[16,64]{1,0:T(8,128)} %param.20) | copy-start | bytes 12292
  77.2 33.7 %copy-start.2 = (f32[256,256]{1,0:T(8,128)S(1)}, f32[256,256]{1,0:T(8,128)}, u32[]{:S(2)}) copy-start(f32[256,256]{1,0:T(8,128)} %convolution_bitcast_fusion) | copy-start | bytes 786436
  113.3 16.8 %copy-start.7 = (f32[128,64]{0,1:T(8,128)S(1)}, f32[128,64]{0,1:T(8,128)}, u32[]{:S(2)}) copy-start(f32[128,64]{0,1:T(8,128)} %param.19) | copy-start | bytes 98308
  113.3 16.8 %copy-start.9 = (f32[128,64]{0,1:T(8,128)S(1)}, f32[128,64]{0,1:T(8,128)}, u32[]{:S(2)}) copy-start(f32[128,64]{0,1:T(8,128)} %param.18) | copy-start | bytes 98308
  113.4 16.2 %all-to-all-start.4 = ((f32[32,1,128]{2,1,0:T(1,128)}), f32[32,1,128]{2,1,0:T(1,128)S(1)}, u32[]{:S(2)}, u32[]{:S(2)}) async-start(f32[32,1,128]{2,1,0:T(1,128)} %broadcast_in_dim.10), calls=%async_computation.4 | async-start | bytes 32768 | tf_op jit(solution)/shard_map/all_to_all | solution.py:20

commit v8 on v7

--- a/solution.py
+++ b/solution.py
@@ -14,15 +14,16 @@
 LINK_SCALE = 32.0
 FIRST_CHIP = 11
 FIRST_CORE = 1
+FIRST_PLANE = 10
 
 
 def swap(pieces, axes, groups=None):
     return lax.all_to_all(pieces, axes, 0, 0, tiled=True, axis_index_groups=groups)
 
 
-def to_all(shard, axes):
+def to_all(shard, axes, groups):
     size = lax.axis_size(axes)
-    return swap(jnp.broadcast_to(shard[None], (size, *shard.shape)), axes)
+    return swap(jnp.broadcast_to(shard[None], (size, *shard.shape)), axes, groups)
 
 
 def core_order(cores):
@@ -67,7 +68,8 @@
     half = tokens // cores
     rings = [[z * cores + c for z in chip_order(chips)] for c in range(cores)]
     whole = [[z * cores + c for z in chip_order(chips) for c in core_order(cores)]]
-    planes = [[f * cores + c for f in range(fs_size) for c in core_order(cores)]]
+    order = [(FIRST_PLANE + f) % fs_size for f in range(fs_size)]
+    planes = [[f * cores + c for f in order for c in core_order(cores)]]
     share = half // chips
 
     rows_here = lax.axis_index(TP) * width + lax.iota(jnp.int32, width)
@@ -84,12 +86,12 @@
     features = jnp.concatenate([kept, came], axis=0)
 
     by_token = features.T.reshape(chips, share, cores * width)
-    by_token, first_map, second_map, blocks, key_master, value_master = lax.optimization_barrier(
+    by_token, first_map, second_map, factor, key_master, value_master = lax.optimization_barrier(
         (
             by_token,
             first_map,
             second_map,
-            factor.reshape(chips, cores, width, rank),
+            factor,
             key_master,
             value_master,
         )
@@ -104,10 +106,11 @@
     sent = lax.dynamic_slice_in_dim(stacked, (1 - core) * half, half, 1)
     masters_here = jnp.concatenate([key_master.T, value_master.T], axis=0)
     masters = jnp.broadcast_to(masters_here[None], (fs_size, *masters_here.shape))
-    late_factor = blocks.reshape(rows, rank)
+    factor = jnp.roll(factor, -FIRST_PLANE * (rank // fs_size), axis=1)
     gram = lax.dot_general(
-        late_factor, late_factor, (((0,), (0,)), ((), ())), preferred_element_type=jnp.float32
-    )
+        factor, factor, (((0,), (0,)), ((), ())), preferred_element_type=jnp.float32
+    )
+    blocks = factor.reshape(chips, cores, width, rank)
     own_first = jnp.where(core == 0, blocks, blocks[:, ::-1])
     own_first = jnp.roll(own_first, -FIRST_CHIP, axis=0).reshape(rows, rank)
     fs_at = lax.axis_index(FS) * fs_rows
@@ -125,7 +128,7 @@
         preferred_element_type=jnp.float32,
     )
     link = (product * LINK_SCALE).astype(jnp.float16)
-    masters = swap(masters, FS)
+    masters = swap(masters, FS, [order])
     link = lax.all_gather(link, TP, axis=0, tiled=True, axis_index_groups=rings)
 
     high, low = in_bf16_parts(link.astype(jnp.float32), 2)
@@ -143,7 +146,7 @@
     first_new = 0.8 * first + 0.2 * small
     second_new = 0.9 * second + 0.1 * small * small
     direction = first_new / (jnp.sqrt(second_new) + 1e-06)
-    directions = to_all(direction, FS).reshape(rank, 2 * width)
+    directions = to_all(direction, FS, [order]).reshape(rank, 2 * width)
 
     seen = jnp.dot(gram, directions, precision=lax.Precision.HIGHEST)
     squares = jnp.sum(directions * seen, axis=0, keepdims=True)
@@ -157,7 +160,7 @@
         for part in in_bf16_parts(directions, 3)
     )
     raw_here = lax.dynamic_slice_in_dim(raw, fs_at, fs_rows, 1, allow_negative_indices=False)
-    all_masters = masters.transpose(1, 0, 2).reshape(2 * width, rows)
+    all_masters = jnp.roll(masters, FIRST_PLANE, axis=0).transpose(1, 0, 2).reshape(2 * width, rows)
     squares = jnp.sum(squares.reshape(cores * chips, 2, width), axis=(0, 2))
     cells = rows * width * cores * chips
     scales = 0.02 / jnp.sqrt(squares / cells + 0.01)

time: 132 us -> 129 us (0.977)
  blocking collectives: 58.9 us -> 52.7 us
  starting transfers between devices: 39.4 us -> 42.1 us
    all_to_all x2, blocking collectives: 33.3 us -> 27.1 us  [swap(): lax.all_to_all(pieces, axes, 0, 0, tiled=True, axis_index_groups=groups)]
    all_to_all x3, starting transfers between devices: 28.3 us -> 31 us  [swap(): lax.all_to_all(pieces, axes, 0, 0, tiled=True, axis_index_groups=groups)]
where the time goes in v8:
time: 129 us
  blocking collectives  52.7 us (41%)
  starting transfers between devices  42.1 us (33%)
  waiting for transfers between devices  14.7 us (11%)
  local copies, waits for them, and re-layouts  7.32 us (6%)
  other arithmetic  6.94 us (5%)
  matrix products  4.13 us (3%)
    all_to_all x3, starting transfers between devices, swap(): lax.all_to_all(pieces, axes, 0, 0, tiled=True, axis_index_groups=groups)  31 us
    all_to_all x2, blocking collectives, swap(): lax.all_to_all(pieces, axes, 0, 0, tiled=True, axis_index_groups=groups)  27.1 us
    all_gather x1, blocking collectives, local(): link = lax.all_gather(link, TP, axis=0, tiled=True, axis_index_groups=rings)  25.6 us
    all_to_all x3, waiting for transfers between devices, swap(): lax.all_to_all(pieces, axes, 0, 0, tiled=True, axis_index_groups=groups)  13 us
    ppermute x1, starting transfers between devices, local(): came = lax.ppermute(normed, 'tp_1', [(0, 1), (1, 0)])  8.75 us
  transfers between devices with their start and end apart: 5, of which 3 were waited for; matrix products, arithmetic and copies ran while one was open for 7% of the time, Pallas kernels for 0%

profile of v8, /device:TPU:1, one launch (start us, length us, event | category | flops | bytes accessed | tf_op | source)
XLA Modules:
  0.0 128.9 jit_solution(10995016397721588849)
XLA Ops:
  0.6 8.7 %collective-permute-start = (bf16[64,3072]{1,0:T(8,128)(2,1)}, bf16[64,3072]{1,0:T(8,128)(2,1)S(1)}, u32[]{:S(2)}, u32[]{:S(2)}) collective-permute-start(bf16[64,3072]{1,0:T(8,128)(2,1)} %param.12), channel_id=1, source_target_pairs={{0,1},{1,0},{2,3},{3,2},{4,5},{5,4},{6,7},{7,6},{8,9},{9,8},{10,11... | collective-permute-start | bytes 1179656 | tf_op jit(solution)/shard_map/ppermute | solution.py:80
  9.4 0.7 select_reduce_fusion
  10.2 0.9 constant_dynamic-slice_fusion.2
  11.1 0.0 copy-start.1
  11.1 0.0 collective-permute-done
  11.2 0.9 copy.31
  12.1 0.3 copy-done.1
  12.4 0.2 slice.60
  12.6 0.6 pad_maximum_fusion
  13.2 0.3 reverse_select_fusion
  13.5 0.1 slice.79
  13.7 10.3 %all-to-all-start = ((bf16[16,96,128]{2,1,0:T(8,128)(2,1)}), bf16[16,96,128]{2,1,0:T(8,128)(2,1)S(1)}, u32[]{:S(2)}, u32[]{:S(2)}) async-start(bf16[16,96,128]{2,1,0:T(8,128)(2,1)} %bitcast.1), calls=%async_computation | async-start | bytes 786432 | tf_op jit(solution)/shard_map/all_to_all | solution.py:21
  23.9 0.0 copy-start.6
  23.9 0.1 pad_maximum_fusion.1
  24.0 0.9 copy-done.5
  24.9 0.1 copy-done.6
  25.0 0.2 subtract_convert_fusion
  25.2 0.8 copy-done.2
  26.0 0.8 fusion.6
  26.8 0.0 copy-done.9
  26.8 1.2 fusion.22
  28.0 1.1 broadcast_in_dim.8
  29.1 2.4 %collective-permute-start.1 = (bf16[128,1536]{1,0:T(8,128)(2,1)}, bf16[128,1536]{1,0:T(8,128)(2,1)}, u32[]{:S(2)}, u32[]{:S(2)}) collective-permute-start(bf16[128,1536]{1,0:T(8,128)(2,1)} %fusion.6), channel_id=1, source_target_pairs={{0,1},{1,0},{2,3},{3,2},{4,5},{5,4},{6,7},{7,6},{8,9},{9,8},{10,11... | collective-permute-start | bytes 1179656 | tf_op jit(solution)/shard_map/ppermute | solution.py:120
  31.5 1.7 %collective-permute-done.1 = bf16[128,1536]{1,0:T(8,128)(2,1)} collective-permute-done((bf16[128,1536]{1,0:T(8,128)(2,1)}, bf16[128,1536]{1,0:T(8,128)(2,1)}, u32[]{:S(2)}, u32[]{:S(2)}) %collective-permute-start.1) | collective-permute-done | bytes 393248 | tf_op jit(solution)/shard_map/ppermute | solution.py:120
  33.2 1.1 broadcast_select_fusion.1
  34.3 1.0 pad_maximum_fusion.2
  35.3 9.1 %all-to-all-done = bf16[16,96,128]{2,1,0:T(8,128)(2,1)S(1)} async-done(((bf16[16,96,128]{2,1,0:T(8,128)(2,1)}), bf16[16,96,128]{2,1,0:T(8,128)(2,1)S(1)}, u32[]{:S(2)}, u32[]{:S(2)}) %all-to-all-start) | async-done | bytes 393248 | tf_op jit(solution)/shard_map/all_to_all | solution.py:21
  44.3 8.8 %all-to-all-start.1 = ((f32[16,128,128]{2,1,0:T(8,128)}), f32[16,128,128]{2,1,0:T(8,128)S(1)}, u32[]{:S(2)}, u32[]{:S(2)}) async-start(f32[16,128,128]{2,1,0:T(8,128)} %broadcast_in_dim.8), calls=%async_computation.1 | async-start | bytes 2097152 | tf_op jit(solution)/shard_map/all_to_all | solution.py:21
  53.2 0.3 fusion.2
  53.5 25.6 %all_gather.3 = f16[1536,256]{1,0:T(8,128)(2,1)S(1)} all-gather(f16[96,256]{1,0:T(8,128)(2,1)S(1)} %fusion.2), channel_id=1, replica_groups={{22,24,26,28,30,0,2,4,6,8,10,12,14,16,18,20},{23,25,27,29,31,1,3,5,7,9,..., dimensions={0}, use_global_device_ids=true | all-gather | bytes 835584 | tf_op jit(solution)/shard_map/all_gather | solution.py:132
  79.1 0.4 fusion.5
  79.5 0.4 convolution_add_fusion.2
  79.9 0.0 copy-start.11
  80.0 0.0 copy-start.12
  80.0 0.0 copy-start.13
  80.0 0.0 copy-start.14
  80.0 0.0 copy-start.3
  80.0 0.1 reshape.112
  80.2 0.0 all-to-all-done.1
  80.2 17.6 %all_to_all.25 = f32[32,16,128]{2,1,0:T(8,128)S(1)} all-to-all(f32[32,16,128]{2,1,0:T(8,128)S(1)} %bitcast.58), channel_id=1, replica_groups={{321,320,353,352,385,384,417,416,449,448,481,480,1,0,33,32,65,64,97,96,..., dimensions={0} | all-to-all | bytes 524288 | tf_op jit(solution)/shard_map/all_to_all | solution.py:21
  97.9 0.1 add_divide_fusion
  98.0 9.4 %all_to_all.26 = f32[16,16,128]{2,1,0:T(8,128)S(1)} all-to-all(f32[16,16,128]{2,1,0:T(8,128)S(1)} %broadcast_in_dim.9), channel_id=1, replica_groups={{320,352,384,416,448,480,0,32,64,96,128,160,192,224,256,288},{321,353,3..., dimensions={0} | all-to-all | bytes 262144 | tf_op jit(solution)/shard_map/all_to_all | solution.py:21
  107.5 0.4 fusion.3
  107.8 0.6 broadcast_in_dim.10
  108.5 0.5 fusion.15
  108.9 0.5 convolution_add_fusion.1
  109.4 0.0 slice-start
  109.4 0.0 slice-start.1
  109.5 0.5 convolution_add_fusion
  109.9 11.9 %all-to-all-start.4 = ((f32[32,1,128]{2,1,0:T(1,128)}), f32[32,1,128]{2,1,0:T(1,128)S(1)}, u32[]{:S(2)}, u32[]{:S(2)}) async-start(f32[32,1,128]{2,1,0:T(1,128)} %broadcast_in_dim.10), calls=%async_computation.4 | async-start | bytes 32768 | tf_op jit(solution)/shard_map/all_to_all | solution.py:21
  121.8 0.7 fusion.20
  122.5 0.0 slice-done
  122.5 0.0 copy-start.8
  122.5 0.0 copy-start.10
  122.5 0.1 copy_bitcast_fusion
  122.6 0.1 constant_dynamic-slice_fusion
  122.7 4.0 %all-to-all-done.4 = f32[32,1,128]{2,1,0:T(1,128)S(1)} async-done(((f32[32,1,128]{2,1,0:T(1,128)}), f32[32,1,128]{2,1,0:T(1,128)S(1)}, u32[]{:S(2)}, u32[]{:S(2)}) %all-to-all-start.4) | async-done | bytes 16416 | tf_op jit(solution)/shard_map/all_to_all | solution.py:21
  126.7 0.1 reduce_sum.47
  126.8 0.1 reduce_sum.48
  126.9 0.1 broadcast_in_dim.11
  127.0 0.1 broadcast_in_dim_reshape.3
  127.1 0.1 slice_bitcast_fusion
  127.2 0.7 subtract_bitcast_fusion
  127.9 1.0 fusion.11
  (27 shorter events, 0.2 us)
Async XLA Ops:
  0.6 10.5 %collective-permute-start = (bf16[64,3072]{1,0:T(8,128)(2,1)}, bf16[64,3072]{1,0:T(8,128)(2,1)S(1)}, u32[]{:S(2)}, u32[]{:S(2)}) collective-permute-start(bf16[64,3072]{1,0:T(8,128)(2,1)} %param.12), channel_id=1, source_target_pairs={{0,1},{1,0},{2,3},{3,2},{4,5},{5,4},{6,7},{7,6},{8,9},{9,8},{10,11... | collective-permute-start | bytes 1179656 | tf_op jit(solution)/shard_map/ppermute | solution.py:80
  11.1 1.3 %copy-start.1 = (bf16[2048,256]{1,0:T(8,128)(2,1)S(1)}, bf16[2048,256]{1,0:T(8,128)(2,1)}, u32[]{:S(2)}) copy-start(bf16[2048,256]{1,0:T(8,128)(2,1)} %param.17) | copy-start | bytes 3145732
  13.7 30.7 %all-to-all-start = ((bf16[16,96,128]{2,1,0:T(8,128)(2,1)}), bf16[16,96,128]{2,1,0:T(8,128)(2,1)S(1)}, u32[]{:S(2)}, u32[]{:S(2)}) async-start(bf16[16,96,128]{2,1,0:T(8,128)(2,1)} %bitcast.1), calls=%async_computation | async-start | bytes 786432 | tf_op jit(solution)/shard_map/all_to_all | solution.py:21
  23.9 1.0 copy-start.5
  23.9 1.1 copy-start.6
  25.0 1.0 copy-start.2
  25.0 1.8 %copy-start.7 = (f32[128,64]{0,1:T(8,128)S(1)}, f32[128,64]{0,1:T(8,128)}, u32[]{:S(2)}) copy-start(f32[128,64]{0,1:T(8,128)} %param.19) | copy-start | bytes 98308
  25.0 1.8 %copy-start.9 = (f32[128,64]{0,1:T(8,128)S(1)}, f32[128,64]{0,1:T(8,128)}, u32[]{:S(2)}) copy-start(f32[128,64]{0,1:T(8,128)} %param.18) | copy-start | bytes 98308
  29.1 4.1 %collective-permute-start.1 = (bf16[128,1536]{1,0:T(8,128)(2,1)}, bf16[128,1536]{1,0:T(8,128)(2,1)}, u32[]{:S(2)}, u32[]{:S(2)}) collective-permute-start(bf16[128,1536]{1,0:T(8,128)(2,1)} %fusion.6), channel_id=1, source_target_pairs={{0,1},{1,0},{2,3},{3,2},{4,5},{5,4},{6,7},{7,6},{8,9},{9,8},{10,11... | collective-permute-start | bytes 1179656 | tf_op jit(solution)/shard_map/ppermute | solution.py:120
  44.3 35.8 %all-to-all-start.1 = ((f32[16,128,128]{2,1,0:T(8,128)}), f32[16,128,128]{2,1,0:T(8,128)S(1)}, u32[]{:S(2)}, u32[]{:S(2)}) async-start(f32[16,128,128]{2,1,0:T(8,128)} %broadcast_in_dim.8), calls=%async_computation.1 | async-start | bytes 2097152 | tf_op jit(solution)/shard_map/all_to_all | solution.py:21
  53.2 25.9 %copy-start.4 = (bf16[256,1536]{1,0:T(8,128)(2,1)S(1)}, bf16[256,1536]{1,0:T(8,128)(2,1)}, u32[]{:S(2)}) copy-start(bf16[256,1536]{1,0:T(8,128)(2,1)} %pad_maximum_fusion.2) | copy-start | bytes 2359300
  79.9 17.9 %copy-start.11 = (f32[16,64]{1,0:T(8,128)S(1)}, f32[16,64]{1,0:T(8,128)}, u32[]{:S(2)}) copy-start(f32[16,64]{1,0:T(8,128)} %param.23) | copy-start | bytes 12292
  80.0 17.9 %copy-start.12 = (f32[16,64]{1,0:T(8,128)S(1)}, f32[16,64]{1,0:T(8,128)}, u32[]{:S(2)}) copy-start(f32[16,64]{1,0:T(8,128)} %param.21) | copy-start | bytes 12292
  80.0 17.9 %copy-start.13 = (f32[16,64]{1,0:T(8,128)S(1)}, f32[16,64]{1,0:T(8,128)}, u32[]{:S(2)}) copy-start(f32[16,64]{1,0:T(8,128)} %param.22) | copy-start | bytes 12292
  80.0 17.9 %copy-start.14 = (f32[16,64]{1,0:T(8,128)S(1)}, f32[16,64]{1,0:T(8,128)}, u32[]{:S(2)}) copy-start(f32[16,64]{1,0:T(8,128)} %param.20) | copy-start | bytes 12292
  80.0 27.5 %copy-start.3 = (f32[256,256]{1,0:T(8,128)S(1)}, f32[256,256]{1,0:T(8,128)}, u32[]{:S(2)}) copy-start(f32[256,256]{1,0:T(8,128)} %fusion.22) | copy-start | bytes 786436
  80.2 28.3 %copy-start = (f32[16,128,128]{2,1,0:T(8,128)}, f32[16,128,128]{2,1,0:T(8,128)S(1)}, u32[]{:S(2)}) copy-start(f32[16,128,128]{2,1,0:T(8,128)S(1)} %all-to-all-done.1) | copy-start | bytes 3145732
  109.4 13.1 %slice-start = ((f32[16,128,128]{2,1,0:T(8,128)}), f32[10,128,128]{2,1,0:T(8,128)S(1)}, s32[]{:S(2)}) async-start(f32[16,128,128]{2,1,0:T(8,128)} %copy-done), calls=%async_computation.5 | async-start | bytes 1310720 | tf_op jit(solution)/shard_map/jit(_roll_static)/slice | solution.py:163
  109.4 13.1 %slice-start.1 = ((f32[16,128,128]{2,1,0:T(8,128)}), f32[6,128,128]{2,1,0:T(8,128)S(1)}, s32[]{:S(2)}) async-start(f32[16,128,128]{2,1,0:T(8,128)} %copy-done), calls=%async_computation.6 | async-start | bytes 786432 | tf_op jit(solution)/shard_map/jit(_roll_static)/slice | solution.py:163
  109.9 16.8 %all-to-all-start.4 = ((f32[32,1,128]{2,1,0:T(1,128)}), f32[32,1,128]{2,1,0:T(1,128)S(1)}, u32[]{:S(2)}, u32[]{:S(2)}) async-start(f32[32,1,128]{2,1,0:T(1,128)} %broadcast_in_dim.10), calls=%async_computation.4 | async-start | bytes 32768 | tf_op jit(solution)/shard_map/all_to_all | solution.py:21
  122.5 4.7 %copy-start.8 = (f32[128,64]{0,1:T(8,128)S(1)}, f32[128,64]{0,1:T(8,128)}, u32[]{:S(2)}) copy-start(f32[128,64]{0,1:T(8,128)} %param.19) | copy-start | bytes 98308
  122.5 4.6 %copy-start.10 = (f32[128,64]{0,1:T(8,128)S(1)}, f32[128,64]{0,1:T(8,128)}, u32[]{:S(2)}) copy-start(f32[128,64]{0,1:T(8,128)} %param.18) | copy-start | bytes 98308

commit v9 on v8

--- a/solution.py
+++ b/solution.py
@@ -12,7 +12,8 @@
 FS = ("fs_0", "fs_1")
 FS_CORE = ("fs_0", "fs_1", "tp_1")
 LINK_SCALE = 32.0
-FIRST_CHIP = 11
+FIRST_CHIP = 12
+GATHER_CHIP = 0
 FIRST_CORE = 1
 FIRST_PLANE = 10
 
@@ -30,8 +31,8 @@
     return [(FIRST_CORE + c) % cores for c in range(cores)]
 
 
-def chip_order(chips):
-    return [(FIRST_CHIP + z) % chips for z in range(chips)]
+def rings_from(first, chips, cores):
+    return [[(first + z) % chips * cores + c for z in range(chips)] for c in range(cores)]
 
 
 def in_bf16_parts(values, count):
@@ -66,16 +67,13 @@
     heads = lambdas.shape[0]
     fs_rows = key_master.shape[0]
     half = tokens // cores
-    rings = [[z * cores + c for z in chip_order(chips)] for c in range(cores)]
-    whole = [[z * cores + c for z in chip_order(chips) for c in core_order(cores)]]
+    rings = rings_from(FIRST_CHIP, chips, cores)
+    gather_rings = rings_from(GATHER_CHIP, chips, cores)
+    whole = [[rings[c][z] for z in range(chips) for c in core_order(cores)]]
     order = [(FIRST_PLANE + f) % fs_size for f in range(fs_size)]
     planes = [[f * cores + c for f in order for c in core_order(cores)]]
     share = half // chips
 
-    rows_here = lax.axis_index(TP) * width + lax.iota(jnp.int32, width)
-    owners = rows_here // VALUE_DIM
-    picked = (owners[:, None] == lax.iota(jnp.int32, heads)[None, :]).astype(jnp.float32)
-    row_lambda = jnp.sum(picked * lambdas[None, :], axis=1)
     core = lax.axis_index("tp_1")
     came = lax.ppermute(normed, "tp_1", [(0, 1), (1, 0)])
     came = with_layout_constraint(came, Layout(major_to_minor=(0, 1)))
@@ -86,18 +84,23 @@
     features = jnp.concatenate([kept, came], axis=0)
 
     by_token = features.T.reshape(chips, share, cores * width)
-    by_token, first_map, second_map, factor, key_master, value_master = lax.optimization_barrier(
-        (
+    by_token, lambdas, first_map, second_map, factor, key_master, value_master = (
+        lax.optimization_barrier((
             by_token,
+            lambdas,
             first_map,
             second_map,
             factor,
             key_master,
             value_master,
-        )
+        ))
     )
     by_token = swap(by_token, TP, rings)
 
+    rows_here = lax.axis_index(TP) * width + lax.iota(jnp.int32, width)
+    owners = rows_here // VALUE_DIM
+    picked = (owners[:, None] == lax.iota(jnp.int32, heads)[None, :]).astype(jnp.float32)
+    row_lambda = jnp.sum(picked * lambdas[None, :], axis=1)
     value_cot = (
         first_map.astype(jnp.float32) - row_lambda[:, None] * second_map.astype(jnp.float32)
     ).astype(jnp.bfloat16)
@@ -120,6 +123,7 @@
     came = lax.ppermute(sent, "tp_1", [(0, 1), (1, 0)])
     is_first = core == FIRST_CORE
     cots = jnp.concatenate([jnp.where(is_first, kept, came), jnp.where(is_first, came, kept)])
+    cots = jnp.roll(cots, (FIRST_CHIP - GATHER_CHIP) % chips * share - half, axis=1)
     cots, masters, by_token = lax.optimization_barrier((cots, masters, by_token))
     product = lax.dot_general(
         by_token.transpose(1, 0, 2).reshape(share, rows),
@@ -129,7 +133,7 @@
     )
     link = (product * LINK_SCALE).astype(jnp.float16)
     masters = swap(masters, FS, [order])
-    link = lax.all_gather(link, TP, axis=0, tiled=True, axis_index_groups=rings)
+    link = lax.all_gather(link, TP, axis=0, tiled=True, axis_index_groups=gather_rings)
 
     high, low = in_bf16_parts(link.astype(jnp.float32), 2)
     dims = (((0,), (1,)), ((), ()))

time: 129 us -> 131 us (1.016)
  blocking collectives: 52.7 us -> 55.2 us
  waiting for transfers between devices: 14.7 us -> 16.3 us
    all_to_all x3, starting transfers between devices: 31 us -> 29.2 us  [swap(): lax.all_to_all(pieces, axes, 0, 0, tiled=True, axis_index_groups=groups)]
    all_to_all x2, blocking collectives: 27.1 us -> 28.7 us  [swap(): lax.all_to_all(pieces, axes, 0, 0, tiled=True, axis_index_groups=groups)]
  transfers between devices with their start and end apart: 5 -> 5, of which waited for: 3 -> 4; matrix products, arithmetic and copies ran while one was open for 7% -> 7% of each run, Pallas kernels for 0% -> 0%
where the time goes in v9:
time: 131 us
  blocking collectives  55.2 us (42%)
  starting transfers between devices  40.8 us (31%)
  waiting for transfers between devices  16.3 us (12%)
  local copies, waits for them, and re-layouts  7.04 us (5%)
  other arithmetic  6.3 us (5%)
  matrix products  4.14 us (3%)
    all_to_all x3, starting transfers between devices, swap(): lax.all_to_all(pieces, axes, 0, 0, tiled=True, axis_index_groups=groups)  29.2 us
    all_to_all x2, blocking collectives, swap(): lax.all_to_all(pieces, axes, 0, 0, tiled=True, axis_index_groups=groups)  28.7 us
    all_gather x1, blocking collectives, local(): lax.all_gather(link, TP, axis=0, tiled=True, axis_index_groups=gather_rings)  26.5 us
    all_to_all x3, waiting for transfers between devices, swap(): lax.all_to_all(pieces, axes, 0, 0, tiled=True, axis_index_groups=groups)  14.1 us
    ppermute x1, starting transfers between devices, local(): came = lax.ppermute(normed, 'tp_1', [(0, 1), (1, 0)])  8.75 us
    ppermute x1, starting transfers between devices, local(): came = lax.ppermute(sent, 'tp_1', [(0, 1), (1, 0)])  2.83 us
  transfers between devices with their start and end apart: 5, of which 4 were waited for; matrix products, arithmetic and copies ran while one was open for 7% of the time, Pallas kernels for 0%

profile of v9, /device:TPU:1, one launch (start us, length us, event | category | flops | bytes accessed | tf_op | source)
XLA Modules:
  0.0 130.7 jit_solution(18230024697244699431)
XLA Ops:
  0.6 8.7 %collective-permute-start = (bf16[64,3072]{1,0:T(8,128)(2,1)}, bf16[64,3072]{1,0:T(8,128)(2,1)S(1)}, u32[]{:S(2)}, u32[]{:S(2)}) collective-permute-start(bf16[64,3072]{1,0:T(8,128)(2,1)} %param.12), channel_id=1, source_target_pairs={{0,1},{1,0},{2,3},{3,2},{4,5},{5,4},{6,7},{7,6},{8,9},{9,8},{10,11... | collective-permute-start | bytes 1179656 | tf_op jit(solution)/shard_map/ppermute | solution.py:78
  9.4 0.9 constant_dynamic-slice_fusion.2
  10.4 0.0 copy-start.1
  10.4 0.5 collective-permute-done
  11.0 0.9 copy.31
  11.9 0.2 slice.68
  12.1 0.6 pad_maximum_fusion
  12.7 1.2 fusion.24
  13.9 0.3 reverse_select_fusion
  14.2 0.0 copy-start.15
  14.2 0.1 slice.89
  14.3 9.8 %all-to-all-start = ((bf16[16,96,128]{2,1,0:T(8,128)(2,1)}), bf16[16,96,128]{2,1,0:T(8,128)(2,1)S(1)}, u32[]{:S(2)}, u32[]{:S(2)}) async-start(bf16[16,96,128]{2,1,0:T(8,128)(2,1)} %bitcast.1), calls=%async_computation | async-start | bytes 786432 | tf_op jit(solution)/shard_map/all_to_all | solution.py:22
  24.1 0.1 select_reduce_fusion
  24.2 0.1 pad_maximum_fusion.1
  24.3 0.9 copy-done.5
  25.2 0.1 copy-done.6
  25.3 0.2 subtract_convert_fusion
  25.5 0.8 copy-done.2
  26.3 0.8 fusion.8
  27.1 0.0 copy-done.9
  27.1 1.1 broadcast_in_dim.8
  28.2 2.8 %collective-permute-start.1 = (bf16[128,1536]{1,0:T(8,128)(2,1)}, bf16[128,1536]{1,0:T(8,128)(2,1)}, u32[]{:S(2)}, u32[]{:S(2)}) collective-permute-start(bf16[128,1536]{1,0:T(8,128)(2,1)} %fusion.8), channel_id=1, source_target_pairs={{0,1},{1,0},{2,3},{3,2},{4,5},{5,4},{6,7},{7,6},{8,9},{9,8},{10,11... | collective-permute-start | bytes 1179656 | tf_op jit(solution)/shard_map/ppermute | solution.py:123
  31.0 1.7 %collective-permute-done.1 = bf16[128,1536]{1,0:T(8,128)(2,1)} collective-permute-done((bf16[128,1536]{1,0:T(8,128)(2,1)}, bf16[128,1536]{1,0:T(8,128)(2,1)}, u32[]{:S(2)}, u32[]{:S(2)}) %collective-permute-start.1) | collective-permute-done | bytes 393248 | tf_op jit(solution)/shard_map/ppermute | solution.py:123
  32.7 1.1 broadcast_select_fusion.1
  33.9 1.0 fusion.6
  34.8 9.5 %all-to-all-done = bf16[16,96,128]{2,1,0:T(8,128)(2,1)S(1)} async-done(((bf16[16,96,128]{2,1,0:T(8,128)(2,1)}), bf16[16,96,128]{2,1,0:T(8,128)(2,1)S(1)}, u32[]{:S(2)}, u32[]{:S(2)}) %all-to-all-start) | async-done | bytes 393248 | tf_op jit(solution)/shard_map/all_to_all | solution.py:22
  44.3 8.8 %all-to-all-start.1 = ((f32[16,128,128]{2,1,0:T(8,128)}), f32[16,128,128]{2,1,0:T(8,128)S(1)}, u32[]{:S(2)}, u32[]{:S(2)}) async-start(f32[16,128,128]{2,1,0:T(8,128)} %broadcast_in_dim.8), calls=%async_computation.1 | async-start | bytes 2097152 | tf_op jit(solution)/shard_map/all_to_all | solution.py:22
  53.2 0.3 fusion.2
  53.5 26.5 %all_gather.3 = f16[1536,256]{1,0:T(8,128)(2,1)S(1)} all-gather(f16[96,256]{1,0:T(8,128)(2,1)S(1)} %fusion.2), channel_id=1, replica_groups={{0,2,4,6,8,10,12,14,16,18,20,22,24,26,28,30},{1,3,5,7,9,11,13,15,17,19,..., dimensions={0}, use_global_device_ids=true | all-gather | bytes 835584 | tf_op jit(solution)/shard_map/all_gather | solution.py:136
  80.0 0.0 copy-done.4
  80.0 0.4 fusion.5
  80.4 0.4 convolution_add_fusion.2
  80.8 0.0 copy-start.11
  80.8 0.0 copy-start.12
  80.9 0.0 copy-start.13
  80.9 0.0 copy-start.14
  80.9 0.0 copy-start.3
  80.9 0.1 reshape.112
  81.1 0.0 all-to-all-done.1
  81.1 19.3 %all_to_all.25 = f32[32,16,128]{2,1,0:T(8,128)S(1)} all-to-all(f32[32,16,128]{2,1,0:T(8,128)S(1)} %bitcast.58), channel_id=1, replica_groups={{321,320,353,352,385,384,417,416,449,448,481,480,1,0,33,32,65,64,97,96,..., dimensions={0} | all-to-all | bytes 524288 | tf_op jit(solution)/shard_map/all_to_all | solution.py:22
  100.4 0.0 copy-done.11
  100.4 0.0 copy-done.12
  100.4 0.1 add_divide_fusion
  100.5 9.4 %all_to_all.26 = f32[16,16,128]{2,1,0:T(8,128)S(1)} all-to-all(f32[16,16,128]{2,1,0:T(8,128)S(1)} %broadcast_in_dim.9), channel_id=1, replica_groups={{320,352,384,416,448,480,0,32,64,96,128,160,192,224,256,288},{321,353,3..., dimensions={0} | all-to-all | bytes 262144 | tf_op jit(solution)/shard_map/all_to_all | solution.py:22
  110.0 0.4 fusion.3
  110.4 0.6 broadcast_in_dim.10
  111.0 10.6 %all-to-all-start.4 = ((f32[32,1,128]{2,1,0:T(1,128)}), f32[32,1,128]{2,1,0:T(1,128)S(1)}, u32[]{:S(2)}, u32[]{:S(2)}) async-start(f32[32,1,128]{2,1,0:T(1,128)} %broadcast_in_dim.10), calls=%async_computation.4 | async-start | bytes 32768 | tf_op jit(solution)/shard_map/all_to_all | solution.py:22
  121.6 0.5 fusion.17
  122.1 0.5 convolution_add_fusion.1
  122.6 0.0 slice-start
  122.6 0.0 slice-start.1
  122.6 0.5 convolution_add_fusion
  123.1 0.7 fusion.22
  123.8 0.0 slice-done.1
  123.8 0.1 copy_bitcast_fusion
  123.9 0.1 constant_dynamic-slice_fusion
  124.0 4.6 %all-to-all-done.4 = f32[32,1,128]{2,1,0:T(1,128)S(1)} async-done(((f32[32,1,128]{2,1,0:T(1,128)}), f32[32,1,128]{2,1,0:T(1,128)S(1)}, u32[]{:S(2)}, u32[]{:S(2)}) %all-to-all-start.4) | async-done | bytes 16416 | tf_op jit(solution)/shard_map/all_to_all | solution.py:22
  128.6 0.1 reduce_sum.47
  128.7 0.1 reduce_sum.48
  128.8 0.1 broadcast_in_dim.11
  128.9 0.1 broadcast_in_dim_reshape.3
  129.0 0.1 slice_bitcast_fusion
  129.1 0.7 subtract_bitcast_fusion
  129.8 1.0 fusion.13
  (30 shorter events, 0.3 us)
Async XLA Ops:
  0.6 10.3 %collective-permute-start = (bf16[64,3072]{1,0:T(8,128)(2,1)}, bf16[64,3072]{1,0:T(8,128)(2,1)S(1)}, u32[]{:S(2)}, u32[]{:S(2)}) collective-permute-start(bf16[64,3072]{1,0:T(8,128)(2,1)} %param.12), channel_id=1, source_target_pairs={{0,1},{1,0},{2,3},{3,2},{4,5},{5,4},{6,7},{7,6},{8,9},{9,8},{10,11... | collective-permute-start | bytes 1179656 | tf_op jit(solution)/shard_map/ppermute | solution.py:78
  10.4 1.5 %copy-start.1 = (bf16[2048,256]{1,0:T(8,128)(2,1)S(1)}, bf16[2048,256]{1,0:T(8,128)(2,1)}, u32[]{:S(2)}) copy-start(bf16[2048,256]{1,0:T(8,128)(2,1)} %param.17) | copy-start | bytes 3145732
  14.2 9.9 %copy-start.15 = (f32[8]{0:T(128)S(1)}, f32[8]{0:T(128)}, u32[]{:S(2)}) copy-start(f32[8]{0:T(128)} %param.16) | copy-start | bytes 100
  14.3 30.0 %all-to-all-start = ((bf16[16,96,128]{2,1,0:T(8,128)(2,1)}), bf16[16,96,128]{2,1,0:T(8,128)(2,1)S(1)}, u32[]{:S(2)}, u32[]{:S(2)}) async-start(bf16[16,96,128]{2,1,0:T(8,128)(2,1)} %bitcast.1), calls=%async_computation | async-start | bytes 786432 | tf_op jit(solution)/shard_map/all_to_all | solution.py:22
  24.2 1.0 copy-start.5
  24.2 1.1 copy-start.6
  25.3 1.0 copy-start.2
  25.3 1.8 %copy-start.7 = (f32[128,64]{0,1:T(8,128)S(1)}, f32[128,64]{0,1:T(8,128)}, u32[]{:S(2)}) copy-start(f32[128,64]{0,1:T(8,128)} %param.19) | copy-start | bytes 98308
  25.3 1.8 %copy-start.9 = (f32[128,64]{0,1:T(8,128)S(1)}, f32[128,64]{0,1:T(8,128)}, u32[]{:S(2)}) copy-start(f32[128,64]{0,1:T(8,128)} %param.18) | copy-start | bytes 98308
  28.2 4.5 %collective-permute-start.1 = (bf16[128,1536]{1,0:T(8,128)(2,1)}, bf16[128,1536]{1,0:T(8,128)(2,1)}, u32[]{:S(2)}, u32[]{:S(2)}) collective-permute-start(bf16[128,1536]{1,0:T(8,128)(2,1)} %fusion.8), channel_id=1, source_target_pairs={{0,1},{1,0},{2,3},{3,2},{4,5},{5,4},{6,7},{7,6},{8,9},{9,8},{10,11... | collective-permute-start | bytes 1179656 | tf_op jit(solution)/shard_map/ppermute | solution.py:123
  44.3 36.7 %all-to-all-start.1 = ((f32[16,128,128]{2,1,0:T(8,128)}), f32[16,128,128]{2,1,0:T(8,128)S(1)}, u32[]{:S(2)}, u32[]{:S(2)}) async-start(f32[16,128,128]{2,1,0:T(8,128)} %broadcast_in_dim.8), calls=%async_computation.1 | async-start | bytes 2097152 | tf_op jit(solution)/shard_map/all_to_all | solution.py:22
  53.2 26.8 %copy-start.4 = (bf16[256,1536]{1,0:T(8,128)(2,1)S(1)}, bf16[256,1536]{1,0:T(8,128)(2,1)}, u32[]{:S(2)}) copy-start(bf16[256,1536]{1,0:T(8,128)(2,1)} %fusion.6) | copy-start | bytes 2359300
  80.8 19.6 %copy-start.11 = (f32[16,64]{1,0:T(8,128)S(1)}, f32[16,64]{1,0:T(8,128)}, u32[]{:S(2)}) copy-start(f32[16,64]{1,0:T(8,128)} %param.23) | copy-start | bytes 12292
  80.8 19.6 %copy-start.12 = (f32[16,64]{1,0:T(8,128)S(1)}, f32[16,64]{1,0:T(8,128)}, u32[]{:S(2)}) copy-start(f32[16,64]{1,0:T(8,128)} %param.21) | copy-start | bytes 12292
  80.9 19.6 %copy-start.13 = (f32[16,64]{1,0:T(8,128)S(1)}, f32[16,64]{1,0:T(8,128)}, u32[]{:S(2)}) copy-start(f32[16,64]{1,0:T(8,128)} %param.22) | copy-start | bytes 12292
  80.9 19.6 %copy-start.14 = (f32[16,64]{1,0:T(8,128)S(1)}, f32[16,64]{1,0:T(8,128)}, u32[]{:S(2)}) copy-start(f32[16,64]{1,0:T(8,128)} %param.20) | copy-start | bytes 12292
  80.9 29.1 %copy-start.3 = (f32[256,256]{1,0:T(8,128)S(1)}, f32[256,256]{1,0:T(8,128)}, u32[]{:S(2)}) copy-start(f32[256,256]{1,0:T(8,128)} %fusion.24) | copy-start | bytes 786436
  81.1 29.9 %copy-start = (f32[16,128,128]{2,1,0:T(8,128)}, f32[16,128,128]{2,1,0:T(8,128)S(1)}, u32[]{:S(2)}) copy-start(f32[16,128,128]{2,1,0:T(8,128)S(1)} %all-to-all-done.1) | copy-start | bytes 3145732
  111.0 17.6 %all-to-all-start.4 = ((f32[32,1,128]{2,1,0:T(1,128)}), f32[32,1,128]{2,1,0:T(1,128)S(1)}, u32[]{:S(2)}, u32[]{:S(2)}) async-start(f32[32,1,128]{2,1,0:T(1,128)} %broadcast_in_dim.10), calls=%async_computation.4 | async-start | bytes 32768 | tf_op jit(solution)/shard_map/all_to_all | solution.py:22
  122.6 1.2 slice-start
  122.6 1.2 slice-start.1
  123.8 5.2 %copy-start.8 = (f32[128,64]{0,1:T(8,128)S(1)}, f32[128,64]{0,1:T(8,128)}, u32[]{:S(2)}) copy-start(f32[128,64]{0,1:T(8,128)} %param.19) | copy-start | bytes 98308
  123.8 5.2 %copy-start.10 = (f32[128,64]{0,1:T(8,128)S(1)}, f32[128,64]{0,1:T(8,128)}, u32[]{:S(2)}) copy-start(f32[128,64]{0,1:T(8,128)} %param.18) | copy-start | bytes 98308

commit v10 on v9

--- a/solution.py
+++ b/solution.py
@@ -12,8 +12,7 @@
 FS = ("fs_0", "fs_1")
 FS_CORE = ("fs_0", "fs_1", "tp_1")
 LINK_SCALE = 32.0
-FIRST_CHIP = 12
-GATHER_CHIP = 0
+FIRST_CHIP = 9
 FIRST_CORE = 1
 FIRST_PLANE = 10
 
@@ -68,7 +67,6 @@
     fs_rows = key_master.shape[0]
     half = tokens // cores
     rings = rings_from(FIRST_CHIP, chips, cores)
-    gather_rings = rings_from(GATHER_CHIP, chips, cores)
     whole = [[rings[c][z] for z in range(chips) for c in core_order(cores)]]
     order = [(FIRST_PLANE + f) % fs_size for f in range(fs_size)]
     planes = [[f * cores + c for f in order for c in core_order(cores)]]
@@ -123,7 +121,6 @@
     came = lax.ppermute(sent, "tp_1", [(0, 1), (1, 0)])
     is_first = core == FIRST_CORE
     cots = jnp.concatenate([jnp.where(is_first, kept, came), jnp.where(is_first, came, kept)])
-    cots = jnp.roll(cots, (FIRST_CHIP - GATHER_CHIP) % chips * share - half, axis=1)
     cots, masters, by_token = lax.optimization_barrier((cots, masters, by_token))
     product = lax.dot_general(
         by_token.transpose(1, 0, 2).reshape(share, rows),
@@ -133,7 +130,7 @@
     )
     link = (product * LINK_SCALE).astype(jnp.float16)
     masters = swap(masters, FS, [order])
-    link = lax.all_gather(link, TP, axis=0, tiled=True, axis_index_groups=gather_rings)
+    link = lax.all_gather(link, TP, axis=0, tiled=True, axis_index_groups=rings)
 
     high, low = in_bf16_parts(link.astype(jnp.float32), 2)
     dims = (((0,), (1,)), ((), ()))

time: 131 us -> 129 us (0.985)
  starting transfers between devices: 40.8 us -> 45.1 us
  waiting for transfers between devices: 16.3 us -> 12.3 us
  blocking collectives: 55.2 us -> 53.3 us
    all_to_all x3, starting transfers between devices: 29.2 us -> 33.5 us  [swap(): lax.all_to_all(pieces, axes, 0, 0, tiled=True, axis_index_groups=groups)]
    all_to_all x3, waiting for transfers between devices: 14.1 us -> 10.1 us  [swap(): lax.all_to_all(pieces, axes, 0, 0, tiled=True, axis_index_groups=groups)]
where the time goes in v10:
time: 129 us
  blocking collectives  53.3 us (41%)
  starting transfers between devices  45.1 us (35%)
  waiting for transfers between devices  12.3 us (10%)
  local copies, waits for them, and re-layouts  6.5 us (5%)
  other arithmetic  6.26 us (5%)
  matrix products  4.13 us (3%)
    all_to_all x3, starting transfers between devices, swap(): lax.all_to_all(pieces, axes, 0, 0, tiled=True, axis_index_groups=groups)  33.5 us
    all_to_all x2, blocking collectives, swap(): lax.all_to_all(pieces, axes, 0, 0, tiled=True, axis_index_groups=groups)  27.5 us
    all_gather x1, blocking collectives, local(): link = lax.all_gather(link, TP, axis=0, tiled=True, axis_index_groups=rings)  25.8 us
    all_to_all x3, waiting for transfers between devices, swap(): lax.all_to_all(pieces, axes, 0, 0, tiled=True, axis_index_groups=groups)  10.1 us
    ppermute x1, starting transfers between devices, local(): came = lax.ppermute(normed, 'tp_1', [(0, 1), (1, 0)])  8.75 us
    ppermute x1, starting transfers between devices, local(): came = lax.ppermute(sent, 'tp_1', [(0, 1), (1, 0)])  2.83 us
  transfers between devices with their start and end apart: 5, of which 4 were waited for; matrix products, arithmetic and copies ran while one was open for 7% of the time, Pallas kernels for 0%

profile of v10, /device:TPU:1, one launch (start us, length us, event | category | flops | bytes accessed | tf_op | source)
XLA Modules:
  0.0 128.5 jit_solution(17620201107097701682)
XLA Ops:
  0.6 8.7 %collective-permute-start = (bf16[64,3072]{1,0:T(8,128)(2,1)}, bf16[64,3072]{1,0:T(8,128)(2,1)S(1)}, u32[]{:S(2)}, u32[]{:S(2)}) collective-permute-start(bf16[64,3072]{1,0:T(8,128)(2,1)} %param.12), channel_id=1, source_target_pairs={{0,1},{1,0},{2,3},{3,2},{4,5},{5,4},{6,7},{7,6},{8,9},{9,8},{10,11... | collective-permute-start | bytes 1179656 | tf_op jit(solution)/shard_map/ppermute | solution.py:76
  9.4 0.9 constant_dynamic-slice_fusion.2
  10.4 0.0 copy-start.1
  10.4 0.5 collective-permute-done
  11.0 0.9 copy.31
  11.9 0.2 slice.60
  12.1 0.6 pad_maximum_fusion
  12.7 0.3 reverse_select_fusion
  13.1 12.1 %all-to-all-start = ((bf16[16,96,128]{2,1,0:T(8,128)(2,1)}), bf16[16,96,128]{2,1,0:T(8,128)(2,1)S(1)}, u32[]{:S(2)}, u32[]{:S(2)}) async-start(bf16[16,96,128]{2,1,0:T(8,128)(2,1)} %bitcast.1), calls=%async_computation | async-start | bytes 786432 | tf_op jit(solution)/shard_map/all_to_all | solution.py:21
  25.2 0.0 copy-start.5
  25.2 0.0 copy-start.6
  25.2 0.1 pad_maximum_fusion.1
  25.3 0.5 copy-done.15
  25.8 0.1 select_reduce_fusion
  25.9 0.3 copy-done.5
  26.2 0.1 copy-done.6
  26.3 0.2 subtract_convert_fusion
  26.5 0.4 copy-done.2
  26.9 0.8 fusion.6
  27.7 1.2 fusion.22
  28.9 1.1 broadcast_in_dim.8
  29.9 2.8 %collective-permute-start.1 = (bf16[128,1536]{1,0:T(8,128)(2,1)}, bf16[128,1536]{1,0:T(8,128)(2,1)}, u32[]{:S(2)}, u32[]{:S(2)}) collective-permute-start(bf16[128,1536]{1,0:T(8,128)(2,1)} %fusion.6), channel_id=1, source_target_pairs={{0,1},{1,0},{2,3},{3,2},{4,5},{5,4},{6,7},{7,6},{8,9},{9,8},{10,11... | collective-permute-start | bytes 1179656 | tf_op jit(solution)/shard_map/ppermute | solution.py:121
  32.8 1.7 %collective-permute-done.1 = bf16[128,1536]{1,0:T(8,128)(2,1)} collective-permute-done((bf16[128,1536]{1,0:T(8,128)(2,1)}, bf16[128,1536]{1,0:T(8,128)(2,1)}, u32[]{:S(2)}, u32[]{:S(2)}) %collective-permute-start.1) | collective-permute-done | bytes 393248 | tf_op jit(solution)/shard_map/ppermute | solution.py:121
  34.4 1.1 broadcast_select_fusion.1
  35.6 1.0 pad_maximum_fusion.2
  36.6 7.9 %all-to-all-done = bf16[16,96,128]{2,1,0:T(8,128)(2,1)S(1)} async-done(((bf16[16,96,128]{2,1,0:T(8,128)(2,1)}), bf16[16,96,128]{2,1,0:T(8,128)(2,1)S(1)}, u32[]{:S(2)}, u32[]{:S(2)}) %all-to-all-start) | async-done | bytes 393248 | tf_op jit(solution)/shard_map/all_to_all | solution.py:21
  44.5 8.8 %all-to-all-start.1 = ((f32[16,128,128]{2,1,0:T(8,128)}), f32[16,128,128]{2,1,0:T(8,128)S(1)}, u32[]{:S(2)}, u32[]{:S(2)}) async-start(f32[16,128,128]{2,1,0:T(8,128)} %broadcast_in_dim.8), calls=%async_computation.1 | async-start | bytes 2097152 | tf_op jit(solution)/shard_map/all_to_all | solution.py:21
  53.3 0.3 fusion.2
  53.7 25.8 %all_gather.3 = f16[1536,256]{1,0:T(8,128)(2,1)S(1)} all-gather(f16[96,256]{1,0:T(8,128)(2,1)S(1)} %fusion.2), channel_id=1, replica_groups={{18,20,22,24,26,28,30,0,2,4,6,8,10,12,14,16},{19,21,23,25,27,29,31,1,3,..., dimensions={0}, use_global_device_ids=true | all-gather | bytes 835584 | tf_op jit(solution)/shard_map/all_gather | solution.py:133
  79.4 0.0 copy-done.4
  79.4 0.4 fusion.5
  79.8 0.4 convolution_add_fusion.2
  80.3 0.0 copy-start.11
  80.3 0.0 copy-start.12
  80.3 0.0 copy-start.13
  80.3 0.0 copy-start.14
  80.3 0.0 copy-start.3
  80.3 0.1 reshape.112
  80.5 0.0 all-to-all-done.1
  80.5 0.0 copy-start
  80.5 18.1 %all_to_all.25 = f32[32,16,128]{2,1,0:T(8,128)S(1)} all-to-all(f32[32,16,128]{2,1,0:T(8,128)S(1)} %bitcast.58), channel_id=1, replica_groups={{321,320,353,352,385,384,417,416,449,448,481,480,1,0,33,32,65,64,97,96,..., dimensions={0} | all-to-all | bytes 524288 | tf_op jit(solution)/shard_map/all_to_all | solution.py:21
  98.7 0.1 add_divide_fusion
  98.8 9.4 %all_to_all.26 = f32[16,16,128]{2,1,0:T(8,128)S(1)} all-to-all(f32[16,16,128]{2,1,0:T(8,128)S(1)} %broadcast_in_dim.9), channel_id=1, replica_groups={{320,352,384,416,448,480,0,32,64,96,128,160,192,224,256,288},{321,353,3..., dimensions={0} | all-to-all | bytes 262144 | tf_op jit(solution)/shard_map/all_to_all | solution.py:21
  108.2 0.4 fusion.3
  108.6 0.6 broadcast_in_dim.10
  109.2 0.5 fusion.15
  109.7 0.5 convolution_add_fusion.1
  110.2 0.0 slice-start
  110.2 0.0 slice-start.1
  110.2 0.5 convolution_add_fusion
  110.7 12.6 %all-to-all-start.4 = ((f32[32,1,128]{2,1,0:T(1,128)}), f32[32,1,128]{2,1,0:T(1,128)S(1)}, u32[]{:S(2)}, u32[]{:S(2)}) async-start(f32[32,1,128]{2,1,0:T(1,128)} %broadcast_in_dim.10), calls=%async_computation.4 | async-start | bytes 32768 | tf_op jit(solution)/shard_map/all_to_all | solution.py:21
  123.3 0.7 fusion.20
  124.0 0.0 copy-start.8
  124.0 0.0 copy-start.10
  124.0 0.1 copy_bitcast_fusion
  124.1 0.1 constant_dynamic-slice_fusion
  124.2 2.1 %all-to-all-done.4 = f32[32,1,128]{2,1,0:T(1,128)S(1)} async-done(((f32[32,1,128]{2,1,0:T(1,128)}), f32[32,1,128]{2,1,0:T(1,128)S(1)}, u32[]{:S(2)}, u32[]{:S(2)}) %all-to-all-start.4) | async-done | bytes 16416 | tf_op jit(solution)/shard_map/all_to_all | solution.py:21
  126.4 0.1 reduce_sum.47
  126.5 0.1 reduce_sum.48
  126.6 0.1 broadcast_in_dim.11
  126.7 0.1 broadcast_in_dim_reshape.3
  126.7 0.1 slice_bitcast_fusion
  126.8 0.7 subtract_bitcast_fusion
  127.5 1.0 fusion.11
  (29 shorter events, 0.3 us)
Async XLA Ops:
  0.6 10.3 %collective-permute-start = (bf16[64,3072]{1,0:T(8,128)(2,1)}, bf16[64,3072]{1,0:T(8,128)(2,1)S(1)}, u32[]{:S(2)}, u32[]{:S(2)}) collective-permute-start(bf16[64,3072]{1,0:T(8,128)(2,1)} %param.12), channel_id=1, source_target_pairs={{0,1},{1,0},{2,3},{3,2},{4,5},{5,4},{6,7},{7,6},{8,9},{9,8},{10,11... | collective-permute-start | bytes 1179656 | tf_op jit(solution)/shard_map/ppermute | solution.py:76
  10.4 1.5 %copy-start.1 = (bf16[2048,256]{1,0:T(8,128)(2,1)S(1)}, bf16[2048,256]{1,0:T(8,128)(2,1)}, u32[]{:S(2)}) copy-start(bf16[2048,256]{1,0:T(8,128)(2,1)} %param.17) | copy-start | bytes 3145732
  13.1 31.4 %all-to-all-start = ((bf16[16,96,128]{2,1,0:T(8,128)(2,1)}), bf16[16,96,128]{2,1,0:T(8,128)(2,1)S(1)}, u32[]{:S(2)}, u32[]{:S(2)}) async-start(bf16[16,96,128]{2,1,0:T(8,128)(2,1)} %bitcast.1), calls=%async_computation | async-start | bytes 786432 | tf_op jit(solution)/shard_map/all_to_all | solution.py:21
  25.2 0.7 copy-start.15
  25.2 1.0 copy-start.5
  25.2 1.1 copy-start.6
  25.8 1.1 copy-start.2
  26.3 1.4 %copy-start.7 = (f32[128,64]{0,1:T(8,128)S(1)}, f32[128,64]{0,1:T(8,128)}, u32[]{:S(2)}) copy-start(f32[128,64]{0,1:T(8,128)} %param.19) | copy-start | bytes 98308
  26.3 1.4 %copy-start.9 = (f32[128,64]{0,1:T(8,128)S(1)}, f32[128,64]{0,1:T(8,128)}, u32[]{:S(2)}) copy-start(f32[128,64]{0,1:T(8,128)} %param.18) | copy-start | bytes 98308
  29.9 4.5 %collective-permute-start.1 = (bf16[128,1536]{1,0:T(8,128)(2,1)}, bf16[128,1536]{1,0:T(8,128)(2,1)}, u32[]{:S(2)}, u32[]{:S(2)}) collective-permute-start(bf16[128,1536]{1,0:T(8,128)(2,1)} %fusion.6), channel_id=1, source_target_pairs={{0,1},{1,0},{2,3},{3,2},{4,5},{5,4},{6,7},{7,6},{8,9},{9,8},{10,11... | collective-permute-start | bytes 1179656 | tf_op jit(solution)/shard_map/ppermute | solution.py:121
  44.5 36.0 %all-to-all-start.1 = ((f32[16,128,128]{2,1,0:T(8,128)}), f32[16,128,128]{2,1,0:T(8,128)S(1)}, u32[]{:S(2)}, u32[]{:S(2)}) async-start(f32[16,128,128]{2,1,0:T(8,128)} %broadcast_in_dim.8), calls=%async_computation.1 | async-start | bytes 2097152 | tf_op jit(solution)/shard_map/all_to_all | solution.py:21
  53.3 26.1 %copy-start.4 = (bf16[256,1536]{1,0:T(8,128)(2,1)S(1)}, bf16[256,1536]{1,0:T(8,128)(2,1)}, u32[]{:S(2)}) copy-start(bf16[256,1536]{1,0:T(8,128)(2,1)} %pad_maximum_fusion.2) | copy-start | bytes 2359300
  80.3 18.4 %copy-start.11 = (f32[16,64]{1,0:T(8,128)S(1)}, f32[16,64]{1,0:T(8,128)}, u32[]{:S(2)}) copy-start(f32[16,64]{1,0:T(8,128)} %param.23) | copy-start | bytes 12292
  80.3 18.4 %copy-start.12 = (f32[16,64]{1,0:T(8,128)S(1)}, f32[16,64]{1,0:T(8,128)}, u32[]{:S(2)}) copy-start(f32[16,64]{1,0:T(8,128)} %param.21) | copy-start | bytes 12292
  80.3 18.4 %copy-start.13 = (f32[16,64]{1,0:T(8,128)S(1)}, f32[16,64]{1,0:T(8,128)}, u32[]{:S(2)}) copy-start(f32[16,64]{1,0:T(8,128)} %param.22) | copy-start | bytes 12292
  80.3 18.4 %copy-start.14 = (f32[16,64]{1,0:T(8,128)S(1)}, f32[16,64]{1,0:T(8,128)}, u32[]{:S(2)}) copy-start(f32[16,64]{1,0:T(8,128)} %param.20) | copy-start | bytes 12292
  80.3 27.9 %copy-start.3 = (f32[256,256]{1,0:T(8,128)S(1)}, f32[256,256]{1,0:T(8,128)}, u32[]{:S(2)}) copy-start(f32[256,256]{1,0:T(8,128)} %fusion.22) | copy-start | bytes 786436
  80.5 28.7 %copy-start = (f32[16,128,128]{2,1,0:T(8,128)}, f32[16,128,128]{2,1,0:T(8,128)S(1)}, u32[]{:S(2)}) copy-start(f32[16,128,128]{2,1,0:T(8,128)S(1)} %all-to-all-done.1) | copy-start | bytes 3145732
  110.2 13.8 %slice-start = ((f32[16,128,128]{2,1,0:T(8,128)}), f32[10,128,128]{2,1,0:T(8,128)S(1)}, s32[]{:S(2)}) async-start(f32[16,128,128]{2,1,0:T(8,128)} %copy-done), calls=%async_computation.5 | async-start | bytes 1310720 | tf_op jit(solution)/shard_map/jit(_roll_static)/slice | solution.py:164
  110.2 13.8 %slice-start.1 = ((f32[16,128,128]{2,1,0:T(8,128)}), f32[6,128,128]{2,1,0:T(8,128)S(1)}, s32[]{:S(2)}) async-start(f32[16,128,128]{2,1,0:T(8,128)} %copy-done), calls=%async_computation.6 | async-start | bytes 786432 | tf_op jit(solution)/shard_map/jit(_roll_static)/slice | solution.py:164
  110.7 15.6 %all-to-all-start.4 = ((f32[32,1,128]{2,1,0:T(1,128)}), f32[32,1,128]{2,1,0:T(1,128)S(1)}, u32[]{:S(2)}, u32[]{:S(2)}) async-start(f32[32,1,128]{2,1,0:T(1,128)} %broadcast_in_dim.10), calls=%async_computation.4 | async-start | bytes 32768 | tf_op jit(solution)/shard_map/all_to_all | solution.py:21
  124.0 2.8 %copy-start.8 = (f32[128,64]{0,1:T(8,128)S(1)}, f32[128,64]{0,1:T(8,128)}, u32[]{:S(2)}) copy-start(f32[128,64]{0,1:T(8,128)} %param.19) | copy-start | bytes 98308
  124.0 2.8 %copy-start.10 = (f32[128,64]{0,1:T(8,128)S(1)}, f32[128,64]{0,1:T(8,128)}, u32[]{:S(2)}) copy-start(f32[128,64]{0,1:T(8,128)} %param.18) | copy-start | bytes 98308
